TPU v7x, 256 devices: a whole 4x4x8 slice. The times are simulated.
256 devices in a mesh: sp: 32 (over z, y), tp: 8 (over x, core).
Axes of the slice: x: 4, y: 4, z: 8, core: 2. Of those that a mesh axis runs over, the one named last changes fastest.
Arguments:
- target: bfloat16 [4096, 2048], P(('sp', 'tp')), may hold values from -0.119628906 to 0.119628906
- source: bfloat16 [16384, 2048], P(('sp', 'tp')), may hold values from -6 to 6
- target_gain: float32 [1, 2048], replicated, may hold values from 0.1 to 16
- source_gain: float32 [1, 2048], replicated, may hold values from 0.1 to 16
- w_query: bfloat16 [1, 2048, 4096], P(None, None, 'tp'), may hold values from -0.125 to 0.125
- w_key: bfloat16 [1, 2048, 512], P(None, None, 'tp'), may hold values from -0.125 to 0.125
- w_value: bfloat16 [1, 2048, 512], P(None, None, 'tp'), may hold values from -0.125 to 0.125
- w_out: bfloat16 [1, 4096, 2048], P(None, 'tp'), may hold values from -0.09375 to 0.09375
- final_gain: float32 [2048], replicated, may hold values from 0.1 to 1.9
Outputs:
- decoded: bfloat16 [4096, 2048], P(('sp', 'tp'))
All inputs are finite; a program needn't handle non-finite values.
Results may differ from a plain program's by a relative error of at most 0.023.
The roundings to bfloat16 on the way count: a program that leaves them out, or rounds other values in their place, can miss the bound.
Values may be sent and summed in bfloat16 or wider, within the bound.
No kernel may reach another device: no remote copies, remote signals or barrier semaphores. Data moves between devices by JAX's collectives and lax.ppermute only.
A program may use at most 128 MiB of HBM per device.

v0:
```python
import functools

import jax
import jax.numpy as jnp
from jax import lax
from jax.experimental import pallas as pl
from jax.experimental.pallas import tpu as pltpu
from jax.sharding import Mesh, PartitionSpec as P

HD = 512
EPSILON = 1e-06
BF = jnp.bfloat16
F32 = jnp.float32
NZ, NY, NX, NC = 8, 4, 4, 2
EXTRA = 16
VMEM = pl.BlockSpec(memory_space=pltpu.VMEM)
ANY = pl.BlockSpec(memory_space=pl.ANY)


def room(mib):
    return pltpu.CompilerParams(vmem_limit_bytes=mib << 20)


def norm_rows(matrix, gain):
    values32 = matrix.astype(F32)
    scale = lax.rsqrt(jnp.mean(values32 * values32, axis=-1, keepdims=True) + EPSILON)
    return values32 * scale * gain


def moved(array, axis, shift):
    n = lax.axis_size(axis)
    return lax.ppermute(array, axis, [(i, (i + shift) % n) for i in range(n)])


def ring4(array, axis):
    far = moved(array, axis, 2)
    one = moved(array, axis, 1)
    back = moved(array, axis, -1)
    return [array, one, far, back]


def norm_kernel(source, target, source_gain, target_gain, source_out, target_out):
    source_out[...] = norm_rows(source[...], source_gain[...]).astype(BF)
    target_out[...] = norm_rows(target[...], target_gain[...]).astype(BF)


def normed_inputs(source, target, source_gain, target_gain):
    return pl.pallas_call(
        norm_kernel,
        out_shape=[jax.ShapeDtypeStruct(source.shape, BF), jax.ShapeDtypeStruct(target.shape, BF)],
        in_specs=[VMEM] * 4,
        out_specs=[VMEM] * 2,
        compiler_params=room(8),
    )(source, target, source_gain, target_gain)


def key_value_kernel(*refs):
    blocks = refs[:NX]
    own_w, other_w, kept_out, sent_out, rows, sems = refs[NX:]
    x = lax.axis_index("x")
    first = lax.axis_index("c") == 0
    copies = []
    for k in range(NX):
        place = pl.multiple_of(lax.rem(x - k + NX, NX) * 64, 64)
        copies.append(pltpu.make_async_copy(blocks[k], rows.at[pl.ds(place, 64), :], sems.at[k]))
    for copy in copies:
        copy.start()
    for copy in copies:
        copy.wait()

    def projected(weight):
        return lax.dot_general(
            weight[...], rows[...], (((1,), (1,)), ((), ())), preferred_element_type=F32)

    own, other = projected(own_w), projected(other_w)
    low = jnp.where(first, own, other)
    high = jnp.where(first, other, own)
    keys = jnp.concatenate([low[:64], high[:64]], axis=0).T
    turned = jnp.concatenate([low[64:], high[64:]], axis=0)
    values = jnp.concatenate([turned[:, :128], turned[:, 128:]], axis=0)
    kept_out[...] = jnp.where(first, keys, values).astype(BF)
    sent_out[...] = jnp.where(first, values, keys).astype(BF)


def key_value(blocks, own_w, other_w):
    return pl.pallas_call(
        key_value_kernel,
        out_shape=[jax.ShapeDtypeStruct((256, 128), BF)] * 2,
        in_specs=[ANY] * NX + [VMEM] * 2,
        out_specs=[VMEM] * 2,
        scratch_shapes=[pltpu.VMEM((256, 2048), BF), pltpu.SemaphoreType.DMA((NX,))],
        compiler_params=room(12),
        cost_estimate=pl.CostEstimate(
            flops=2 * 256 * 2048 * 256, bytes_accessed=3 << 20, transcendentals=0),
    )(*blocks, own_w, other_w)


def query_kernel(*refs):
    weight, out, full = refs[NX:]
    x = lax.axis_index("x")
    rows = jnp.concatenate([ref[...] for ref in refs[:NX]], axis=0)
    full[...] = jnp.dot(rows, weight[...], preferred_element_type=F32)
    for k in range(NX):
        place = pl.multiple_of(lax.rem(x - k + NX, NX) * 128, 128)
        block = full[:, pl.ds(place, 128)].astype(BF)
        for copy in range(NZ):
            out[copy, :, pl.ds(k * 128, 128)] = block


def query_rows(blocks, weight):
    return pl.pallas_call(
        query_kernel,
        out_shape=jax.ShapeDtypeStruct((NZ, 128, HD), BF),
        in_specs=[VMEM] * (NX + 1),
        out_specs=VMEM,
        scratch_shapes=[pltpu.VMEM((128, HD), F32)],
        compiler_params=room(12),
        cost_estimate=pl.CostEstimate(
            flops=2 * 128 * 2048 * HD, bytes_accessed=3 << 20, transcendentals=0),
    )(*blocks, weight)


def soft_part(q, keys, values, outs):
    scores = []
    for m in range(NY):
        block = jnp.concatenate([keys[m, k] for k in range(NX)], axis=1)
        scores.append(lax.dot_general(
            block, q, (((1,), (1,)), ((), ())), preferred_element_type=F32) * HD ** (-0.5))
    top = functools.reduce(
        jnp.maximum, [jnp.max(score, axis=0, keepdims=True) for score in scores])
    total, numerator = 0.0, 0.0
    for m in range(NY):
        weights = jnp.exp(scores[m] - top)
        total = total + jnp.sum(weights, axis=0, keepdims=True)
        block = jnp.concatenate([
            jnp.concatenate(
                [values[k, m, pl.ds(row, 128), :] for row in (256, 384, 0, 128)], axis=1)
            for k in range(NX)], axis=0)
        numerator = numerator + jnp.dot(
            block, weights.astype(BF), preferred_element_type=F32)
    part = numerator / total
    for side, out in enumerate(outs):
        cols = slice(side * 128, side * 128 + 128)
        out[pl.ds(0, HD), :] = part[:, cols].astype(BF)
        pieces = []
        for stat in (top[:, cols], total[:, cols]):
            for _ in range(3):
                piece = stat.astype(BF).astype(F32)
                pieces.append(piece)
                stat = stat - piece
        pieces.append(jnp.zeros((EXTRA - 6, 128), F32))
        out[pl.ds(HD, EXTRA), :] = jnp.concatenate(pieces, axis=0).astype(BF)


def attend_kernel(*refs):
    n = (len(refs) - 11) // 2
    near, other = refs[n : n + NX], refs[n + NX : n + 2 * NX]
    outs = refs[n + 8 : 2 * n + 8]
    keys, values, sems = refs[2 * n + 8 :]
    core = lax.axis_index("c")

    def copies(key_blocks, value_blocks):
        return [
            pltpu.make_async_copy(block, place.at[i], sems.at[side * 4 + i])
            for side, (blocks, place) in enumerate(((key_blocks, keys), (value_blocks, values)))
            for i, block in enumerate(blocks)]

    @pl.when(core == 0)
    def _():
        for copy in copies(near, other):
            copy.start()

    @pl.when(core == 1)
    def _():
        for copy in copies(other, near):
            copy.start()

    for copy in copies(near, other):
        copy.wait()
    for i in range(0, n, 2):
        q = jnp.concatenate([ref[...] for ref in refs[i : i + 2]], axis=0)
        soft_part(q, keys, values, outs[i : i + 2])


def attend(queries, near, other):
    n = len(queries)
    return pl.pallas_call(
        attend_kernel,
        out_shape=[jax.ShapeDtypeStruct((HD + EXTRA, 128), BF)] * n,
        in_specs=[VMEM] * n + [ANY] * 8,
        out_specs=[VMEM] * n,
        scratch_shapes=[pltpu.VMEM((4, 4, 512, 128), BF)] * 2 + [pltpu.SemaphoreType.DMA((8,))],
        compiler_params=room(28),
        cost_estimate=pl.CostEstimate(
            flops=4 * 128 * n * 2048 * HD, bytes_accessed=4 << 20,
            transcendentals=n * 128 * 2048),
    )(*queries, *near, *other)


def combine_kernel(*refs):
    arrived = refs[:NZ]
    weight, kept, sent, attended = refs[NZ:]
    x = lax.axis_index("x")
    tops, totals = [], []
    for part in arrived:
        stats = part[pl.ds(HD, EXTRA), :].astype(F32)
        tops.append(stats[0:1] + stats[1:2] + stats[2:3])
        totals.append(stats[3:4] + stats[4:5] + stats[5:6])
    top = functools.reduce(jnp.maximum, tops)
    shares = [total * jnp.exp(t - top) for t, total in zip(tops, totals)]
    whole = sum(shares)
    shares = [share / whole for share in shares]
    for k in range(NX):
        block = sum(
            part[pl.ds(k * 128, 128), :].astype(F32) * share
            for part, share in zip(arrived, shares))
        place = pl.multiple_of(lax.rem(x - k + NX, NX) * 128, 128)
        attended[:, pl.ds(place, 128)] = block.T.astype(BF)
    projected = jnp.dot(attended[...], weight[...], preferred_element_type=F32)
    for k in range(NX):
        kept[pl.ds(k * 16, 16), :] = projected[k * 32 : k * 32 + 16]
        sent[pl.ds(k * 16, 16), :] = projected[k * 32 + 16 : k * 32 + 32].astype(BF)


def combine(arrived, weight):
    return pl.pallas_call(
        combine_kernel,
        out_shape=[jax.ShapeDtypeStruct((64, 2048), F32), jax.ShapeDtypeStruct((64, 2048), BF)],
        in_specs=[VMEM] * (NZ + 1),
        out_specs=[VMEM] * 2,
        scratch_shapes=[pltpu.VMEM((128, HD), BF)],
        compiler_params=room(16),
        cost_estimate=pl.CostEstimate(
            flops=2 * 128 * 2048 * HD, bytes_accessed=4 << 20, transcendentals=1024),
    )(*arrived, weight)


def pair_kernel(kept, met, own, *outs):
    own[...] = kept[pl.ds(0, 16), :] + met[pl.ds(0, 16), :].astype(F32)
    for k, out in enumerate(outs, 1):
        rows = pl.ds(k * 16, 16)
        out[...] = (kept[rows, :] + met[rows, :].astype(F32)).astype(BF)


def pair_sum(kept, met):
    return pl.pallas_call(
        pair_kernel,
        out_shape=[jax.ShapeDtypeStruct((16, 2048), F32)]
        + [jax.ShapeDtypeStruct((16, 2048), BF)] * 3,
        in_specs=[VMEM] * 2,
        out_specs=[VMEM] * 4,
        compiler_params=room(8),
    )(kept, met)


def last_kernel(target, own, one, two, three, gain, out):
    stream = target[...].astype(F32) + (
        own[...] + one[...].astype(F32) + two[...].astype(F32) + three[...].astype(F32))
    out[...] = norm_rows(stream, gain[...]).astype(BF)


def last_norm(*arrays):
    return pl.pallas_call(
        last_kernel,
        out_shape=jax.ShapeDtypeStruct((16, 2048), BF),
        in_specs=[VMEM] * 6,
        out_specs=VMEM,
        compiler_params=room(8),
    )(*arrays)


def by_role(array, shift, axes):
    pairs = []
    for y in range(NY):
        for x in range(NX):
            for core, axis in enumerate(axes):
                to_y = (y + shift) % NY if axis == "y" else y
                to_x = (x + shift) % NX if axis == "x" else x
                pairs.append((((y * NX) + x) * NC + core, ((to_y * NX) + to_x) * NC + core))
    return lax.ppermute(array, ("y", "x", "c"), pairs)


def role_ring4(array, axes):
    far = by_role(array, 2, axes)
    one = by_role(array, 1, axes)
    back = by_role(array, -1, axes)
    return [array, one, far, back]


def on_device(target, source, target_gain, source_gain, w_query, w_key, w_value, w_out, final_gain):
    rows, normed = normed_inputs(source, target, source_gain, target_gain)
    other_normed = moved(normed, "c", 1)
    rows, other_normed = lax.optimization_barrier((rows, other_normed))
    chip_normed = jnp.concatenate([normed, other_normed], axis=0)
    row_blocks = ring4(rows, "x")
    target_blocks = ring4(chip_normed, "x")
    copies = query_rows(target_blocks, w_query[0])
    queries = lax.all_to_all(copies, "z", 0, 0, tiled=True)

    own_w = jnp.concatenate([w_key[0].T, w_value[0].T], axis=0)
    other_w = moved(own_w, "c", 1)

    piece, sent = key_value(row_blocks, own_w, other_w)
    piece = jnp.concatenate([piece, moved(sent, "c", 1)], axis=0)
    line = jnp.stack(role_ring4(piece, ("x", "y")))
    near = role_ring4(line, ("y", "x"))
    other = [moved(block, "c", 1) for block in near]

    z = lax.axis_index("z")
    picked = [
        lax.dynamic_slice(queries, (lax.rem(z - k + NZ, NZ), 0, 0), (1, 128, HD)).reshape(128, HD)
        for k in range(NZ)]
    parts = dict(zip((4, 3), attend([picked[4], picked[3]], near, other)))
    arrived = []
    for k in (4, 3):
        arrived.append(moved(parts[k], "z", -k))
    rest = (5, 2, 6, 1, 7, 0)
    parts.update(zip(rest, attend([picked[k] for k in rest], near, other)))
    for k in rest[:-1]:
        arrived.append(moved(parts[k], "z", -k))
    arrived.append(parts[0])
    kept, sent = combine(arrived, w_out[0])
    met = moved(sent, "c", 1)
    own, one, two, three = pair_sum(kept, met)
    two = moved(two, "x", -2)
    one = moved(one, "x", -1)
    three = moved(three, "x", -3)
    return last_norm(target, own, one, two, three, final_gain.reshape(1, -1))


def solution(mesh):
    grid = Mesh(mesh.devices.reshape(NZ, NY, NX, NC), ("z", "y", "x", "c"))
    every = P(("z", "y", "x", "c"), None)
    in_specs = (
        every, every, P(), P(),
        P(None, None, ("x", "c")), P(None, None, ("x", "c")), P(None, None, ("x", "c")),
        P(None, ("x", "c"), None), P(),
    )
    return jax.shard_map(
        on_device, mesh=grid, in_specs=in_specs, out_specs=every, check_vma=False)
```

profile of v0, /device:TPU:1, one launch (start us, length us, event | category | flops | bytes accessed | tf_op | source)
XLA Modules:
  0.0 126.2 jit_solution(12765568599958202809)
XLA Ops:
  3.4 3.3 %collective-permute-start = (bf16[16,2048]{1,0:T(8,128)(2,1)S(1)}, bf16[16,2048]{1,0:T(8,128)(2,1)S(1)}, u32[]{:S(2)}, u32[]{:S(2)}) collective-permute-start(bf16[16,2048]{1,0:T(8,128)(2,1)S(1)} %get-tuple-element.25), channel_id=1, source_target_pairs={{0,1},{1,0},{2,3},{3,2},{4,5},{5,4},{6,7},{7,6},{8,9},{9,8},{10,11... | collective-permute-start | bytes 196616 | tf_op jit(solution)/shard_map/ppermute | solution.py:32
  7.6 1.9 %collective-permute-start.2 = (bf16[32,2048]{1,0:T(8,128)(2,1)S(1)}, bf16[32,2048]{1,0:T(8,128)(2,1)S(1)}, u32[]{:S(2)}, u32[]{:S(2)}) collective-permute-start(bf16[32,2048]{1,0:T(8,128)(2,1)S(1)} %constant_dynamic-update-slice_fusion.refs_0_), channel_id=1, source_target_pairs={{0,4},{2,6},{4,0},{6,2},{1,5},{3,7},{5,1},{7,3},{8,12},{10,14},{12... | collective-permute-start | bytes 393224 | tf_op jit(solution)/shard_map/ppermute | solution.py:32
  19.7 7.2 %all-to-all-start = ((bf16[8,128,512]{2,1,0:T(8,128)(2,1)}), bf16[8,128,512]{2,1,0:T(8,128)(2,1)}, u32[]{:S(2)}, u32[]{:S(2)}) async-start(bf16[8,128,512]{2,1,0:T(8,128)(2,1)} %shard_map.92), calls=%async_computation | async-start | bytes 2097152 | tf_op jit(solution)/shard_map/all_to_all | solution.py:298
  28.0 2.2 %collective-permute-start.5 = (bf16[64,2048]{1,0:T(8,128)(2,1)S(1)}, bf16[64,2048]{1,0:T(8,128)(2,1)S(1)}, u32[]{:S(2)}, u32[]{:S(2)}) collective-permute-start(bf16[64,2048]{1,0:T(8,128)(2,1)S(1)} %get-tuple-element.28.refs_0_), channel_id=1, source_target_pairs={{0,4},{2,6},{4,0},{6,2},{1,5},{3,7},{5,1},{7,3},{8,12},{10,14},{12... | collective-permute-start | bytes 786440 | tf_op jit(solution)/shard_map/ppermute | solution.py:32
  31.1 3.4 %collective-permute-done.4.refs_1_ = bf16[64,2048]{1,0:T(8,128)(2,1)S(1)} collective-permute-done((bf16[64,2048]{1,0:T(8,128)(2,1)S(1)}, bf16[64,2048]{1,0:T(8,128)(2,1)S(1)}, u32[]{:S(2)}, u32[]{:S(2)}) %collective-permute-start.4) | collective-permute-done | bytes 262176 | tf_op jit(solution)/shard_map/ppermute | solution.py:32
  34.5 6.5 %collective-permute-done.5.refs_2_ = bf16[64,2048]{1,0:T(8,128)(2,1)S(1)} collective-permute-done((bf16[64,2048]{1,0:T(8,128)(2,1)S(1)}, bf16[64,2048]{1,0:T(8,128)(2,1)S(1)}, u32[]{:S(2)}, u32[]{:S(2)}) %collective-permute-start.5) | collective-permute-done | bytes 262176 | tf_op jit(solution)/shard_map/ppermute | solution.py:32
  42.3 1.9 %collective-permute-start.8 = (bf16[256,128]{1,0:T(8,128)(2,1)S(1)}, bf16[256,128]{1,0:T(8,128)(2,1)S(1)}, u32[]{:S(2)}, u32[]{:S(2)}) collective-permute-start(bf16[256,128]{1,0:T(8,128)(2,1)S(1)} %get-tuple-element.30), channel_id=1, source_target_pairs={{0,1},{1,0},{2,3},{3,2},{4,5},{5,4},{6,7},{7,6},{8,9},{9,8},{10,11... | collective-permute-start | bytes 196616 | tf_op jit(solution)/shard_map/ppermute | solution.py:32
  45.1 2.8 %collective-permute-start.11 = (bf16[512,128]{1,0:T(8,128)(2,1)S(1)}, bf16[512,128]{1,0:T(8,128)(2,1)S(1)}, u32[]{:S(2)}, u32[]{:S(2)}) collective-permute-start(bf16[512,128]{1,0:T(8,128)(2,1)S(1)} %constant_dynamic-update-slice_fusion.2), channel_id=1, source_target_pairs={{0,6},{1,25},{2,0},{3,27},{4,2},{5,29},{6,4},{7,31},{8,14},{9,1},{... | collective-permute-start | bytes 393224 | tf_op jit(solution)/shard_map/ppermute | solution.py:280
  49.0 2.3 %collective-permute-done.11 = bf16[512,128]{1,0:T(8,128)(2,1)S(1)} collective-permute-done((bf16[512,128]{1,0:T(8,128)(2,1)S(1)}, bf16[512,128]{1,0:T(8,128)(2,1)S(1)}, u32[]{:S(2)}, u32[]{:S(2)}) %collective-permute-start.11) | collective-permute-done | bytes 131104 | tf_op jit(solution)/shard_map/ppermute | solution.py:280
  51.2 2.4 %collective-permute-done.10 = bf16[512,128]{1,0:T(8,128)(2,1)S(1)} collective-permute-done((bf16[512,128]{1,0:T(8,128)(2,1)S(1)}, bf16[512,128]{1,0:T(8,128)(2,1)S(1)}, u32[]{:S(2)}, u32[]{:S(2)}) %collective-permute-start.10) | collective-permute-done | bytes 131104 | tf_op jit(solution)/shard_map/ppermute | solution.py:280
  56.6 2.1 %collective-permute-start.13 = (bf16[4,512,128]{2,1,0:T(8,128)(2,1)S(1)}, bf16[4,512,128]{2,1,0:T(8,128)(2,1)S(1)}, u32[]{:S(2)}, u32[]{:S(2)}) collective-permute-start(bf16[4,512,128]{2,1,0:T(8,128)(2,1)S(1)} %pad_maximum_fusion.1.refs_2_.refs_6_), channel_id=1, source_target_pairs={{0,16},{1,5},{2,18},{3,7},{4,20},{5,1},{6,22},{7,3},{8,24},{9,13},... | collective-permute-start | bytes 1572872 | tf_op jit(solution)/shard_map/ppermute | solution.py:280
  59.4 2.6 %collective-permute-start.15 = (bf16[4,512,128]{2,1,0:T(8,128)(2,1)S(1)}, bf16[4,512,128]{2,1,0:T(8,128)(2,1)S(1)}, u32[]{:S(2)}, u32[]{:S(2)}) collective-permute-start(bf16[4,512,128]{2,1,0:T(8,128)(2,1)S(1)} %pad_maximum_fusion.1.refs_2_.refs_6_), channel_id=1, source_target_pairs={{0,1},{1,0},{2,3},{3,2},{4,5},{5,4},{6,7},{7,6},{8,9},{9,8},{10,11... | collective-permute-start | bytes 1572872 | tf_op jit(solution)/shard_map/ppermute | solution.py:32
  62.0 2.7 %collective-permute-done.12.refs_3_.refs_7_ = bf16[4,512,128]{2,1,0:T(8,128)(2,1)S(1)} collective-permute-done((bf16[4,512,128]{2,1,0:T(8,128)(2,1)S(1)}, bf16[4,512,128]{2,1,0:T(8,128)(2,1)S(1)}, u32[]{:S(2)}, u32[]{:S(2)}) %collective-permute-start.12) | collective-permute-done | bytes 524320 | tf_op jit(solution)/shard_map/ppermute | solution.py:280
  66.6 4.6 %collective-permute-done.13.refs_4_.refs_8_ = bf16[4,512,128]{2,1,0:T(8,128)(2,1)S(1)} collective-permute-done((bf16[4,512,128]{2,1,0:T(8,128)(2,1)S(1)}, bf16[4,512,128]{2,1,0:T(8,128)(2,1)S(1)}, u32[]{:S(2)}, u32[]{:S(2)}) %collective-permute-start.13) | collective-permute-done | bytes 524320 | tf_op jit(solution)/shard_map/ppermute | solution.py:280
  71.2 2.2 %collective-permute-start.17 = (bf16[4,512,128]{2,1,0:T(8,128)(2,1)S(1)}, bf16[4,512,128]{2,1,0:T(8,128)(2,1)}, u32[]{:S(2)}, u32[]{:S(2)}) collective-permute-start(bf16[4,512,128]{2,1,0:T(8,128)(2,1)S(1)} %collective-permute-done.13.refs_4_.refs_8_), channel_id=1, source_target_pairs={{0,1},{1,0},{2,3},{3,2},{4,5},{5,4},{6,7},{7,6},{8,9},{9,8},{10,11... | collective-permute-start | bytes 1572872 | tf_op jit(solution)/shard_map/ppermute | solution.py:32
  75.8 4.2 %shard_map.94 = (bf16[528,128]{1,0:T(8,128)(2,1)S(1)}, bf16[528,128]{1,0:T(8,128)(2,1)S(1)}) custom-call(bf16[128,512]{1,0:T(8,128)(2,1)S(1)} %get-tuple-element.52.refs_0_, bf16[128,512]{1,0:T(8,128)(2,1)S(1)} %get-tuple-element.51.refs_1_, bf16[4,512,128]{2,1,0:T(8,128)(2,1)S(1)} %pad_maximum_fusion.1.refs_2_.refs_6_, ...), custom_call_target="tpu_custom_call" | custom-call | flops 1073741824 | bytes 4194304 | tf_op jit(solution)/shard_map/pallas_call | solution.py:187
  80.0 5.5 %collective-permute-start.19 = (bf16[528,128]{1,0:T(8,128)(2,1)S(1)}, bf16[528,128]{1,0:T(8,128)(2,1)S(1)}, u32[]{:S(2)}, u32[]{:S(2)}) collective-permute-start(bf16[528,128]{1,0:T(8,128)(2,1)S(1)} %get-tuple-element.31), channel_id=1, source_target_pairs={{0,128},{32,160},{64,192},{96,224},{128,0},{160,32},{192,64},{224,... | collective-permute-start | bytes 405512 | tf_op jit(solution)/shard_map/ppermute | solution.py:32
  85.8 7.2 %shard_map.95 = (bf16[528,128]{1,0:T(8,128)(2,1)S(1)}, bf16[528,128]{1,0:T(8,128)(2,1)S(1)}, bf16[528,128]{1,0:T(8,128)(2,1)S(1)}, bf16[528,128]{1,0:T(8,128)(2,...) custom-call(bf16[128,512]{1,0:T(8,128)(2,1)S(1)} %get-tuple-element.50.refs_0_, ...), custom_call_target="tpu_custom_call" | custom-call | flops 3221225472 | bytes 4194304 | tf_op jit(solution)/shard_map/pallas_call | solution.py:187
  93.0 3.1 %collective-permute-start.21 = (bf16[528,128]{1,0:T(8,128)(2,1)S(1)}, bf16[528,128]{1,0:T(8,128)(2,1)S(1)}, u32[]{:S(2)}, u32[]{:S(2)}) collective-permute-start(bf16[528,128]{1,0:T(8,128)(2,1)S(1)} %get-tuple-element.33), channel_id=1, source_target_pairs={{0,96},{32,128},{64,160},{96,192},{128,224},{160,0},{192,32},{224,... | collective-permute-start | bytes 405512 | tf_op jit(solution)/shard_map/ppermute | solution.py:32
  98.4 2.7 %collective-permute-start.24 = (bf16[528,128]{1,0:T(8,128)(2,1)S(1)}, bf16[528,128]{1,0:T(8,128)(2,1)S(1)}, u32[]{:S(2)}, u32[]{:S(2)}) collective-permute-start(bf16[528,128]{1,0:T(8,128)(2,1)S(1)} %get-tuple-element.36), channel_id=1, source_target_pairs={{0,224},{32,0},{64,32},{96,64},{128,96},{160,128},{192,160},{224,1... | collective-permute-start | bytes 405512 | tf_op jit(solution)/shard_map/ppermute | solution.py:32
  101.2 6.5 %collective-permute-done.21.refs_2_ = bf16[528,128]{1,0:T(8,128)(2,1)S(1)} collective-permute-done((bf16[528,128]{1,0:T(8,128)(2,1)S(1)}, bf16[528,128]{1,0:T(8,128)(2,1)S(1)}, u32[]{:S(2)}, u32[]{:S(2)}) %collective-permute-start.21) | collective-permute-done | bytes 135200 | tf_op jit(solution)/shard_map/ppermute | solution.py:32
  107.7 3.3 %collective-permute-done.23.refs_4_ = bf16[528,128]{1,0:T(8,128)(2,1)S(1)} collective-permute-done((bf16[528,128]{1,0:T(8,128)(2,1)S(1)}, bf16[528,128]{1,0:T(8,128)(2,1)S(1)}, u32[]{:S(2)}, u32[]{:S(2)}) %collective-permute-start.23) | collective-permute-done | bytes 135200 | tf_op jit(solution)/shard_map/ppermute | solution.py:32
  111.0 4.5 %collective-permute-done.25.refs_6_ = bf16[528,128]{1,0:T(8,128)(2,1)S(1)} collective-permute-done((bf16[528,128]{1,0:T(8,128)(2,1)S(1)}, bf16[528,128]{1,0:T(8,128)(2,1)S(1)}, u32[]{:S(2)}, u32[]{:S(2)}) %collective-permute-start.25) | collective-permute-done | bytes 135200 | tf_op jit(solution)/shard_map/ppermute | solution.py:32
  123.6 1.8 %collective-permute-done.29.three = bf16[16,2048]{1,0:T(8,128)(2,1)S(1)} collective-permute-done((bf16[16,2048]{1,0:T(8,128)(2,1)S(1)}, bf16[16,2048]{1,0:T(8,128)(2,1)S(1)}, u32[]{:S(2)}, u32[]{:S(2)}) %collective-permute-start.29) | collective-permute-done | bytes 65568 | tf_op jit(solution)/shard_map/ppermute | solution.py:32
  (69 shorter events, 39.1 us)
Async XLA Ops:
  7.6 6.6 %collective-permute-start.1 = (bf16[32,2048]{1,0:T(8,128)(2,1)S(1)}, bf16[32,2048]{1,0:T(8,128)(2,1)S(1)}, u32[]{:S(2)}, u32[]{:S(2)}) collective-permute-start(bf16[32,2048]{1,0:T(8,128)(2,1)S(1)} %constant_dynamic-update-slice_fusion.refs_0_), channel_id=1, source_target_pairs={{0,2},{2,4},{4,6},{6,0},{1,3},{3,5},{5,7},{7,1},{8,10},{10,12},{12... | collective-permute-start | bytes 393224 | tf_op jit(solution)/shard_map/ppermute | solution.py:32
  7.6 8.0 %collective-permute-start.2 = (bf16[32,2048]{1,0:T(8,128)(2,1)S(1)}, bf16[32,2048]{1,0:T(8,128)(2,1)S(1)}, u32[]{:S(2)}, u32[]{:S(2)}) collective-permute-start(bf16[32,2048]{1,0:T(8,128)(2,1)S(1)} %constant_dynamic-update-slice_fusion.refs_0_), channel_id=1, source_target_pairs={{0,4},{2,6},{4,0},{6,2},{1,5},{3,7},{5,1},{7,3},{8,12},{10,14},{12... | collective-permute-start | bytes 393224 | tf_op jit(solution)/shard_map/ppermute | solution.py:32
  9.5 7.1 %collective-permute-start.3 = (bf16[32,2048]{1,0:T(8,128)(2,1)S(1)}, bf16[32,2048]{1,0:T(8,128)(2,1)S(1)}, u32[]{:S(2)}, u32[]{:S(2)}) collective-permute-start(bf16[32,2048]{1,0:T(8,128)(2,1)S(1)} %constant_dynamic-update-slice_fusion.refs_0_), channel_id=1, source_target_pairs={{0,6},{2,0},{4,2},{6,4},{1,7},{3,1},{5,3},{7,5},{8,14},{10,8},{12,... | collective-permute-start | bytes 393224 | tf_op jit(solution)/shard_map/ppermute | solution.py:32
  11.7 29.6 %collective-permute-start.7 = (bf16[128,2048]{1,0:T(8,128)(2,1)S(1)}, bf16[128,2048]{1,0:T(8,128)(2,1)S(1)}, u32[]{:S(2)}, u32[]{:S(2)}) collective-permute-start(bf16[128,2048]{1,0:T(8,128)(2,1)S(1)} %pad_maximum_fusion.refs_4_), channel_id=1, source_target_pairs={{0,1},{1,0},{2,3},{3,2},{4,5},{5,4},{6,7},{7,6},{8,9},{9,8},{10,11... | collective-permute-start | bytes 1572872 | tf_op jit(solution)/shard_map/ppermute | solution.py:32
  19.7 53.7 %all-to-all-start = ((bf16[8,128,512]{2,1,0:T(8,128)(2,1)}), bf16[8,128,512]{2,1,0:T(8,128)(2,1)}, u32[]{:S(2)}, u32[]{:S(2)}) async-start(bf16[8,128,512]{2,1,0:T(8,128)(2,1)} %shard_map.92), calls=%async_computation | async-start | bytes 2097152 | tf_op jit(solution)/shard_map/all_to_all | solution.py:298
  26.9 7.6 %collective-permute-start.4 = (bf16[64,2048]{1,0:T(8,128)(2,1)S(1)}, bf16[64,2048]{1,0:T(8,128)(2,1)S(1)}, u32[]{:S(2)}, u32[]{:S(2)}) collective-permute-start(bf16[64,2048]{1,0:T(8,128)(2,1)S(1)} %get-tuple-element.28.refs_0_), channel_id=1, source_target_pairs={{0,2},{2,4},{4,6},{6,0},{1,3},{3,5},{5,7},{7,1},{8,10},{10,12},{12... | collective-permute-start | bytes 786440 | tf_op jit(solution)/shard_map/ppermute | solution.py:32
  28.0 13.0 %collective-permute-start.5 = (bf16[64,2048]{1,0:T(8,128)(2,1)S(1)}, bf16[64,2048]{1,0:T(8,128)(2,1)S(1)}, u32[]{:S(2)}, u32[]{:S(2)}) collective-permute-start(bf16[64,2048]{1,0:T(8,128)(2,1)S(1)} %get-tuple-element.28.refs_0_), channel_id=1, source_target_pairs={{0,4},{2,6},{4,0},{6,2},{1,5},{3,7},{5,1},{7,3},{8,12},{10,14},{12... | collective-permute-start | bytes 786440 | tf_op jit(solution)/shard_map/ppermute | solution.py:32
  30.2 11.1 %collective-permute-start.6 = (bf16[64,2048]{1,0:T(8,128)(2,1)S(1)}, bf16[64,2048]{1,0:T(8,128)(2,1)S(1)}, u32[]{:S(2)}, u32[]{:S(2)}) collective-permute-start(bf16[64,2048]{1,0:T(8,128)(2,1)S(1)} %get-tuple-element.28.refs_0_), channel_id=1, source_target_pairs={{0,6},{2,0},{4,2},{6,4},{1,7},{3,1},{5,3},{7,5},{8,14},{10,8},{12,... | collective-permute-start | bytes 786440 | tf_op jit(solution)/shard_map/ppermute | solution.py:32
  45.1 6.1 %collective-permute-start.11 = (bf16[512,128]{1,0:T(8,128)(2,1)S(1)}, bf16[512,128]{1,0:T(8,128)(2,1)S(1)}, u32[]{:S(2)}, u32[]{:S(2)}) collective-permute-start(bf16[512,128]{1,0:T(8,128)(2,1)S(1)} %constant_dynamic-update-slice_fusion.2), channel_id=1, source_target_pairs={{0,6},{1,25},{2,0},{3,27},{4,2},{5,29},{6,4},{7,31},{8,14},{9,1},{... | collective-permute-start | bytes 393224 | tf_op jit(solution)/shard_map/ppermute | solution.py:280
  47.9 5.7 %collective-permute-start.10 = (bf16[512,128]{1,0:T(8,128)(2,1)S(1)}, bf16[512,128]{1,0:T(8,128)(2,1)S(1)}, u32[]{:S(2)}, u32[]{:S(2)}) collective-permute-start(bf16[512,128]{1,0:T(8,128)(2,1)S(1)} %constant_dynamic-update-slice_fusion.2), channel_id=1, source_target_pairs={{0,4},{1,17},{2,6},{3,19},{4,0},{5,21},{6,2},{7,23},{8,12},{9,25},... | collective-permute-start | bytes 393224 | tf_op jit(solution)/shard_map/ppermute | solution.py:280
  48.3 6.8 %collective-permute-start.9 = (bf16[512,128]{1,0:T(8,128)(2,1)S(1)}, bf16[512,128]{1,0:T(8,128)(2,1)S(1)}, u32[]{:S(2)}, u32[]{:S(2)}) collective-permute-start(bf16[512,128]{1,0:T(8,128)(2,1)S(1)} %constant_dynamic-update-slice_fusion.2), channel_id=1, source_target_pairs={{0,2},{1,9},{2,4},{3,11},{4,6},{5,13},{6,0},{7,15},{8,10},{9,17},{... | collective-permute-start | bytes 393224 | tf_op jit(solution)/shard_map/ppermute | solution.py:280
  55.1 9.6 %collective-permute-start.12 = (bf16[4,512,128]{2,1,0:T(8,128)(2,1)S(1)}, bf16[4,512,128]{2,1,0:T(8,128)(2,1)S(1)}, u32[]{:S(2)}, u32[]{:S(2)}) collective-permute-start(bf16[4,512,128]{2,1,0:T(8,128)(2,1)S(1)} %pad_maximum_fusion.1.refs_2_.refs_6_), channel_id=1, source_target_pairs={{0,8},{1,3},{2,10},{3,5},{4,12},{5,7},{6,14},{7,1},{8,16},{9,11},{... | collective-permute-start | bytes 1572872 | tf_op jit(solution)/shard_map/ppermute | solution.py:280
  56.6 14.6 %collective-permute-start.13 = (bf16[4,512,128]{2,1,0:T(8,128)(2,1)S(1)}, bf16[4,512,128]{2,1,0:T(8,128)(2,1)S(1)}, u32[]{:S(2)}, u32[]{:S(2)}) collective-permute-start(bf16[4,512,128]{2,1,0:T(8,128)(2,1)S(1)} %pad_maximum_fusion.1.refs_2_.refs_6_), channel_id=1, source_target_pairs={{0,16},{1,5},{2,18},{3,7},{4,20},{5,1},{6,22},{7,3},{8,24},{9,13},... | collective-permute-start | bytes 1572872 | tf_op jit(solution)/shard_map/ppermute | solution.py:280
  58.7 14.7 %collective-permute-start.14 = (bf16[4,512,128]{2,1,0:T(8,128)(2,1)S(1)}, bf16[4,512,128]{2,1,0:T(8,128)(2,1)S(1)}, u32[]{:S(2)}, u32[]{:S(2)}) collective-permute-start(bf16[4,512,128]{2,1,0:T(8,128)(2,1)S(1)} %pad_maximum_fusion.1.refs_2_.refs_6_), channel_id=1, source_target_pairs={{0,24},{1,7},{2,26},{3,1},{4,28},{5,3},{6,30},{7,5},{8,0},{9,15},{... | collective-permute-start | bytes 1572872 | tf_op jit(solution)/shard_map/ppermute | solution.py:280
  59.4 15.4 %collective-permute-start.15 = (bf16[4,512,128]{2,1,0:T(8,128)(2,1)S(1)}, bf16[4,512,128]{2,1,0:T(8,128)(2,1)S(1)}, u32[]{:S(2)}, u32[]{:S(2)}) collective-permute-start(bf16[4,512,128]{2,1,0:T(8,128)(2,1)S(1)} %pad_maximum_fusion.1.refs_2_.refs_6_), channel_id=1, source_target_pairs={{0,1},{1,0},{2,3},{3,2},{4,5},{5,4},{6,7},{7,6},{8,9},{9,8},{10,11... | collective-permute-start | bytes 1572872 | tf_op jit(solution)/shard_map/ppermute | solution.py:32
  64.7 10.1 %collective-permute-start.16 = (bf16[4,512,128]{2,1,0:T(8,128)(2,1)S(1)}, bf16[4,512,128]{2,1,0:T(8,128)(2,1)S(1)}, u32[]{:S(2)}, u32[]{:S(2)}) collective-permute-start(bf16[4,512,128]{2,1,0:T(8,128)(2,1)S(1)} %collective-permute-done.12.refs_3_.refs_7_), channel_id=1, source_target_pairs={{0,1},{1,0},{2,3},{3,2},{4,5},{5,4},{6,7},{7,6},{8,9},{9,8},{10,11... | collective-permute-start | bytes 1572872 | tf_op jit(solution)/shard_map/ppermute | solution.py:32
  80.0 18.4 %collective-permute-start.19 = (bf16[528,128]{1,0:T(8,128)(2,1)S(1)}, bf16[528,128]{1,0:T(8,128)(2,1)S(1)}, u32[]{:S(2)}, u32[]{:S(2)}) collective-permute-start(bf16[528,128]{1,0:T(8,128)(2,1)S(1)} %get-tuple-element.31), channel_id=1, source_target_pairs={{0,128},{32,160},{64,192},{96,224},{128,0},{160,32},{192,64},{224,... | collective-permute-start | bytes 405512 | tf_op jit(solution)/shard_map/ppermute | solution.py:32
  85.5 15.7 %collective-permute-start.20 = (bf16[528,128]{1,0:T(8,128)(2,1)S(1)}, bf16[528,128]{1,0:T(8,128)(2,1)S(1)}, u32[]{:S(2)}, u32[]{:S(2)}) collective-permute-start(bf16[528,128]{1,0:T(8,128)(2,1)S(1)} %get-tuple-element.32), channel_id=1, source_target_pairs={{0,160},{32,192},{64,224},{96,0},{128,32},{160,64},{192,96},{224,1... | collective-permute-start | bytes 405512 | tf_op jit(solution)/shard_map/ppermute | solution.py:32
  93.0 14.7 %collective-permute-start.21 = (bf16[528,128]{1,0:T(8,128)(2,1)S(1)}, bf16[528,128]{1,0:T(8,128)(2,1)S(1)}, u32[]{:S(2)}, u32[]{:S(2)}) collective-permute-start(bf16[528,128]{1,0:T(8,128)(2,1)S(1)} %get-tuple-element.33), channel_id=1, source_target_pairs={{0,96},{32,128},{64,160},{96,192},{128,224},{160,0},{192,32},{224,... | collective-permute-start | bytes 405512 | tf_op jit(solution)/shard_map/ppermute | solution.py:32
  96.1 11.6 %collective-permute-start.22 = (bf16[528,128]{1,0:T(8,128)(2,1)S(1)}, bf16[528,128]{1,0:T(8,128)(2,1)S(1)}, u32[]{:S(2)}, u32[]{:S(2)}) collective-permute-start(bf16[528,128]{1,0:T(8,128)(2,1)S(1)} %get-tuple-element.34), channel_id=1, source_target_pairs={{0,192},{32,224},{64,0},{96,32},{128,64},{160,96},{192,128},{224,1... | collective-permute-start | bytes 405512 | tf_op jit(solution)/shard_map/ppermute | solution.py:32
  97.6 13.5 %collective-permute-start.23 = (bf16[528,128]{1,0:T(8,128)(2,1)S(1)}, bf16[528,128]{1,0:T(8,128)(2,1)S(1)}, u32[]{:S(2)}, u32[]{:S(2)}) collective-permute-start(bf16[528,128]{1,0:T(8,128)(2,1)S(1)} %get-tuple-element.35), channel_id=1, source_target_pairs={{0,64},{32,96},{64,128},{96,160},{128,192},{160,224},{192,0},{224,... | collective-permute-start | bytes 405512 | tf_op jit(solution)/shard_map/ppermute | solution.py:32
  98.4 12.6 %collective-permute-start.24 = (bf16[528,128]{1,0:T(8,128)(2,1)S(1)}, bf16[528,128]{1,0:T(8,128)(2,1)S(1)}, u32[]{:S(2)}, u32[]{:S(2)}) collective-permute-start(bf16[528,128]{1,0:T(8,128)(2,1)S(1)} %get-tuple-element.36), channel_id=1, source_target_pairs={{0,224},{32,0},{64,32},{96,64},{128,96},{160,128},{192,160},{224,1... | collective-permute-start | bytes 405512 | tf_op jit(solution)/shard_map/ppermute | solution.py:32
  101.2 14.4 %collective-permute-start.25 = (bf16[528,128]{1,0:T(8,128)(2,1)S(1)}, bf16[528,128]{1,0:T(8,128)(2,1)S(1)}, u32[]{:S(2)}, u32[]{:S(2)}) collective-permute-start(bf16[528,128]{1,0:T(8,128)(2,1)S(1)} %get-tuple-element.37), channel_id=1, source_target_pairs={{0,32},{32,64},{64,96},{96,128},{128,160},{160,192},{192,224},{224... | collective-permute-start | bytes 405512 | tf_op jit(solution)/shard_map/ppermute | solution.py:32
  119.8 5.6 %collective-permute-start.29 = (bf16[16,2048]{1,0:T(8,128)(2,1)S(1)}, bf16[16,2048]{1,0:T(8,128)(2,1)S(1)}, u32[]{:S(2)}, u32[]{:S(2)}) collective-permute-start(bf16[16,2048]{1,0:T(8,128)(2,1)S(1)} %get-tuple-element.44), channel_id=1, source_target_pairs={{0,2},{2,4},{4,6},{6,0},{1,3},{3,5},{5,7},{7,1},{8,10},{10,12},{12... | collective-permute-start | bytes 196616 | tf_op jit(solution)/shard_map/ppermute | solution.py:32
  (15 other events, 122.8 us)
where the time goes:
time: 127 us; the launch traced here: 126 us
  starting transfers between devices  52.5 us (41%)
  waiting for transfers between devices  50.6 us (40%)
  Pallas kernels  15.7 us (12%)
  local copies, waits for them, and re-layouts  6.22 us (5%)
    ppermute x24, starting transfers between devices, moved(): return lax.ppermute(array, axis, [(i, (i + shift) % n) for i in range(n)])  37.2 us
    ppermute x24, waiting for transfers between devices, moved(): return lax.ppermute(array, axis, [(i, (i + shift) % n) for i in range(n)])  37.1 us
    ppermute x6, waiting for transfers between devices, by_role(): return lax.ppermute(array, ('y', 'x', 'c'), pairs)  13.4 us
    pallas_call x2, Pallas kernels, attend(): pl.pallas_call(attend_kernel, out_shape=[jax.ShapeDtypeStruct((HD + EXTRA...  11.4 us
    ppermute x6, starting transfers between devices, by_role(): return lax.ppermute(array, ('y', 'x', 'c'), pairs)  8.14 us
    all_to_all x1, starting transfers between devices, on_device(): queries = lax.all_to_all(copies, 'z', 0, 0, tiled=True)  7.15 us
    unnamed x18, local copies, waits for them, and re-layouts  4.8 us
  transfers between devices with their start and end apart: 31, of which 22 were waited for; matrix products, arithmetic and copies ran while one was open for 2% of the time, Pallas kernels for 8%

commit v1 on v0

--- a/solution.py
+++ b/solution.py
@@ -39,19 +39,28 @@
     return [array, one, far, back]
 
 
-def norm_kernel(source, target, source_gain, target_gain, source_out, target_out):
-    source_out[...] = norm_rows(source[...], source_gain[...]).astype(BF)
-    target_out[...] = norm_rows(target[...], target_gain[...]).astype(BF)
-
-
-def normed_inputs(source, target, source_gain, target_gain):
+def norm_kernel(*refs):
+    normed, rows = refs[4:6]
+    held, sems = refs[6:10], refs[10]
+    copies = [pltpu.make_async_copy(refs[i], held[i], sems.at[i]) for i in range(4)]
+    for copy in copies:
+        copy.start()
+    for value, gain, out in ((0, 1, normed), (2, 3, rows)):
+        copies[value].wait()
+        copies[gain].wait()
+        out[...] = norm_rows(held[value][...], held[gain][...]).astype(BF)
+
+
+def normed_inputs(*arrays):
+    target, _, source, _ = arrays
     return pl.pallas_call(
         norm_kernel,
-        out_shape=[jax.ShapeDtypeStruct(source.shape, BF), jax.ShapeDtypeStruct(target.shape, BF)],
-        in_specs=[VMEM] * 4,
+        out_shape=[jax.ShapeDtypeStruct(a.shape, BF) for a in (target, source)],
+        in_specs=[ANY] * 4,
         out_specs=[VMEM] * 2,
-        compiler_params=room(8),
-    )(source, target, source_gain, target_gain)
+        scratch_shapes=[pltpu.VMEM(a.shape, a.dtype) for a in arrays]
+        + [pltpu.SemaphoreType.DMA((4,))],
+    )(*arrays)
 
 
 def key_value_kernel(*refs):
@@ -96,45 +105,55 @@
 
 
 def query_kernel(*refs):
-    weight, out, full = refs[NX:]
+    weight, out, held, rows, full, sems = refs[2 * NX :]
     x = lax.axis_index("x")
-    rows = jnp.concatenate([ref[...] for ref in refs[:NX]], axis=0)
-    full[...] = jnp.dot(rows, weight[...], preferred_element_type=F32)
+    copies = [pltpu.make_async_copy(weight, held, sems.at[0])]
+    for i, block in enumerate(refs[: 2 * NX]):
+        copies.append(pltpu.make_async_copy(block, rows.at[pl.ds(i * 16, 16), :], sems.at[i + 1]))
+    for copy in copies:
+        copy.start()
+    for copy in copies:
+        copy.wait()
+    full[...] = jnp.dot(rows[...], held[...], preferred_element_type=F32)
     for k in range(NX):
         place = pl.multiple_of(lax.rem(x - k + NX, NX) * 128, 128)
-        block = full[:, pl.ds(place, 128)].astype(BF)
-        for copy in range(NZ):
-            out[copy, :, pl.ds(k * 128, 128)] = block
+        out[:, pl.ds(k * 128, 128)] = full[:, pl.ds(place, 128)].astype(BF)
 
 
 def query_rows(blocks, weight):
     return pl.pallas_call(
         query_kernel,
-        out_shape=jax.ShapeDtypeStruct((NZ, 128, HD), BF),
-        in_specs=[VMEM] * (NX + 1),
+        out_shape=jax.ShapeDtypeStruct((128, HD), BF),
+        in_specs=[ANY] * (2 * NX + 1),
         out_specs=VMEM,
-        scratch_shapes=[pltpu.VMEM((128, HD), F32)],
-        compiler_params=room(12),
+        scratch_shapes=[
+            pltpu.VMEM((2048, HD), BF), pltpu.VMEM((128, 2048), BF), pltpu.VMEM((128, HD), F32),
+            pltpu.SemaphoreType.DMA((2 * NX + 1,))],
+        compiler_params=room(60),
         cost_estimate=pl.CostEstimate(
             flops=2 * 128 * 2048 * HD, bytes_accessed=3 << 20, transcendentals=0),
     )(*blocks, weight)
 
 
-def soft_part(q, keys, values, outs):
+def soft_part(q, keys, values, outs, arrivals):
     scores = []
     for m in range(NY):
-        block = jnp.concatenate([keys[m, k] for k in range(NX)], axis=1)
+        if arrivals:
+            arrivals[m].wait()
+        block = jnp.concatenate([keys[m][k] for k in range(NX)], axis=1)
         scores.append(lax.dot_general(
             block, q, (((1,), (1,)), ((), ())), preferred_element_type=F32) * HD ** (-0.5))
     top = functools.reduce(
         jnp.maximum, [jnp.max(score, axis=0, keepdims=True) for score in scores])
+    for arrival in arrivals[NY:]:
+        arrival.wait()
     total, numerator = 0.0, 0.0
     for m in range(NY):
         weights = jnp.exp(scores[m] - top)
         total = total + jnp.sum(weights, axis=0, keepdims=True)
         block = jnp.concatenate([
             jnp.concatenate(
-                [values[k, m, pl.ds(row, 128), :] for row in (256, 384, 0, 128)], axis=1)
+                [values[k][m, pl.ds(row, 128), :] for row in (256, 384, 0, 128)], axis=1)
             for k in range(NX)], axis=0)
         numerator = numerator + jnp.dot(
             block, weights.astype(BF), preferred_element_type=F32)
@@ -152,11 +171,11 @@
         out[pl.ds(HD, EXTRA), :] = jnp.concatenate(pieces, axis=0).astype(BF)
 
 
-def attend_kernel(*refs):
-    n = (len(refs) - 11) // 2
-    near, other = refs[n : n + NX], refs[n + NX : n + 2 * NX]
-    outs = refs[n + 8 : 2 * n + 8]
-    keys, values, sems = refs[2 * n + 8 :]
+def attend_kernel(n, *refs):
+    queries, refs = refs[:n], refs[n:]
+    near, other = refs[:NX], refs[NX : 2 * NX]
+    outs = refs[2 * NX : -3]
+    keys, values, sems = refs[-3:]
     core = lax.axis_index("c")
 
     def copies(key_blocks, value_blocks):
@@ -175,17 +194,16 @@
         for copy in copies(other, near):
             copy.start()
 
-    for copy in copies(near, other):
-        copy.wait()
+    arrivals = copies(near, other)
     for i in range(0, n, 2):
-        q = jnp.concatenate([ref[...] for ref in refs[i : i + 2]], axis=0)
-        soft_part(q, keys, values, outs[i : i + 2])
-
-
-def attend(queries, near, other):
-    n = len(queries)
-    return pl.pallas_call(
-        attend_kernel,
+        q = jnp.concatenate([query[...] for query in queries[i : i + 2]], axis=0)
+        soft_part(q, keys, values, outs[i : i + 2], arrivals if i == 0 else [])
+
+
+def attend(shifts, queries, near, other):
+    n = len(shifts)
+    return dict(zip(shifts, pl.pallas_call(
+        functools.partial(attend_kernel, n),
         out_shape=[jax.ShapeDtypeStruct((HD + EXTRA, 128), BF)] * n,
         in_specs=[VMEM] * n + [ANY] * 8,
         out_specs=[VMEM] * n,
@@ -194,7 +212,7 @@
         cost_estimate=pl.CostEstimate(
             flops=4 * 128 * n * 2048 * HD, bytes_accessed=4 << 20,
             transcendentals=n * 128 * 2048),
-    )(*queries, *near, *other)
+    )(*[queries[k] for k in shifts], *near, *other)))
 
 
 def combine_kernel(*refs):
@@ -288,14 +306,15 @@
 
 
 def on_device(target, source, target_gain, source_gain, w_query, w_key, w_value, w_out, final_gain):
-    rows, normed = normed_inputs(source, target, source_gain, target_gain)
-    other_normed = moved(normed, "c", 1)
-    rows, other_normed = lax.optimization_barrier((rows, other_normed))
-    chip_normed = jnp.concatenate([normed, other_normed], axis=0)
+    normed, rows = normed_inputs(target, target_gain, source, source_gain)
+    own_targets = ring4(normed, "x")
     row_blocks = ring4(rows, "x")
-    target_blocks = ring4(chip_normed, "x")
-    copies = query_rows(target_blocks, w_query[0])
-    queries = lax.all_to_all(copies, "z", 0, 0, tiled=True)
+    targets = [t for own in own_targets for t in (own, moved(own, "c", 1))]
+    query = query_rows(targets, w_query[0])
+    queries = {0: query}
+    for shifts in ((4,), (3, 5), (2, 6, 1, 7)):
+        for k in shifts:
+            queries[k] = moved(query, "z", k)
 
     own_w = jnp.concatenate([w_key[0].T, w_value[0].T], axis=0)
     other_w = moved(own_w, "c", 1)
@@ -306,18 +325,13 @@
     near = role_ring4(line, ("y", "x"))
     other = [moved(block, "c", 1) for block in near]
 
-    z = lax.axis_index("z")
-    picked = [
-        lax.dynamic_slice(queries, (lax.rem(z - k + NZ, NZ), 0, 0), (1, 128, HD)).reshape(128, HD)
-        for k in range(NZ)]
-    parts = dict(zip((4, 3), attend([picked[4], picked[3]], near, other)))
-    arrived = []
-    for k in (4, 3):
-        arrived.append(moved(parts[k], "z", -k))
-    rest = (5, 2, 6, 1, 7, 0)
-    parts.update(zip(rest, attend([picked[k] for k in rest], near, other)))
-    for k in rest[:-1]:
-        arrived.append(moved(parts[k], "z", -k))
+
+    parts, arrived = {}, []
+    for shifts in ((3, 5), (4, 2, 6, 1), (7, 0)):
+        parts.update(attend(shifts, queries, near, other))
+        for k in shifts:
+            if k:
+                arrived.append(moved(parts[k], "z", -k))
     arrived.append(parts[0])
     kept, sent = combine(arrived, w_out[0])
     met = moved(sent, "c", 1)

time: 127 us -> 138 us (1.087)
  starting transfers between devices: 52.5 us -> 59.1 us
  Pallas kernels: 15.7 us -> 20.9 us
  local copies, waits for them, and re-layouts: 6.22 us -> 1.6 us
  waiting for transfers between devices: 50.6 us -> 55 us
    ppermute x24 -> x34, starting transfers between devices: 37.2 us -> 51.7 us  [moved(): return lax.ppermute(array, axis, [(i, (i + shift) % n) for i in range(n)])]
    ppermute x24 -> x34, waiting for transfers between devices: 37.1 us -> 51.1 us  [moved(): return lax.ppermute(array, axis, [(i, (i + shift) % n) for i in range(n)])]
    ppermute x6, waiting for transfers between devices: 13.4 us -> 3.9 us  [by_role(): return lax.ppermute(array, ('y', 'x', 'c'), pairs)]
    all_to_all x1 -> x0, starting transfers between devices: 7.15 us -> none  [on_device(): queries = lax.all_to_all(copies, 'z', 0, 0, tiled=True)]
    pallas_call x4 -> x5, Pallas kernels: 13.1 us -> 18.4 us  [the longest x3 13.7 us: attend(): pl.pallas_call(functools.partial(attend_kernel, n), out_shape=[jax.ShapeD...]
    unnamed x18 -> x25, local copies, waits for them, and re-layouts: 4.8 us -> 1.59 us
    reshape x1 -> x0, local copies, waits for them, and re-layouts: 1.4 us -> none  [on_device(): lax.dynamic_slice(queries, (lax.rem(z - k + NZ, NZ), 0, 0), (1, 128, HD))]
  transfers between devices with their start and end apart: 31 -> 40, of which waited for: 22 -> 22; matrix products, arithmetic and copies ran while one was open for 2% -> 0% of each run, Pallas kernels for 8% -> 13%
where the time goes in v1:
time: 138 us
  starting transfers between devices  59.1 us (43%)
  waiting for transfers between devices  55 us (40%)
  Pallas kernels  20.9 us (15%)
  local copies, waits for them, and re-layouts  1.6 us (1%)
    ppermute x34, starting transfers between devices, moved(): return lax.ppermute(array, axis, [(i, (i + shift) % n) for i in range(n)])  51.7 us
    ppermute x34, waiting for transfers between devices, moved(): return lax.ppermute(array, axis, [(i, (i + shift) % n) for i in range(n)])  51.1 us
    pallas_call x3, Pallas kernels, attend(): pl.pallas_call(functools.partial(attend_kernel, n), out_shape=[jax.ShapeD...  13.7 us
    ppermute x6, starting transfers between devices, by_role(): return lax.ppermute(array, ('y', 'x', 'c'), pairs)  7.39 us
    ppermute x6, waiting for transfers between devices, by_role(): return lax.ppermute(array, ('y', 'x', 'c'), pairs)  3.9 us
    pallas_call x1, Pallas kernels, query_rows(): pl.pallas_call(query_kernel, out_shape=jax.ShapeDtypeStruct((128, HD), BF...  2.83 us
  transfers between devices with their start and end apart: 40, of which 22 were waited for; matrix products, arithmetic and copies ran while one was open for 0% of the time, Pallas kernels for 13%

profile of v1, /device:TPU:1, one launch (start us, length us, event | category | flops | bytes accessed | tf_op | source)
XLA Modules:
  0.0 137.9 jit_solution(6313445881872075552)
XLA Ops:
  1.1 3.3 %collective-permute-start.12 = (bf16[128,2048]{1,0:T(8,128)(2,1)S(1)}, bf16[128,2048]{1,0:T(8,128)(2,1)S(1)}, u32[]{:S(2)}, u32[]{:S(2)}) collective-permute-start(bf16[128,2048]{1,0:T(8,128)(2,1)S(1)} %pad_maximum_fusion.refs_4_), channel_id=1, source_target_pairs={{0,1},{1,0},{2,3},{3,2},{4,5},{5,4},{6,7},{7,6},{8,9},{9,8},{10,11... | collective-permute-start | bytes 1572872 | tf_op jit(solution)/shard_map/ppermute | solution.py:32
  8.9 7.1 %collective-permute-done.10.refs_2_ = bf16[64,2048]{1,0:T(8,128)(2,1)S(1)} collective-permute-done((bf16[64,2048]{1,0:T(8,128)(2,1)}, bf16[64,2048]{1,0:T(8,128)(2,1)S(1)}, u32[]{:S(2)}, u32[]{:S(2)}) %collective-permute-start.10) | collective-permute-done | bytes 262176 | tf_op jit(solution)/shard_map/ppermute | solution.py:32
  15.9 4.0 %collective-permute-done.11.refs_3_ = bf16[64,2048]{1,0:T(8,128)(2,1)S(1)} collective-permute-done((bf16[64,2048]{1,0:T(8,128)(2,1)}, bf16[64,2048]{1,0:T(8,128)(2,1)S(1)}, u32[]{:S(2)}, u32[]{:S(2)}) %collective-permute-start.11) | collective-permute-done | bytes 262176 | tf_op jit(solution)/shard_map/ppermute | solution.py:32
  25.5 2.3 %collective-permute-start.15 = (bf16[512,128]{1,0:T(8,128)(2,1)S(1)}, bf16[512,128]{1,0:T(8,128)(2,1)S(1)}, u32[]{:S(2)}, u32[]{:S(2)}) collective-permute-start(bf16[512,128]{1,0:T(8,128)(2,1)S(1)} %constant_dynamic-update-slice_fusion), channel_id=1, source_target_pairs={{0,4},{1,17},{2,6},{3,19},{4,0},{5,21},{6,2},{7,23},{8,12},{9,25},... | collective-permute-start | bytes 393224 | tf_op jit(solution)/shard_map/ppermute | solution.py:298
  28.9 3.3 %collective-permute-done.14 = bf16[512,128]{1,0:T(8,128)(2,1)S(1)} collective-permute-done((bf16[512,128]{1,0:T(8,128)(2,1)S(1)}, bf16[512,128]{1,0:T(8,128)(2,1)S(1)}, u32[]{:S(2)}, u32[]{:S(2)}) %collective-permute-start.14) | collective-permute-done | bytes 131104 | tf_op jit(solution)/shard_map/ppermute | solution.py:298
  33.2 2.4 %collective-permute-start.18 = (bf16[4,512,128]{2,1,0:T(8,128)(2,1)S(1)}, bf16[4,512,128]{2,1,0:T(8,128)(2,1)S(1)}, u32[]{:S(2)}, u32[]{:S(2)}) collective-permute-start(bf16[4,512,128]{2,1,0:T(8,128)(2,1)S(1)} %pad_maximum_fusion.1.refs_2_.refs_4_), channel_id=1, source_target_pairs={{0,16},{1,5},{2,18},{3,7},{4,20},{5,1},{6,22},{7,3},{8,24},{9,13},... | collective-permute-start | bytes 1572872 | tf_op jit(solution)/shard_map/ppermute | solution.py:298
  38.0 12.1 %collective-permute-done.1.refs_2_ = bf16[16,2048]{1,0:T(8,128)(2,1)S(1)} collective-permute-done((bf16[16,2048]{1,0:T(8,128)(2,1)S(1)}, bf16[16,2048]{1,0:T(8,128)(2,1)S(1)}, u32[]{:S(2)}, u32[]{:S(2)}) %collective-permute-start.1) | collective-permute-done | bytes 65568 | tf_op jit(solution)/shard_map/ppermute | solution.py:32
  51.3 2.4 %collective-permute-start.5 = (bf16[16,2048]{1,0:T(8,128)(2,1)S(1)}, bf16[16,2048]{1,0:T(8,128)(2,1)S(1)}, u32[]{:S(2)}, u32[]{:S(2)}) collective-permute-start(bf16[16,2048]{1,0:T(8,128)(2,1)S(1)} %copy-done.4), channel_id=1, source_target_pairs={{0,6},{2,0},{4,2},{6,4},{1,7},{3,1},{5,3},{7,5},{8,14},{10,8},{12,... | collective-permute-start | bytes 196616 | tf_op jit(solution)/shard_map/ppermute | solution.py:32
  61.5 2.8 %shard_map.92.refs_1_ = bf16[128,512]{1,0:T(8,128)(2,1)} custom-call(bf16[16,2048]{1,0:T(8,128)(2,1)} %get-tuple-element.23.refs_0_, bf16[16,2048]{1,0:T(8,128)(2,1)} %copy-done.8, bf16[16,2048]{1,0:T(8,128)(2,1)} %copy-done.5, bf16[16,2048]{1,0:T(8,128)(2,1)} %copy-done.9, bf16[16,2048]{1,0:T(8,128)(2,1)} %copy-done.6, bf16[16,2048]{1,0:T(8,128)(2,1)} %copy-done.10, ...), custom_call_target="tpu_custom_call" | custom-call | flops 268435456 | bytes 3145728 | tf_op jit(solution)/shard_map/pallas_call | solution.py:124
  64.3 5.3 %collective-permute-start.34 = (bf16[128,512]{1,0:T(8,128)(2,1)}, bf16[128,512]{1,0:T(8,128)(2,1)S(1)}, u32[]{:S(2)}, u32[]{:S(2)}) collective-permute-start(bf16[128,512]{1,0:T(8,128)(2,1)} %shard_map.92.refs_1_), channel_id=1, source_target_pairs={{0,224},{32,0},{64,32},{96,64},{128,96},{160,128},{192,160},{224,1... | collective-permute-start | bytes 393224 | tf_op jit(solution)/shard_map/ppermute | solution.py:32
  69.5 2.8 %collective-permute-done.34.refs_0_ = bf16[128,512]{1,0:T(8,128)(2,1)S(1)} collective-permute-done((bf16[128,512]{1,0:T(8,128)(2,1)}, bf16[128,512]{1,0:T(8,128)(2,1)S(1)}, u32[]{:S(2)}, u32[]{:S(2)}) %collective-permute-start.34) | collective-permute-done | bytes 131104 | tf_op jit(solution)/shard_map/ppermute | solution.py:32
  72.4 3.4 %collective-permute-start.26 = (bf16[128,512]{1,0:T(8,128)(2,1)}, bf16[128,512]{1,0:T(8,128)(2,1)S(1)}, u32[]{:S(2)}, u32[]{:S(2)}) collective-permute-start(bf16[128,512]{1,0:T(8,128)(2,1)} %shard_map.92.refs_1_), channel_id=1, source_target_pairs={{0,128},{32,160},{64,192},{96,224},{128,0},{160,32},{192,64},{224,... | collective-permute-start | bytes 393224 | tf_op jit(solution)/shard_map/ppermute | solution.py:32
  77.0 2.4 %collective-permute-start.28 = (bf16[128,512]{1,0:T(8,128)(2,1)}, bf16[128,512]{1,0:T(8,128)(2,1)S(1)}, u32[]{:S(2)}, u32[]{:S(2)}) collective-permute-start(bf16[128,512]{1,0:T(8,128)(2,1)} %shard_map.92.refs_1_), channel_id=1, source_target_pairs={{0,192},{32,224},{64,0},{96,32},{128,64},{160,96},{192,128},{224,1... | collective-permute-start | bytes 393224 | tf_op jit(solution)/shard_map/ppermute | solution.py:32
  81.6 4.6 %shard_map.96 = (bf16[528,128]{1,0:T(8,128)(2,1)S(1)}, bf16[528,128]{1,0:T(8,128)(2,1)S(1)}) custom-call(bf16[128,512]{1,0:T(8,128)(2,1)S(1)} %collective-permute-done.34.refs_0_, bf16[128,512]{1,0:T(8,128)(2,1)} %shard_map.92.refs_1_, bf16[4,512,128]{2,1,0:T(8,128)(2,1)S(1)} %pad_maximum_fusion.1.refs_2_.refs_4_, ...), custom_call_target="tpu_custom_call" | custom-call | flops 1073741824 | bytes 4194304 | tf_op jit(solution)/shard_map/pallas_call | solution.py:205
  86.3 3.1 %collective-permute-start.8 = (bf16[128,512]{1,0:T(8,128)(2,1)}, bf16[128,512]{1,0:T(8,128)(2,1)S(1)}, u32[]{:S(2)}, u32[]{:S(2)}) collective-permute-start(bf16[128,512]{1,0:T(8,128)(2,1)} %shard_map.92.refs_1_), channel_id=1, source_target_pairs={{0,160},{32,192},{64,224},{96,0},{128,32},{160,64},{192,96},{224,1... | collective-permute-start | bytes 393224 | tf_op jit(solution)/shard_map/ppermute | solution.py:32
  91.7 5.3 %shard_map.95 = (bf16[528,128]{1,0:T(8,128)(2,1)S(1)}, bf16[528,128]{1,0:T(8,128)(2,1)S(1)}, bf16[528,128]{1,0:T(8,128)(2,1)S(1)}, bf16[528,128]{1,0:T(8,128)(2,1)S(1)}) custom-call(bf16[128,512]{1,0:T(8,128)(2,1)S(1)} %collective-permute-done.26.refs_0_, bf16[128,512]{1,0:T(8,128)(2,1)S(1)} %collective-permute-done.27.refs_1_, ...), custom_call_target="tpu_custom_call" | custom-call | flops 2147483648 | bytes 4194304 | tf_op jit(solution)/shard_map/pallas_call | solution.py:205
  97.1 6.6 %collective-permute-start.30 = (bf16[528,128]{1,0:T(8,128)(2,1)S(1)}, bf16[528,128]{1,0:T(8,128)(2,1)S(1)}, u32[]{:S(2)}, u32[]{:S(2)}) collective-permute-start(bf16[528,128]{1,0:T(8,128)(2,1)S(1)} %get-tuple-element.29), channel_id=1, source_target_pairs={{0,128},{32,160},{64,192},{96,224},{128,0},{160,32},{192,64},{224,... | collective-permute-start | bytes 405512 | tf_op jit(solution)/shard_map/ppermute | solution.py:32
  103.6 2.4 %collective-permute-start.32 = (bf16[528,128]{1,0:T(8,128)(2,1)S(1)}, bf16[528,128]{1,0:T(8,128)(2,1)S(1)}, u32[]{:S(2)}, u32[]{:S(2)}) collective-permute-start(bf16[528,128]{1,0:T(8,128)(2,1)S(1)} %get-tuple-element.31), channel_id=1, source_target_pairs={{0,64},{32,96},{64,128},{96,160},{128,192},{160,224},{192,0},{224,... | collective-permute-start | bytes 405512 | tf_op jit(solution)/shard_map/ppermute | solution.py:32
  106.0 3.7 %shard_map.94 = (bf16[528,128]{1,0:T(8,128)(2,1)S(1)}, bf16[528,128]{1,0:T(8,128)(2,1)S(1)}) custom-call(bf16[128,512]{1,0:T(8,128)(2,1)S(1)} %collective-permute-done.7.refs_0_, bf16[128,512]{1,0:T(8,128)(2,1)S(1)} %collective-permute-done.8.refs_1_, bf16[4,512,128]{2,1,0:T(8,128)(2,1)S(1)} %pad_maximum_fusion.1.refs_2_.refs_4_, ...), custom_call_target="tpu_custom_call" | custom-call | flops 1073741824 | bytes 4194304 | tf_op jit(solution)/shard_map/pallas_call | solution.py:205
  110.7 2.4 %collective-permute-start.25 = (bf16[528,128]{1,0:T(8,128)(2,1)S(1)}, bf16[528,128]{1,0:T(8,128)(2,1)S(1)}, u32[]{:S(2)}, u32[]{:S(2)}) collective-permute-start(bf16[528,128]{1,0:T(8,128)(2,1)S(1)} %get-tuple-element.28), channel_id=1, source_target_pairs={{0,96},{32,128},{64,160},{96,192},{128,224},{160,0},{192,32},{224,... | collective-permute-start | bytes 405512 | tf_op jit(solution)/shard_map/ppermute | solution.py:32
  115.5 5.7 %collective-permute-done.24.refs_0_ = bf16[528,128]{1,0:T(8,128)(2,1)S(1)} collective-permute-done((bf16[528,128]{1,0:T(8,128)(2,1)S(1)}, bf16[528,128]{1,0:T(8,128)(2,1)S(1)}, u32[]{:S(2)}, u32[]{:S(2)}) %collective-permute-start.24) | collective-permute-done | bytes 135200 | tf_op jit(solution)/shard_map/ppermute | solution.py:32
  121.9 3.9 %collective-permute-start.36 = (bf16[64,2048]{1,0:T(8,128)(2,1)S(1)}, bf16[64,2048]{1,0:T(8,128)(2,1)S(1)}, u32[]{:S(2)}, u32[]{:S(2)}) collective-permute-start(bf16[64,2048]{1,0:T(8,128)(2,1)S(1)} %get-tuple-element.36), channel_id=1, source_target_pairs={{0,1},{1,0},{2,3},{3,2},{4,5},{5,4},{6,7},{7,6},{8,9},{9,8},{10,11... | collective-permute-start | bytes 786440 | tf_op jit(solution)/shard_map/ppermute | solution.py:32
  127.0 4.2 %collective-permute-start.37 = (bf16[16,2048]{1,0:T(8,128)(2,1)S(1)}, bf16[16,2048]{1,0:T(8,128)(2,1)S(1)}, u32[]{:S(2)}, u32[]{:S(2)}) collective-permute-start(bf16[16,2048]{1,0:T(8,128)(2,1)S(1)} %get-tuple-element.38), channel_id=1, source_target_pairs={{0,6},{2,0},{4,2},{6,4},{1,7},{3,1},{5,3},{7,5},{8,14},{10,8},{12,... | collective-permute-start | bytes 196616 | tf_op jit(solution)/shard_map/ppermute | solution.py:32
  132.6 3.4 %collective-permute-done.38.two = bf16[16,2048]{1,0:T(8,128)(2,1)S(1)} collective-permute-done((bf16[16,2048]{1,0:T(8,128)(2,1)S(1)}, bf16[16,2048]{1,0:T(8,128)(2,1)S(1)}, u32[]{:S(2)}, u32[]{:S(2)}) %collective-permute-start.38) | collective-permute-done | bytes 65568 | tf_op jit(solution)/shard_map/ppermute | solution.py:32
  (93 shorter events, 38.8 us)
Async XLA Ops:
  1.1 20.8 %collective-permute-start.12 = (bf16[128,2048]{1,0:T(8,128)(2,1)S(1)}, bf16[128,2048]{1,0:T(8,128)(2,1)S(1)}, u32[]{:S(2)}, u32[]{:S(2)}) collective-permute-start(bf16[128,2048]{1,0:T(8,128)(2,1)S(1)} %pad_maximum_fusion.refs_4_), channel_id=1, source_target_pairs={{0,1},{1,0},{2,3},{3,2},{4,5},{5,4},{6,7},{7,6},{8,9},{9,8},{10,11... | collective-permute-start | bytes 1572872 | tf_op jit(solution)/shard_map/ppermute | solution.py:32
  7.4 12.6 %collective-permute-start.11 = (bf16[64,2048]{1,0:T(8,128)(2,1)}, bf16[64,2048]{1,0:T(8,128)(2,1)S(1)}, u32[]{:S(2)}, u32[]{:S(2)}) collective-permute-start(bf16[64,2048]{1,0:T(8,128)(2,1)} %get-tuple-element.24.refs_0_), channel_id=1, source_target_pairs={{0,6},{2,0},{4,2},{6,4},{1,7},{3,1},{5,3},{7,5},{8,14},{10,8},{12,... | collective-permute-start | bytes 786440 | tf_op jit(solution)/shard_map/ppermute | solution.py:32
  8.2 13.7 %collective-permute-start.9 = (bf16[64,2048]{1,0:T(8,128)(2,1)}, bf16[64,2048]{1,0:T(8,128)(2,1)S(1)}, u32[]{:S(2)}, u32[]{:S(2)}) collective-permute-start(bf16[64,2048]{1,0:T(8,128)(2,1)} %get-tuple-element.24.refs_0_), channel_id=1, source_target_pairs={{0,2},{2,4},{4,6},{6,0},{1,3},{3,5},{5,7},{7,1},{8,10},{10,12},{12... | collective-permute-start | bytes 786440 | tf_op jit(solution)/shard_map/ppermute | solution.py:32
  32.8 17.7 %collective-permute-start.17 = (bf16[4,512,128]{2,1,0:T(8,128)(2,1)S(1)}, bf16[4,512,128]{2,1,0:T(8,128)(2,1)S(1)}, u32[]{:S(2)}, u32[]{:S(2)}) collective-permute-start(bf16[4,512,128]{2,1,0:T(8,128)(2,1)S(1)} %pad_maximum_fusion.1.refs_2_.refs_4_), channel_id=1, source_target_pairs={{0,8},{1,3},{2,10},{3,5},{4,12},{5,7},{6,14},{7,1},{8,16},{9,11},{... | collective-permute-start | bytes 1572872 | tf_op jit(solution)/shard_map/ppermute | solution.py:298
  33.2 17.5 %collective-permute-start.18 = (bf16[4,512,128]{2,1,0:T(8,128)(2,1)S(1)}, bf16[4,512,128]{2,1,0:T(8,128)(2,1)S(1)}, u32[]{:S(2)}, u32[]{:S(2)}) collective-permute-start(bf16[4,512,128]{2,1,0:T(8,128)(2,1)S(1)} %pad_maximum_fusion.1.refs_2_.refs_4_), channel_id=1, source_target_pairs={{0,16},{1,5},{2,18},{3,7},{4,20},{5,1},{6,22},{7,3},{8,24},{9,13},... | collective-permute-start | bytes 1572872 | tf_op jit(solution)/shard_map/ppermute | solution.py:298
  35.6 15.5 %collective-permute-start.19 = (bf16[4,512,128]{2,1,0:T(8,128)(2,1)S(1)}, bf16[4,512,128]{2,1,0:T(8,128)(2,1)S(1)}, u32[]{:S(2)}, u32[]{:S(2)}) collective-permute-start(bf16[4,512,128]{2,1,0:T(8,128)(2,1)S(1)} %pad_maximum_fusion.1.refs_2_.refs_4_), channel_id=1, source_target_pairs={{0,24},{1,7},{2,26},{3,1},{4,28},{5,3},{6,30},{7,5},{8,0},{9,15},{... | collective-permute-start | bytes 1572872 | tf_op jit(solution)/shard_map/ppermute | solution.py:298
  36.7 13.3 %collective-permute-start.1 = (bf16[16,2048]{1,0:T(8,128)(2,1)S(1)}, bf16[16,2048]{1,0:T(8,128)(2,1)S(1)}, u32[]{:S(2)}, u32[]{:S(2)}) collective-permute-start(bf16[16,2048]{1,0:T(8,128)(2,1)S(1)} %copy-done.4), channel_id=1, source_target_pairs={{0,2},{2,4},{4,6},{6,0},{1,3},{3,5},{5,7},{7,1},{8,10},{10,12},{12... | collective-permute-start | bytes 196616 | tf_op jit(solution)/shard_map/ppermute | solution.py:32
  37.1 14.3 %collective-permute-start.3 = (bf16[16,2048]{1,0:T(8,128)(2,1)S(1)}, bf16[16,2048]{1,0:T(8,128)(2,1)S(1)}, u32[]{:S(2)}, u32[]{:S(2)}) collective-permute-start(bf16[16,2048]{1,0:T(8,128)(2,1)S(1)} %copy-done.4), channel_id=1, source_target_pairs={{0,4},{2,6},{4,0},{6,2},{1,5},{3,7},{5,1},{7,3},{8,12},{10,14},{12... | collective-permute-start | bytes 196616 | tf_op jit(solution)/shard_map/ppermute | solution.py:32
  50.1 25.7 %collective-permute-start.20 = (bf16[4,512,128]{2,1,0:T(8,128)(2,1)S(1)}, bf16[4,512,128]{2,1,0:T(8,128)(2,1)S(1)}, u32[]{:S(2)}, u32[]{:S(2)}) collective-permute-start(bf16[4,512,128]{2,1,0:T(8,128)(2,1)S(1)} %pad_maximum_fusion.1.refs_2_.refs_4_), channel_id=1, source_target_pairs={{0,1},{1,0},{2,3},{3,2},{4,5},{5,4},{6,7},{7,6},{8,9},{9,8},{10,11... | collective-permute-start | bytes 1572872 | tf_op jit(solution)/shard_map/ppermute | solution.py:32
  50.6 26.4 %collective-permute-start.21 = (bf16[4,512,128]{2,1,0:T(8,128)(2,1)S(1)}, bf16[4,512,128]{2,1,0:T(8,128)(2,1)S(1)}, u32[]{:S(2)}, u32[]{:S(2)}) collective-permute-start(bf16[4,512,128]{2,1,0:T(8,128)(2,1)S(1)} %collective-permute-done.17.refs_3_.refs_5_), channel_id=1, source_target_pairs={{0,1},{1,0},{2,3},{3,2},{4,5},{5,4},{6,7},{7,6},{8,9},{9,8},{10,11... | collective-permute-start | bytes 1572872 | tf_op jit(solution)/shard_map/ppermute | solution.py:32
  50.7 28.7 %collective-permute-start.22 = (bf16[4,512,128]{2,1,0:T(8,128)(2,1)S(1)}, bf16[4,512,128]{2,1,0:T(8,128)(2,1)S(1)}, u32[]{:S(2)}, u32[]{:S(2)}) collective-permute-start(bf16[4,512,128]{2,1,0:T(8,128)(2,1)S(1)} %collective-permute-done.18.refs_4_.refs_6_), channel_id=1, source_target_pairs={{0,1},{1,0},{2,3},{3,2},{4,5},{5,4},{6,7},{7,6},{8,9},{9,8},{10,11... | collective-permute-start | bytes 1572872 | tf_op jit(solution)/shard_map/ppermute | solution.py:32
  51.1 29.0 %collective-permute-start.23 = (bf16[4,512,128]{2,1,0:T(8,128)(2,1)S(1)}, bf16[4,512,128]{2,1,0:T(8,128)(2,1)}, u32[]{:S(2)}, u32[]{:S(2)}) collective-permute-start(bf16[4,512,128]{2,1,0:T(8,128)(2,1)S(1)} %collective-permute-done.19.refs_5_.refs_7_), channel_id=1, source_target_pairs={{0,1},{1,0},{2,3},{3,2},{4,5},{5,4},{6,7},{7,6},{8,9},{9,8},{10,11... | collective-permute-start | bytes 1572872 | tf_op jit(solution)/shard_map/ppermute | solution.py:32
  72.4 13.9 %collective-permute-start.26 = (bf16[128,512]{1,0:T(8,128)(2,1)}, bf16[128,512]{1,0:T(8,128)(2,1)S(1)}, u32[]{:S(2)}, u32[]{:S(2)}) collective-permute-start(bf16[128,512]{1,0:T(8,128)(2,1)} %shard_map.92.refs_1_), channel_id=1, source_target_pairs={{0,128},{32,160},{64,192},{96,224},{128,0},{160,32},{192,64},{224,... | collective-permute-start | bytes 393224 | tf_op jit(solution)/shard_map/ppermute | solution.py:32
  75.8 13.5 %collective-permute-start.27 = (bf16[128,512]{1,0:T(8,128)(2,1)}, bf16[128,512]{1,0:T(8,128)(2,1)S(1)}, u32[]{:S(2)}, u32[]{:S(2)}) collective-permute-start(bf16[128,512]{1,0:T(8,128)(2,1)} %shard_map.92.refs_1_), channel_id=1, source_target_pairs={{0,64},{32,96},{64,128},{96,160},{128,192},{160,224},{192,0},{224,... | collective-permute-start | bytes 393224 | tf_op jit(solution)/shard_map/ppermute | solution.py:32
  77.0 12.4 %collective-permute-start.28 = (bf16[128,512]{1,0:T(8,128)(2,1)}, bf16[128,512]{1,0:T(8,128)(2,1)S(1)}, u32[]{:S(2)}, u32[]{:S(2)}) collective-permute-start(bf16[128,512]{1,0:T(8,128)(2,1)} %shard_map.92.refs_1_), channel_id=1, source_target_pairs={{0,192},{32,224},{64,0},{96,32},{128,64},{160,96},{192,128},{224,1... | collective-permute-start | bytes 393224 | tf_op jit(solution)/shard_map/ppermute | solution.py:32
  79.4 12.4 %collective-permute-start.29 = (bf16[128,512]{1,0:T(8,128)(2,1)}, bf16[128,512]{1,0:T(8,128)(2,1)S(1)}, u32[]{:S(2)}, u32[]{:S(2)}) collective-permute-start(bf16[128,512]{1,0:T(8,128)(2,1)} %shard_map.92.refs_1_), channel_id=1, source_target_pairs={{0,32},{32,64},{64,96},{96,128},{128,160},{160,192},{192,224},{224... | collective-permute-start | bytes 393224 | tf_op jit(solution)/shard_map/ppermute | solution.py:32
  80.1 23.5 %collective-permute-start.7 = (bf16[128,512]{1,0:T(8,128)(2,1)}, bf16[128,512]{1,0:T(8,128)(2,1)S(1)}, u32[]{:S(2)}, u32[]{:S(2)}) collective-permute-start(bf16[128,512]{1,0:T(8,128)(2,1)} %shard_map.92.refs_1_), channel_id=1, source_target_pairs={{0,96},{32,128},{64,160},{96,192},{128,224},{160,0},{192,32},{224,... | collective-permute-start | bytes 393224 | tf_op jit(solution)/shard_map/ppermute | solution.py:32
  86.3 19.7 %collective-permute-start.8 = (bf16[128,512]{1,0:T(8,128)(2,1)}, bf16[128,512]{1,0:T(8,128)(2,1)S(1)}, u32[]{:S(2)}, u32[]{:S(2)}) collective-permute-start(bf16[128,512]{1,0:T(8,128)(2,1)} %shard_map.92.refs_1_), channel_id=1, source_target_pairs={{0,160},{32,192},{64,224},{96,0},{128,32},{160,64},{192,96},{224,1... | collective-permute-start | bytes 393224 | tf_op jit(solution)/shard_map/ppermute | solution.py:32
  89.3 20.4 %collective-permute-start.35 = (bf16[528,128]{1,0:T(8,128)(2,1)S(1)}, bf16[528,128]{1,0:T(8,128)(2,1)S(1)}, u32[]{:S(2)}, u32[]{:S(2)}) collective-permute-start(bf16[528,128]{1,0:T(8,128)(2,1)S(1)} %get-tuple-element.33), channel_id=1, source_target_pairs={{0,32},{32,64},{64,96},{96,128},{128,160},{160,192},{192,224},{224... | collective-permute-start | bytes 405512 | tf_op jit(solution)/shard_map/ppermute | solution.py:32
  97.1 13.6 %collective-permute-start.30 = (bf16[528,128]{1,0:T(8,128)(2,1)S(1)}, bf16[528,128]{1,0:T(8,128)(2,1)S(1)}, u32[]{:S(2)}, u32[]{:S(2)}) collective-permute-start(bf16[528,128]{1,0:T(8,128)(2,1)S(1)} %get-tuple-element.29), channel_id=1, source_target_pairs={{0,128},{32,160},{64,192},{96,224},{128,0},{160,32},{192,64},{224,... | collective-permute-start | bytes 405512 | tf_op jit(solution)/shard_map/ppermute | solution.py:32
  103.6 9.9 %collective-permute-start.31 = (bf16[528,128]{1,0:T(8,128)(2,1)S(1)}, bf16[528,128]{1,0:T(8,128)(2,1)S(1)}, u32[]{:S(2)}, u32[]{:S(2)}) collective-permute-start(bf16[528,128]{1,0:T(8,128)(2,1)S(1)} %get-tuple-element.30), channel_id=1, source_target_pairs={{0,192},{32,224},{64,0},{96,32},{128,64},{160,96},{192,128},{224,1... | collective-permute-start | bytes 405512 | tf_op jit(solution)/shard_map/ppermute | solution.py:32
  103.6 9.9 %collective-permute-start.32 = (bf16[528,128]{1,0:T(8,128)(2,1)S(1)}, bf16[528,128]{1,0:T(8,128)(2,1)S(1)}, u32[]{:S(2)}, u32[]{:S(2)}) collective-permute-start(bf16[528,128]{1,0:T(8,128)(2,1)S(1)} %get-tuple-element.31), channel_id=1, source_target_pairs={{0,64},{32,96},{64,128},{96,160},{128,192},{160,224},{192,0},{224,... | collective-permute-start | bytes 405512 | tf_op jit(solution)/shard_map/ppermute | solution.py:32
  109.8 11.4 %collective-permute-start.24 = (bf16[528,128]{1,0:T(8,128)(2,1)S(1)}, bf16[528,128]{1,0:T(8,128)(2,1)S(1)}, u32[]{:S(2)}, u32[]{:S(2)}) collective-permute-start(bf16[528,128]{1,0:T(8,128)(2,1)S(1)} %get-tuple-element.27), channel_id=1, source_target_pairs={{0,160},{32,192},{64,224},{96,0},{128,32},{160,64},{192,96},{224,1... | collective-permute-start | bytes 405512 | tf_op jit(solution)/shard_map/ppermute | solution.py:32
  110.7 10.5 %collective-permute-start.25 = (bf16[528,128]{1,0:T(8,128)(2,1)S(1)}, bf16[528,128]{1,0:T(8,128)(2,1)S(1)}, u32[]{:S(2)}, u32[]{:S(2)}) collective-permute-start(bf16[528,128]{1,0:T(8,128)(2,1)S(1)} %get-tuple-element.28), channel_id=1, source_target_pairs={{0,96},{32,128},{64,160},{96,192},{128,224},{160,0},{192,32},{224,... | collective-permute-start | bytes 405512 | tf_op jit(solution)/shard_map/ppermute | solution.py:32
  (28 other events, 197.1 us)

commit v2 on v1

--- a/solution.py
+++ b/solution.py
@@ -135,47 +135,87 @@
     )(*blocks, weight)
 
 
-def soft_part(q, keys, values, outs, arrivals):
-    scores = []
-    for m in range(NY):
-        if arrivals:
-            arrivals[m].wait()
-        block = jnp.concatenate([keys[m][k] for k in range(NX)], axis=1)
-        scores.append(lax.dot_general(
-            block, q, (((1,), (1,)), ((), ())), preferred_element_type=F32) * HD ** (-0.5))
-    top = functools.reduce(
-        jnp.maximum, [jnp.max(score, axis=0, keepdims=True) for score in scores])
+def write_part(out, part, top, total):
+    out[pl.ds(0, HD), :] = part.astype(BF)
+    pieces = []
+    for stat in (top, total):
+        for _ in range(3):
+            piece = stat.astype(BF).astype(F32)
+            pieces.append(piece)
+            stat = stat - piece
+    pieces.append(jnp.zeros((EXTRA - 6, 128), F32))
+    out[pl.ds(HD, EXTRA), :] = jnp.concatenate(pieces, axis=0).astype(BF)
+
+
+def shares_of(parts):
+    tops, totals = [], []
+    for part in parts:
+        stats = part[pl.ds(HD, EXTRA), :].astype(F32)
+        tops.append(stats[0:1] + stats[1:2] + stats[2:3])
+        totals.append(stats[3:4] + stats[4:5] + stats[5:6])
+    top = functools.reduce(jnp.maximum, tops)
+    shares = [total * jnp.exp(t - top) for t, total in zip(tops, totals)]
+    whole = functools.reduce(jnp.add, shares)
+    return [share / whole for share in shares], top, whole
+
+
+def merge_kernel(*refs):
+    n = len(refs) // 3
+    for i in range(n):
+        own, met, out = refs[i], refs[n + i], refs[2 * n + i]
+        (first, second), top, total = shares_of((own, met))
+        part = own[pl.ds(0, HD), :].astype(F32) * first + met[pl.ds(0, HD), :].astype(F32) * second
+        write_part(out, part, top, total)
+
+
+def merged(own, met):
+    n = len(own)
+    return pl.pallas_call(
+        merge_kernel,
+        out_shape=[jax.ShapeDtypeStruct((HD + EXTRA, 128), BF)] * n,
+        in_specs=[VMEM] * (2 * n),
+        out_specs=[VMEM] * n,
+        compiler_params=room(8),
+    )(*own, *met)
+
+
+def soft_part(q, keys, values, outs, arrivals, scores, numerator):
+    width = q.shape[0]
+    for arrival in arrivals[:NY]:
+        arrival.wait()
+
+    def score_step(m, top):
+        block = jnp.concatenate([keys[m, k] for k in range(NX)], axis=1)
+        scores[m] = lax.dot_general(
+            block, q, (((1,), (1,)), ((), ())), preferred_element_type=F32) * HD ** (-0.5)
+        return jnp.maximum(top, jnp.max(scores[m], axis=0, keepdims=True))
+
+    top = lax.fori_loop(0, NY, score_step, jnp.full((1, width), -jnp.inf, F32))
     for arrival in arrivals[NY:]:
         arrival.wait()
-    total, numerator = 0.0, 0.0
-    for m in range(NY):
+    numerator[...] = jnp.zeros_like(numerator)
+
+    def weight_step(m, total):
         weights = jnp.exp(scores[m] - top)
-        total = total + jnp.sum(weights, axis=0, keepdims=True)
         block = jnp.concatenate([
             jnp.concatenate(
-                [values[k][m, pl.ds(row, 128), :] for row in (256, 384, 0, 128)], axis=1)
+                [values[k, m, pl.ds(row, 128), :] for row in (256, 384, 0, 128)], axis=1)
             for k in range(NX)], axis=0)
-        numerator = numerator + jnp.dot(
-            block, weights.astype(BF), preferred_element_type=F32)
-    part = numerator / total
+        numerator[...] += jnp.dot(block, weights.astype(BF), preferred_element_type=F32)
+        return total + jnp.sum(weights, axis=0, keepdims=True)
+
+    total = lax.fori_loop(0, NY, weight_step, jnp.zeros((1, width), F32))
     for side, out in enumerate(outs):
         cols = slice(side * 128, side * 128 + 128)
-        out[pl.ds(0, HD), :] = part[:, cols].astype(BF)
-        pieces = []
-        for stat in (top[:, cols], total[:, cols]):
-            for _ in range(3):
-                piece = stat.astype(BF).astype(F32)
-                pieces.append(piece)
-                stat = stat - piece
-        pieces.append(jnp.zeros((EXTRA - 6, 128), F32))
-        out[pl.ds(HD, EXTRA), :] = jnp.concatenate(pieces, axis=0).astype(BF)
+        write_part(out, numerator[:, cols] / total[:, cols], top[:, cols], total[:, cols])
 
 
 def attend_kernel(n, *refs):
     queries, refs = refs[:n], refs[n:]
     near, other = refs[:NX], refs[NX : 2 * NX]
-    outs = refs[2 * NX : -3]
-    keys, values, sems = refs[-3:]
+    outs = refs[2 * NX : 2 * NX + n]
+    keys, values, sems = refs[2 * NX + n : 2 * NX + n + 3]
+    work = refs[2 * NX + n + 3 :]
     core = lax.axis_index("c")
 
     def copies(key_blocks, value_blocks):
@@ -197,17 +237,19 @@
     arrivals = copies(near, other)
     for i in range(0, n, 2):
         q = jnp.concatenate([query[...] for query in queries[i : i + 2]], axis=0)
-        soft_part(q, keys, values, outs[i : i + 2], arrivals if i == 0 else [])
+        soft_part(q, keys, values, outs[i : i + 2], arrivals if i == 0 else [], *work)
 
 
 def attend(shifts, queries, near, other):
     n = len(shifts)
+    work = [pltpu.VMEM((4, 512, 256), F32), pltpu.VMEM((HD, 256), F32)]
     return dict(zip(shifts, pl.pallas_call(
         functools.partial(attend_kernel, n),
         out_shape=[jax.ShapeDtypeStruct((HD + EXTRA, 128), BF)] * n,
         in_specs=[VMEM] * n + [ANY] * 8,
         out_specs=[VMEM] * n,
-        scratch_shapes=[pltpu.VMEM((4, 4, 512, 128), BF)] * 2 + [pltpu.SemaphoreType.DMA((8,))],
+        scratch_shapes=[pltpu.VMEM((4, 4, 512, 128), BF)] * 2 + [
+            pltpu.SemaphoreType.DMA((8,))] + work,
         compiler_params=room(28),
         cost_estimate=pl.CostEstimate(
             flops=4 * 128 * n * 2048 * HD, bytes_accessed=4 << 20,
@@ -216,18 +258,10 @@
 
 
 def combine_kernel(*refs):
-    arrived = refs[:NZ]
-    weight, kept, sent, attended = refs[NZ:]
+    arrived = refs[:3]
+    weight, kept, sent, attended = refs[3:]
     x = lax.axis_index("x")
-    tops, totals = [], []
-    for part in arrived:
-        stats = part[pl.ds(HD, EXTRA), :].astype(F32)
-        tops.append(stats[0:1] + stats[1:2] + stats[2:3])
-        totals.append(stats[3:4] + stats[4:5] + stats[5:6])
-    top = functools.reduce(jnp.maximum, tops)
-    shares = [total * jnp.exp(t - top) for t, total in zip(tops, totals)]
-    whole = sum(shares)
-    shares = [share / whole for share in shares]
+    shares, _, _ = shares_of(arrived)
     for k in range(NX):
         block = sum(
             part[pl.ds(k * 128, 128), :].astype(F32) * share
@@ -244,7 +278,7 @@
     return pl.pallas_call(
         combine_kernel,
         out_shape=[jax.ShapeDtypeStruct((64, 2048), F32), jax.ShapeDtypeStruct((64, 2048), BF)],
-        in_specs=[VMEM] * (NZ + 1),
+        in_specs=[VMEM] * 4,
         out_specs=[VMEM] * 2,
         scratch_shapes=[pltpu.VMEM((128, HD), BF)],
         compiler_params=room(16),
@@ -326,14 +360,20 @@
     other = [moved(block, "c", 1) for block in near]
 
 
-    parts, arrived = {}, []
-    for shifts in ((3, 5), (4, 2, 6, 1), (7, 0)):
-        parts.update(attend(shifts, queries, near, other))
-        for k in shifts:
-            if k:
-                arrived.append(moved(parts[k], "z", -k))
-    arrived.append(parts[0])
-    kept, sent = combine(arrived, w_out[0])
+    sums = []
+    for step, shifts in enumerate(((4, 3), (5, 2), (6, 1), (7, 0))):
+        parts = attend(shifts, queries, near, other)
+        if step == 0:
+            sums = [parts[4], parts[3]]
+        elif step < 3:
+            sums = list(merged([parts[k] for k in shifts], sums))
+        else:
+            sums[0] = merged([parts[7]], sums[:1])[0]
+        sums[0] = moved(sums[0], "z", 1)
+        if step < 3:
+            sums[1] = moved(sums[1], "z", -1)
+    last = parts[0]
+    kept, sent = combine([last] + sums, w_out[0])
     met = moved(sent, "c", 1)
     own, one, two, three = pair_sum(kept, met)
     two = moved(two, "x", -2)

time: 138 us -> 145 us (1.051)
  waiting for transfers between devices: 55 us -> 59.2 us
  Pallas kernels: 20.9 us -> 23.8 us
    ppermute x34, waiting for transfers between devices: 51.1 us -> 56.2 us  [moved(): return lax.ppermute(array, axis, [(i, (i + shift) % n) for i in range(n)])]
    pallas_call x3 -> x4, Pallas kernels: 13.7 us -> 16.2 us  [attend(): pl.pallas_call(functools.partial(attend_kernel, n), out_shape=[jax.ShapeD...]
  transfers between devices with their start and end apart: 40 -> 40, of which waited for: 22 -> 19; matrix products, arithmetic and copies ran while one was open for 0% -> 0% of each run, Pallas kernels for 13% -> 15%
where the time goes in v2:
time: 145 us; the launch traced here: 144 us
  waiting for transfers between devices  59.2 us (41%)
  starting transfers between devices  58.3 us (40%)
  Pallas kernels  23.8 us (16%)
  local copies, waits for them, and re-layouts  1.6 us (1%)
    ppermute x34, waiting for transfers between devices, moved(): return lax.ppermute(array, axis, [(i, (i + shift) % n) for i in range(n)])  56.2 us
    ppermute x34, starting transfers between devices, moved(): return lax.ppermute(array, axis, [(i, (i + shift) % n) for i in range(n)])  50.5 us
    pallas_call x4, Pallas kernels, attend(): pl.pallas_call(functools.partial(attend_kernel, n), out_shape=[jax.ShapeD...  16.2 us
    ppermute x6, starting transfers between devices, by_role(): return lax.ppermute(array, ('y', 'x', 'c'), pairs)  7.81 us
    ppermute x6, waiting for transfers between devices, by_role(): return lax.ppermute(array, ('y', 'x', 'c'), pairs)  3.05 us
  transfers between devices with their start and end apart: 40, of which 19 were waited for; matrix products, arithmetic and copies ran while one was open for 0% of the time, Pallas kernels for 15%

profile of v2, /device:TPU:1, one launch (start us, length us, event | category | flops | bytes accessed | tf_op | source)
XLA Modules:
  0.0 144.3 jit_solution(3182675828799911047)
XLA Ops:
  1.1 3.3 %collective-permute-start.11 = (bf16[128,2048]{1,0:T(8,128)(2,1)S(1)}, bf16[128,2048]{1,0:T(8,128)(2,1)S(1)}, u32[]{:S(2)}, u32[]{:S(2)}) collective-permute-start(bf16[128,2048]{1,0:T(8,128)(2,1)S(1)} %pad_maximum_fusion.refs_4_), channel_id=1, source_target_pairs={{0,1},{1,0},{2,3},{3,2},{4,5},{5,4},{6,7},{7,6},{8,9},{9,8},{10,11... | collective-permute-start | bytes 1572872 | tf_op jit(solution)/shard_map/ppermute | solution.py:32
  8.9 5.6 %collective-permute-done.10.refs_3_ = bf16[64,2048]{1,0:T(8,128)(2,1)S(1)} collective-permute-done((bf16[64,2048]{1,0:T(8,128)(2,1)}, bf16[64,2048]{1,0:T(8,128)(2,1)S(1)}, u32[]{:S(2)}, u32[]{:S(2)}) %collective-permute-start.10) | collective-permute-done | bytes 262176 | tf_op jit(solution)/shard_map/ppermute | solution.py:32
  14.4 7.3 %collective-permute-done.8.refs_1_ = bf16[64,2048]{1,0:T(8,128)(2,1)S(1)} collective-permute-done((bf16[64,2048]{1,0:T(8,128)(2,1)}, bf16[64,2048]{1,0:T(8,128)(2,1)S(1)}, u32[]{:S(2)}, u32[]{:S(2)}) %collective-permute-start.8) | collective-permute-done | bytes 262176 | tf_op jit(solution)/shard_map/ppermute | solution.py:32
  27.2 2.6 %collective-permute-start.14 = (bf16[512,128]{1,0:T(8,128)(2,1)S(1)}, bf16[512,128]{1,0:T(8,128)(2,1)S(1)}, u32[]{:S(2)}, u32[]{:S(2)}) collective-permute-start(bf16[512,128]{1,0:T(8,128)(2,1)S(1)} %constant_dynamic-update-slice_fusion), channel_id=1, source_target_pairs={{0,4},{1,17},{2,6},{3,19},{4,0},{5,21},{6,2},{7,23},{8,12},{9,25},... | collective-permute-start | bytes 393224 | tf_op jit(solution)/shard_map/ppermute | solution.py:332
  39.2 12.6 %collective-permute-done.1.refs_2_ = bf16[16,2048]{1,0:T(8,128)(2,1)S(1)} collective-permute-done((bf16[16,2048]{1,0:T(8,128)(2,1)S(1)}, bf16[16,2048]{1,0:T(8,128)(2,1)S(1)}, u32[]{:S(2)}, u32[]{:S(2)}) %collective-permute-start.1) | collective-permute-done | bytes 65568 | tf_op jit(solution)/shard_map/ppermute | solution.py:32
  51.9 3.5 %collective-permute-done.5.refs_6_ = bf16[16,2048]{1,0:T(8,128)(2,1)S(1)} collective-permute-done((bf16[16,2048]{1,0:T(8,128)(2,1)S(1)}, bf16[16,2048]{1,0:T(8,128)(2,1)S(1)}, u32[]{:S(2)}, u32[]{:S(2)}) %collective-permute-start.5) | collective-permute-done | bytes 65568 | tf_op jit(solution)/shard_map/ppermute | solution.py:32
  56.9 2.9 %collective-permute-done.2.refs_3_ = bf16[16,2048]{1,0:T(8,128)(2,1)S(1)} collective-permute-done((bf16[16,2048]{1,0:T(8,128)(2,1)S(1)}, bf16[16,2048]{1,0:T(8,128)(2,1)S(1)}, u32[]{:S(2)}, u32[]{:S(2)}) %collective-permute-start.2) | collective-permute-done | bytes 65568 | tf_op jit(solution)/shard_map/ppermute | solution.py:32
  62.9 2.8 %shard_map.92.refs_1_ = bf16[128,512]{1,0:T(8,128)(2,1)} custom-call(bf16[16,2048]{1,0:T(8,128)(2,1)} %get-tuple-element.27.refs_0_, bf16[16,2048]{1,0:T(8,128)(2,1)} %copy-done.9, bf16[16,2048]{1,0:T(8,128)(2,1)} %copy-done.6, bf16[16,2048]{1,0:T(8,128)(2,1)} %copy-done.10, bf16[16,2048]{1,0:T(8,128)(2,1)} %copy-done.7, bf16[16,2048]{1,0:T(8,128)(2,1)} %copy-done.11, ...), custom_call_target="tpu_custom_call" | custom-call | flops 268435456 | bytes 3145728 | tf_op jit(solution)/shard_map/pallas_call | solution.py:124
  65.8 7.0 %collective-permute-start.27 = (bf16[128,512]{1,0:T(8,128)(2,1)}, bf16[128,512]{1,0:T(8,128)(2,1)S(1)}, u32[]{:S(2)}, u32[]{:S(2)}) collective-permute-start(bf16[128,512]{1,0:T(8,128)(2,1)} %shard_map.92.refs_1_), channel_id=1, source_target_pairs={{0,128},{32,160},{64,192},{96,224},{128,0},{160,32},{192,64},{224,... | collective-permute-start | bytes 393224 | tf_op jit(solution)/shard_map/ppermute | solution.py:32
  72.8 3.7 %collective-permute-done.27.refs_0_ = bf16[128,512]{1,0:T(8,128)(2,1)S(1)} collective-permute-done((bf16[128,512]{1,0:T(8,128)(2,1)}, bf16[128,512]{1,0:T(8,128)(2,1)S(1)}, u32[]{:S(2)}, u32[]{:S(2)}) %collective-permute-start.27) | collective-permute-done | bytes 131104 | tf_op jit(solution)/shard_map/ppermute | solution.py:32
  76.5 2.5 %collective-permute-start.28 = (bf16[128,512]{1,0:T(8,128)(2,1)}, bf16[128,512]{1,0:T(8,128)(2,1)S(1)}, u32[]{:S(2)}, u32[]{:S(2)}) collective-permute-start(bf16[128,512]{1,0:T(8,128)(2,1)} %shard_map.92.refs_1_), channel_id=1, source_target_pairs={{0,96},{32,128},{64,160},{96,192},{128,224},{160,0},{192,32},{224,... | collective-permute-start | bytes 393224 | tf_op jit(solution)/shard_map/ppermute | solution.py:32
  79.0 6.2 %collective-permute-done.28.refs_1_ = bf16[128,512]{1,0:T(8,128)(2,1)S(1)} collective-permute-done((bf16[128,512]{1,0:T(8,128)(2,1)}, bf16[128,512]{1,0:T(8,128)(2,1)S(1)}, u32[]{:S(2)}, u32[]{:S(2)}) %collective-permute-start.28) | collective-permute-done | bytes 131104 | tf_op jit(solution)/shard_map/ppermute | solution.py:32
  85.2 6.8 %collective-permute-start.25 = (bf16[128,512]{1,0:T(8,128)(2,1)}, bf16[128,512]{1,0:T(8,128)(2,1)S(1)}, u32[]{:S(2)}, u32[]{:S(2)}) collective-permute-start(bf16[128,512]{1,0:T(8,128)(2,1)} %shard_map.92.refs_1_), channel_id=1, source_target_pairs={{0,160},{32,192},{64,224},{96,0},{128,32},{160,64},{192,96},{224,1... | collective-permute-start | bytes 393224 | tf_op jit(solution)/shard_map/ppermute | solution.py:32
  92.1 4.1 %shard_map.97 = (bf16[528,128]{1,0:T(8,128)(2,1)S(1)}, bf16[528,128]{1,0:T(8,128)(2,1)S(1)}) custom-call(bf16[128,512]{1,0:T(8,128)(2,1)S(1)} %collective-permute-done.27.refs_0_, bf16[128,512]{1,0:T(8,128)(2,1)S(1)} %collective-permute-done.28.refs_1_, bf16[4,512,128]{2,1,0:T(8,128)(2,1)S(1)} %pad_maximum_fusion.1.refs_2_, ...), custom_call_target="tpu_custom_call" | custom-call | flops 1073741824 | bytes 4194304 | tf_op jit(solution)/shard_map/pallas_call | solution.py:246
  96.2 6.2 %collective-permute-start.29 = (bf16[528,128]{1,0:T(8,128)(2,1)S(1)}, bf16[528,128]{1,0:T(8,128)(2,1)S(1)}, u32[]{:S(2)}, u32[]{:S(2)}) collective-permute-start(bf16[528,128]{1,0:T(8,128)(2,1)S(1)} %get-tuple-element.37), channel_id=1, source_target_pairs={{0,32},{32,64},{64,96},{96,128},{128,160},{160,192},{192,224},{224... | collective-permute-start | bytes 405512 | tf_op jit(solution)/shard_map/ppermute | solution.py:32
  107.4 4.1 %shard_map.96 = (bf16[528,128]{1,0:T(8,128)(2,1)S(1)}, bf16[528,128]{1,0:T(8,128)(2,1)S(1)}) custom-call(bf16[128,512]{1,0:T(8,128)(2,1)S(1)} %collective-permute-done.25.refs_0_, bf16[128,512]{1,0:T(8,128)(2,1)S(1)} %collective-permute-done.26.refs_1_, bf16[4,512,128]{2,1,0:T(8,128)(2,1)S(1)} %pad_maximum_fusion.1.refs_2_, ...), custom_call_target="tpu_custom_call" | custom-call | flops 1073741824 | bytes 4194304 | tf_op jit(solution)/shard_map/pallas_call | solution.py:246
  111.7 2.6 %collective-permute-start.32 = (bf16[528,128]{1,0:T(8,128)(2,1)S(1)}, bf16[528,128]{1,0:T(8,128)(2,1)S(1)}, u32[]{:S(2)}, u32[]{:S(2)}) collective-permute-start(bf16[528,128]{1,0:T(8,128)(2,1)S(1)} %get-tuple-element.40), channel_id=1, source_target_pairs={{0,224},{32,0},{64,32},{96,64},{128,96},{160,128},{192,160},{224,1... | collective-permute-start | bytes 405512 | tf_op jit(solution)/shard_map/ppermute | solution.py:32
  114.4 4.0 %shard_map.95 = (bf16[528,128]{1,0:T(8,128)(2,1)S(1)}, bf16[528,128]{1,0:T(8,128)(2,1)S(1)}) custom-call(bf16[128,512]{1,0:T(8,128)(2,1)S(1)} %collective-permute-done.23.refs_0_, bf16[128,512]{1,0:T(8,128)(2,1)S(1)} %collective-permute-done.24.refs_1_, bf16[4,512,128]{2,1,0:T(8,128)(2,1)S(1)} %pad_maximum_fusion.1.refs_2_, ...), custom_call_target="tpu_custom_call" | custom-call | flops 1073741824 | bytes 4194304 | tf_op jit(solution)/shard_map/pallas_call | solution.py:246
  120.2 4.1 %shard_map.94 = (bf16[528,128]{1,0:T(8,128)(2,1)S(1)}, bf16[528,128]{1,0:T(8,128)(2,1)S(1)}) custom-call(bf16[128,512]{1,0:T(8,128)(2,1)S(1)} %collective-permute-done.7.refs_0_, bf16[128,512]{1,0:T(8,128)(2,1)S(1)} %copy-done.1, bf16[4,512,128]{2,1,0:T(8,128)(2,1)S(1)} %pad_maximum_fusion.1.refs_2_, ...), custom_call_target="tpu_custom_call" | custom-call | flops 1073741824 | bytes 4194304 | tf_op jit(solution)/shard_map/pallas_call | solution.py:246
  124.3 2.5 %collective-permute-start.35 = (bf16[528,128]{1,0:T(8,128)(2,1)S(1)}, bf16[528,128]{1,0:T(8,128)(2,1)S(1)}, u32[]{:S(2)}, u32[]{:S(2)}) collective-permute-start(bf16[528,128]{1,0:T(8,128)(2,1)S(1)} %get-tuple-element.42), channel_id=1, source_target_pairs={{0,224},{32,0},{64,32},{96,64},{128,96},{160,128},{192,160},{224,1... | collective-permute-start | bytes 405512 | tf_op jit(solution)/shard_map/ppermute | solution.py:32
  126.9 2.5 %collective-permute-done.35.refs_2_ = bf16[528,128]{1,0:T(8,128)(2,1)S(1)} collective-permute-done((bf16[528,128]{1,0:T(8,128)(2,1)S(1)}, bf16[528,128]{1,0:T(8,128)(2,1)S(1)}, u32[]{:S(2)}, u32[]{:S(2)}) %collective-permute-start.35) | collective-permute-done | bytes 135200 | tf_op jit(solution)/shard_map/ppermute | solution.py:32
  129.4 2.6 %collective-permute-done.34.refs_1_ = bf16[528,128]{1,0:T(8,128)(2,1)S(1)} collective-permute-done((bf16[528,128]{1,0:T(8,128)(2,1)S(1)}, bf16[528,128]{1,0:T(8,128)(2,1)S(1)}, u32[]{:S(2)}, u32[]{:S(2)}) %collective-permute-start.34) | collective-permute-done | bytes 135200 | tf_op jit(solution)/shard_map/ppermute | solution.py:32
  132.6 2.4 %collective-permute-start.36 = (bf16[64,2048]{1,0:T(8,128)(2,1)S(1)}, bf16[64,2048]{1,0:T(8,128)(2,1)S(1)}, u32[]{:S(2)}, u32[]{:S(2)}) collective-permute-start(bf16[64,2048]{1,0:T(8,128)(2,1)S(1)} %get-tuple-element.44), channel_id=1, source_target_pairs={{0,1},{1,0},{2,3},{3,2},{4,5},{5,4},{6,7},{7,6},{8,9},{9,8},{10,11... | collective-permute-start | bytes 786440 | tf_op jit(solution)/shard_map/ppermute | solution.py:32
  139.4 2.7 %collective-permute-done.38.two = bf16[16,2048]{1,0:T(8,128)(2,1)S(1)} collective-permute-done((bf16[16,2048]{1,0:T(8,128)(2,1)S(1)}, bf16[16,2048]{1,0:T(8,128)(2,1)S(1)}, u32[]{:S(2)}, u32[]{:S(2)}) %collective-permute-start.38) | collective-permute-done | bytes 65568 | tf_op jit(solution)/shard_map/ppermute | solution.py:32
  (99 shorter events, 39.3 us)
Async XLA Ops:
  1.1 20.7 %collective-permute-start.11 = (bf16[128,2048]{1,0:T(8,128)(2,1)S(1)}, bf16[128,2048]{1,0:T(8,128)(2,1)S(1)}, u32[]{:S(2)}, u32[]{:S(2)}) collective-permute-start(bf16[128,2048]{1,0:T(8,128)(2,1)S(1)} %pad_maximum_fusion.refs_4_), channel_id=1, source_target_pairs={{0,1},{1,0},{2,3},{3,2},{4,5},{5,4},{6,7},{7,6},{8,9},{9,8},{10,11... | collective-permute-start | bytes 1572872 | tf_op jit(solution)/shard_map/ppermute | solution.py:32
  6.3 8.1 %collective-permute-start.10 = (bf16[64,2048]{1,0:T(8,128)(2,1)}, bf16[64,2048]{1,0:T(8,128)(2,1)S(1)}, u32[]{:S(2)}, u32[]{:S(2)}) collective-permute-start(bf16[64,2048]{1,0:T(8,128)(2,1)} %get-tuple-element.28.refs_0_), channel_id=1, source_target_pairs={{0,6},{2,0},{4,2},{6,4},{1,7},{3,1},{5,3},{7,5},{8,14},{10,8},{12,... | collective-permute-start | bytes 786440 | tf_op jit(solution)/shard_map/ppermute | solution.py:32
  7.1 14.6 %collective-permute-start.8 = (bf16[64,2048]{1,0:T(8,128)(2,1)}, bf16[64,2048]{1,0:T(8,128)(2,1)S(1)}, u32[]{:S(2)}, u32[]{:S(2)}) collective-permute-start(bf16[64,2048]{1,0:T(8,128)(2,1)} %get-tuple-element.28.refs_0_), channel_id=1, source_target_pairs={{0,2},{2,4},{4,6},{6,0},{1,3},{3,5},{5,7},{7,1},{8,10},{10,12},{12... | collective-permute-start | bytes 786440 | tf_op jit(solution)/shard_map/ppermute | solution.py:32
  7.8 13.9 %collective-permute-start.9 = (bf16[64,2048]{1,0:T(8,128)(2,1)}, bf16[64,2048]{1,0:T(8,128)(2,1)S(1)}, u32[]{:S(2)}, u32[]{:S(2)}) collective-permute-start(bf16[64,2048]{1,0:T(8,128)(2,1)} %get-tuple-element.28.refs_0_), channel_id=1, source_target_pairs={{0,4},{2,6},{4,0},{6,2},{1,5},{3,7},{5,1},{7,3},{8,12},{10,14},{12... | collective-permute-start | bytes 786440 | tf_op jit(solution)/shard_map/ppermute | solution.py:32
  34.1 21.8 %collective-permute-start.16 = (bf16[4,512,128]{2,1,0:T(8,128)(2,1)S(1)}, bf16[4,512,128]{2,1,0:T(8,128)(2,1)S(1)}, u32[]{:S(2)}, u32[]{:S(2)}) collective-permute-start(bf16[4,512,128]{2,1,0:T(8,128)(2,1)S(1)} %pad_maximum_fusion.1.refs_2_), channel_id=1, source_target_pairs={{0,8},{1,3},{2,10},{3,5},{4,12},{5,7},{6,14},{7,1},{8,16},{9,11},{... | collective-permute-start | bytes 1572872 | tf_op jit(solution)/shard_map/ppermute | solution.py:332
  34.1 21.8 %collective-permute-start.17 = (bf16[4,512,128]{2,1,0:T(8,128)(2,1)S(1)}, bf16[4,512,128]{2,1,0:T(8,128)(2,1)S(1)}, u32[]{:S(2)}, u32[]{:S(2)}) collective-permute-start(bf16[4,512,128]{2,1,0:T(8,128)(2,1)S(1)} %pad_maximum_fusion.1.refs_2_), channel_id=1, source_target_pairs={{0,16},{1,5},{2,18},{3,7},{4,20},{5,1},{6,22},{7,3},{8,24},{9,13},... | collective-permute-start | bytes 1572872 | tf_op jit(solution)/shard_map/ppermute | solution.py:332
  35.3 21.0 %collective-permute-start.18 = (bf16[4,512,128]{2,1,0:T(8,128)(2,1)S(1)}, bf16[4,512,128]{2,1,0:T(8,128)(2,1)S(1)}, u32[]{:S(2)}, u32[]{:S(2)}) collective-permute-start(bf16[4,512,128]{2,1,0:T(8,128)(2,1)S(1)} %pad_maximum_fusion.1.refs_2_), channel_id=1, source_target_pairs={{0,24},{1,7},{2,26},{3,1},{4,28},{5,3},{6,30},{7,5},{8,0},{9,15},{... | collective-permute-start | bytes 1572872 | tf_op jit(solution)/shard_map/ppermute | solution.py:332
  36.8 15.0 %collective-permute-start.1 = (bf16[16,2048]{1,0:T(8,128)(2,1)S(1)}, bf16[16,2048]{1,0:T(8,128)(2,1)S(1)}, u32[]{:S(2)}, u32[]{:S(2)}) collective-permute-start(bf16[16,2048]{1,0:T(8,128)(2,1)S(1)} %copy-done.5), channel_id=1, source_target_pairs={{0,2},{2,4},{4,6},{6,0},{1,3},{3,5},{5,7},{7,1},{8,10},{10,12},{12... | collective-permute-start | bytes 196616 | tf_op jit(solution)/shard_map/ppermute | solution.py:32
  37.4 14.4 %collective-permute-start.3 = (bf16[16,2048]{1,0:T(8,128)(2,1)S(1)}, bf16[16,2048]{1,0:T(8,128)(2,1)S(1)}, u32[]{:S(2)}, u32[]{:S(2)}) collective-permute-start(bf16[16,2048]{1,0:T(8,128)(2,1)S(1)} %copy-done.5), channel_id=1, source_target_pairs={{0,4},{2,6},{4,0},{6,2},{1,5},{3,7},{5,1},{7,3},{8,12},{10,14},{12... | collective-permute-start | bytes 196616 | tf_op jit(solution)/shard_map/ppermute | solution.py:32
  55.4 36.6 %collective-permute-start.19 = (bf16[4,512,128]{2,1,0:T(8,128)(2,1)S(1)}, bf16[4,512,128]{2,1,0:T(8,128)(2,1)S(1)}, u32[]{:S(2)}, u32[]{:S(2)}) collective-permute-start(bf16[4,512,128]{2,1,0:T(8,128)(2,1)S(1)} %pad_maximum_fusion.1.refs_2_), channel_id=1, source_target_pairs={{0,1},{1,0},{2,3},{3,2},{4,5},{5,4},{6,7},{7,6},{8,9},{9,8},{10,11... | collective-permute-start | bytes 1572872 | tf_op jit(solution)/shard_map/ppermute | solution.py:32
  55.8 36.2 %collective-permute-start.20 = (bf16[4,512,128]{2,1,0:T(8,128)(2,1)S(1)}, bf16[4,512,128]{2,1,0:T(8,128)(2,1)S(1)}, u32[]{:S(2)}, u32[]{:S(2)}) collective-permute-start(bf16[4,512,128]{2,1,0:T(8,128)(2,1)S(1)} %collective-permute-done.16.refs_3_), channel_id=1, source_target_pairs={{0,1},{1,0},{2,3},{3,2},{4,5},{5,4},{6,7},{7,6},{8,9},{9,8},{10,11... | collective-permute-start | bytes 1572872 | tf_op jit(solution)/shard_map/ppermute | solution.py:32
  55.9 36.1 %collective-permute-start.21 = (bf16[4,512,128]{2,1,0:T(8,128)(2,1)S(1)}, bf16[4,512,128]{2,1,0:T(8,128)(2,1)S(1)}, u32[]{:S(2)}, u32[]{:S(2)}) collective-permute-start(bf16[4,512,128]{2,1,0:T(8,128)(2,1)S(1)} %collective-permute-done.17.refs_4_), channel_id=1, source_target_pairs={{0,1},{1,0},{2,3},{3,2},{4,5},{5,4},{6,7},{7,6},{8,9},{9,8},{10,11... | collective-permute-start | bytes 1572872 | tf_op jit(solution)/shard_map/ppermute | solution.py:32
  56.3 35.7 %collective-permute-start.22 = (bf16[4,512,128]{2,1,0:T(8,128)(2,1)S(1)}, bf16[4,512,128]{2,1,0:T(8,128)(2,1)}, u32[]{:S(2)}, u32[]{:S(2)}) collective-permute-start(bf16[4,512,128]{2,1,0:T(8,128)(2,1)S(1)} %collective-permute-done.18.refs_5_), channel_id=1, source_target_pairs={{0,1},{1,0},{2,3},{3,2},{4,5},{5,4},{6,7},{7,6},{8,9},{9,8},{10,11... | collective-permute-start | bytes 1572872 | tf_op jit(solution)/shard_map/ppermute | solution.py:32
  65.8 10.7 %collective-permute-start.27 = (bf16[128,512]{1,0:T(8,128)(2,1)}, bf16[128,512]{1,0:T(8,128)(2,1)S(1)}, u32[]{:S(2)}, u32[]{:S(2)}) collective-permute-start(bf16[128,512]{1,0:T(8,128)(2,1)} %shard_map.92.refs_1_), channel_id=1, source_target_pairs={{0,128},{32,160},{64,192},{96,224},{128,0},{160,32},{192,64},{224,... | collective-permute-start | bytes 393224 | tf_op jit(solution)/shard_map/ppermute | solution.py:32
  76.5 8.7 %collective-permute-start.28 = (bf16[128,512]{1,0:T(8,128)(2,1)}, bf16[128,512]{1,0:T(8,128)(2,1)S(1)}, u32[]{:S(2)}, u32[]{:S(2)}) collective-permute-start(bf16[128,512]{1,0:T(8,128)(2,1)} %shard_map.92.refs_1_), channel_id=1, source_target_pairs={{0,96},{32,128},{64,160},{96,192},{128,224},{160,0},{192,32},{224,... | collective-permute-start | bytes 393224 | tf_op jit(solution)/shard_map/ppermute | solution.py:32
  85.2 20.7 %collective-permute-start.25 = (bf16[128,512]{1,0:T(8,128)(2,1)}, bf16[128,512]{1,0:T(8,128)(2,1)S(1)}, u32[]{:S(2)}, u32[]{:S(2)}) collective-permute-start(bf16[128,512]{1,0:T(8,128)(2,1)} %shard_map.92.refs_1_), channel_id=1, source_target_pairs={{0,160},{32,192},{64,224},{96,0},{128,32},{160,64},{192,96},{224,1... | collective-permute-start | bytes 393224 | tf_op jit(solution)/shard_map/ppermute | solution.py:32
  92.1 15.3 %collective-permute-start.26 = (bf16[128,512]{1,0:T(8,128)(2,1)}, bf16[128,512]{1,0:T(8,128)(2,1)S(1)}, u32[]{:S(2)}, u32[]{:S(2)}) collective-permute-start(bf16[128,512]{1,0:T(8,128)(2,1)} %shard_map.92.refs_1_), channel_id=1, source_target_pairs={{0,64},{32,96},{64,128},{96,160},{128,192},{160,224},{192,0},{224,... | collective-permute-start | bytes 393224 | tf_op jit(solution)/shard_map/ppermute | solution.py:32
  96.2 15.3 %collective-permute-start.29 = (bf16[528,128]{1,0:T(8,128)(2,1)S(1)}, bf16[528,128]{1,0:T(8,128)(2,1)S(1)}, u32[]{:S(2)}, u32[]{:S(2)}) collective-permute-start(bf16[528,128]{1,0:T(8,128)(2,1)S(1)} %get-tuple-element.37), channel_id=1, source_target_pairs={{0,32},{32,64},{64,96},{96,128},{128,160},{160,192},{192,224},{224... | collective-permute-start | bytes 405512 | tf_op jit(solution)/shard_map/ppermute | solution.py:32
  102.4 9.1 %collective-permute-start.30 = (bf16[528,128]{1,0:T(8,128)(2,1)S(1)}, bf16[528,128]{1,0:T(8,128)(2,1)S(1)}, u32[]{:S(2)}, u32[]{:S(2)}) collective-permute-start(bf16[528,128]{1,0:T(8,128)(2,1)S(1)} %get-tuple-element.38), channel_id=1, source_target_pairs={{0,224},{32,0},{64,32},{96,64},{128,96},{160,128},{192,160},{224,1... | collective-permute-start | bytes 405512 | tf_op jit(solution)/shard_map/ppermute | solution.py:32
  104.8 9.6 %collective-permute-start.23 = (bf16[128,512]{1,0:T(8,128)(2,1)S(1)}, bf16[128,512]{1,0:T(8,128)(2,1)S(1)}, u32[]{:S(2)}, u32[]{:S(2)}) collective-permute-start(bf16[128,512]{1,0:T(8,128)(2,1)S(1)} %copy-done.1), channel_id=1, source_target_pairs={{0,192},{32,224},{64,0},{96,32},{128,64},{160,96},{192,128},{224,1... | collective-permute-start | bytes 393224 | tf_op jit(solution)/shard_map/ppermute | solution.py:32
  105.9 8.5 %collective-permute-start.24 = (bf16[128,512]{1,0:T(8,128)(2,1)S(1)}, bf16[128,512]{1,0:T(8,128)(2,1)S(1)}, u32[]{:S(2)}, u32[]{:S(2)}) collective-permute-start(bf16[128,512]{1,0:T(8,128)(2,1)S(1)} %copy-done.1), channel_id=1, source_target_pairs={{0,32},{32,64},{64,96},{96,128},{128,160},{160,192},{192,224},{224... | collective-permute-start | bytes 393224 | tf_op jit(solution)/shard_map/ppermute | solution.py:32
  111.6 6.8 %collective-permute-start.31 = (bf16[528,128]{1,0:T(8,128)(2,1)S(1)}, bf16[528,128]{1,0:T(8,128)(2,1)S(1)}, u32[]{:S(2)}, u32[]{:S(2)}) collective-permute-start(bf16[528,128]{1,0:T(8,128)(2,1)S(1)} %get-tuple-element.39), channel_id=1, source_target_pairs={{0,32},{32,64},{64,96},{96,128},{128,160},{160,192},{192,224},{224... | collective-permute-start | bytes 405512 | tf_op jit(solution)/shard_map/ppermute | solution.py:32
  111.7 6.7 %collective-permute-start.32 = (bf16[528,128]{1,0:T(8,128)(2,1)S(1)}, bf16[528,128]{1,0:T(8,128)(2,1)S(1)}, u32[]{:S(2)}, u32[]{:S(2)}) collective-permute-start(bf16[528,128]{1,0:T(8,128)(2,1)S(1)} %get-tuple-element.40), channel_id=1, source_target_pairs={{0,224},{32,0},{64,32},{96,64},{128,96},{160,128},{192,160},{224,1... | collective-permute-start | bytes 405512 | tf_op jit(solution)/shard_map/ppermute | solution.py:32
  118.6 8.1 %collective-permute-start.33 = (bf16[528,128]{1,0:T(8,128)(2,1)S(1)}, bf16[528,128]{1,0:T(8,128)(2,1)S(1)}, u32[]{:S(2)}, u32[]{:S(2)}) collective-permute-start(bf16[528,128]{1,0:T(8,128)(2,1)S(1)} %get-tuple-element.41), channel_id=1, source_target_pairs={{0,32},{32,64},{64,96},{96,128},{128,160},{160,192},{192,224},{224... | collective-permute-start | bytes 405512 | tf_op jit(solution)/shard_map/ppermute | solution.py:32
  (29 other events, 209.5 us)

commit v3 on v2

--- a/solution.py
+++ b/solution.py
@@ -13,6 +13,7 @@
 F32 = jnp.float32
 NZ, NY, NX, NC = 8, 4, 4, 2
 EXTRA = 16
+ROOM_A, ROOM_B = 16, 12
 VMEM = pl.BlockSpec(memory_space=pltpu.VMEM)
 ANY = pl.BlockSpec(memory_space=pl.ANY)
 
@@ -210,12 +211,9 @@
         write_part(out, numerator[:, cols] / total[:, cols], top[:, cols], total[:, cols])
 
 
-def attend_kernel(n, *refs):
-    queries, refs = refs[:n], refs[n:]
+def first_kernel(query, *refs):
     near, other = refs[:NX], refs[NX : 2 * NX]
-    outs = refs[2 * NX : 2 * NX + n]
-    keys, values, sems = refs[2 * NX + n : 2 * NX + n + 3]
-    work = refs[2 * NX + n + 3 :]
+    out, keys, values, sems, scores, numerator = refs[2 * NX :]
     core = lax.axis_index("c")
 
     def copies(key_blocks, value_blocks):
@@ -234,27 +232,49 @@
         for copy in copies(other, near):
             copy.start()
 
-    arrivals = copies(near, other)
-    for i in range(0, n, 2):
-        q = jnp.concatenate([query[...] for query in queries[i : i + 2]], axis=0)
-        soft_part(q, keys, values, outs[i : i + 2], arrivals if i == 0 else [], *work)
-
-
-def attend(shifts, queries, near, other):
-    n = len(shifts)
-    work = [pltpu.VMEM((4, 512, 256), F32), pltpu.VMEM((HD, 256), F32)]
-    return dict(zip(shifts, pl.pallas_call(
+    soft_part(query[...], keys, values, [out], copies(near, other), scores, numerator)
+
+
+def work_for(n):
+    return [pltpu.VMEM((4, 512, 128 * n), F32), pltpu.VMEM((HD, 128 * n), F32)]
+
+
+def cost_of(n):
+    return pl.CostEstimate(
+        flops=4 * 128 * n * 2048 * HD, bytes_accessed=4 << 20, transcendentals=n * 128 * 2048)
+
+
+def attend_first(query, near, other):
+    held = jax.ShapeDtypeStruct((4, 4, 512, 128), BF)
+    return pl.pallas_call(
+        first_kernel,
+        out_shape=[jax.ShapeDtypeStruct((HD + EXTRA, 128), BF), held, held],
+        in_specs=[VMEM] + [ANY] * 8,
+        out_specs=[VMEM] * 3,
+        scratch_shapes=[pltpu.SemaphoreType.DMA((8,))] + work_for(1),
+        compiler_params=room(ROOM_A),
+        cost_estimate=cost_of(1),
+    )(query, *near, *other)
+
+
+def attend_kernel(n, *refs):
+    keys, values = refs[n : n + 2]
+    outs, work = refs[n + 2 : 2 * n + 2], refs[2 * n + 2 :]
+    q = jnp.concatenate([query[...] for query in refs[:n]], axis=0)
+    soft_part(q, keys, values, outs, [], *work)
+
+
+def attend(queries, keys, values):
+    n = len(queries)
+    return pl.pallas_call(
         functools.partial(attend_kernel, n),
         out_shape=[jax.ShapeDtypeStruct((HD + EXTRA, 128), BF)] * n,
-        in_specs=[VMEM] * n + [ANY] * 8,
+        in_specs=[VMEM] * (n + 2),
         out_specs=[VMEM] * n,
-        scratch_shapes=[pltpu.VMEM((4, 4, 512, 128), BF)] * 2 + [
-            pltpu.SemaphoreType.DMA((8,))] + work,
-        compiler_params=room(28),
-        cost_estimate=pl.CostEstimate(
-            flops=4 * 128 * n * 2048 * HD, bytes_accessed=4 << 20,
-            transcendentals=n * 128 * 2048),
-    )(*[queries[k] for k in shifts], *near, *other)))
+        scratch_shapes=work_for(n),
+        compiler_params=room(ROOM_B),
+        cost_estimate=cost_of(n),
+    )(*queries, keys, values)
 
 
 def combine_kernel(*refs):
@@ -360,20 +380,23 @@
     other = [moved(block, "c", 1) for block in near]
 
 
-    sums = []
-    for step, shifts in enumerate(((4, 3), (5, 2), (6, 1), (7, 0))):
-        parts = attend(shifts, queries, near, other)
+    for step, shifts in enumerate(((4,), (5, 3), (6, 2), (7, 1), (0,))):
+        blocks = [queries[k] for k in shifts]
         if step == 0:
-            sums = [parts[4], parts[3]]
-        elif step < 3:
-            sums = list(merged([parts[k] for k in shifts], sums))
+            ahead, keys, values = attend_first(*blocks, near, other)
         else:
-            sums[0] = merged([parts[7]], sums[:1])[0]
-        sums[0] = moved(sums[0], "z", 1)
-        if step < 3:
-            sums[1] = moved(sums[1], "z", -1)
-    last = parts[0]
-    kept, sent = combine([last] + sums, w_out[0])
+            parts = attend(blocks, keys, values)
+        if step in (1, 2, 3):
+            ahead = merged(parts[:1], [ahead])[0]
+        if step == 1:
+            behind = parts[1]
+        elif step in (2, 3):
+            behind = merged(parts[1:], [behind])[0]
+        if step < 4:
+            ahead = moved(ahead, "z", 1)
+        if step in (1, 2, 3):
+            behind = moved(behind, "z", -1)
+    kept, sent = combine([parts[0], ahead, behind], w_out[0])
     met = moved(sent, "c", 1)
     own, one, two, three = pair_sum(kept, met)
     two = moved(two, "x", -2)

time: 145 us -> 133 us (0.917)
  waiting for transfers between devices: 59.2 us -> 49.6 us
    ppermute x34, waiting for transfers between devices: 56.2 us -> 46.6 us  [moved(): return lax.ppermute(array, axis, [(i, (i + shift) % n) for i in range(n)])]
    pallas_call x4, Pallas kernels: 16.2 us -> 11.1 us  [attend(): pl.pallas_call(functools.partial(attend_kernel, n), out_shape=[jax.ShapeD...]
    pallas_call x0 -> x1, Pallas kernels: none -> 3.77 us  [attend_first(): pl.pallas_call(first_kernel, out_shape=[jax.ShapeDtypeStruct((HD + EXTRA,...]
where the time goes in v3:
time: 133 us
  starting transfers between devices  58 us (44%)
  waiting for transfers between devices  49.6 us (37%)
  Pallas kernels  22.4 us (17%)
  local copies, waits for them, and re-layouts  1.59 us (1%)
    ppermute x34, starting transfers between devices, moved(): return lax.ppermute(array, axis, [(i, (i + shift) % n) for i in range(n)])  50.2 us
    ppermute x34, waiting for transfers between devices, moved(): return lax.ppermute(array, axis, [(i, (i + shift) % n) for i in range(n)])  46.6 us
    pallas_call x4, Pallas kernels, attend(): pl.pallas_call(functools.partial(attend_kernel, n), out_shape=[jax.ShapeD...  11.1 us
    ppermute x6, starting transfers between devices, by_role(): return lax.ppermute(array, ('y', 'x', 'c'), pairs)  7.81 us
    pallas_call x1, Pallas kernels, attend_first(): pl.pallas_call(first_kernel, out_shape=[jax.ShapeDtypeStruct((HD + EXTRA,...  3.77 us
    ppermute x6, waiting for transfers between devices, by_role(): return lax.ppermute(array, ('y', 'x', 'c'), pairs)  3.05 us
    pallas_call x1, Pallas kernels, query_rows(): pl.pallas_call(query_kernel, out_shape=jax.ShapeDtypeStruct((128, HD), BF...  2.83 us
  transfers between devices with their start and end apart: 40, of which 19 were waited for; matrix products, arithmetic and copies ran while one was open for 0% of the time, Pallas kernels for 15%

profile of v3, /device:TPU:1, one launch (start us, length us, event | category | flops | bytes accessed | tf_op | source)
XLA Modules:
  0.0 133.1 jit_solution(14811589022799897217)
XLA Ops:
  1.1 3.3 %collective-permute-start.11 = (bf16[128,2048]{1,0:T(8,128)(2,1)S(1)}, bf16[128,2048]{1,0:T(8,128)(2,1)S(1)}, u32[]{:S(2)}, u32[]{:S(2)}) collective-permute-start(bf16[128,2048]{1,0:T(8,128)(2,1)S(1)} %pad_maximum_fusion.refs_4_), channel_id=1, source_target_pairs={{0,1},{1,0},{2,3},{3,2},{4,5},{5,4},{6,7},{7,6},{8,9},{9,8},{10,11... | collective-permute-start | bytes 1572872 | tf_op jit(solution)/shard_map/ppermute | solution.py:33
  8.9 5.6 %collective-permute-done.10.refs_3_ = bf16[64,2048]{1,0:T(8,128)(2,1)S(1)} collective-permute-done((bf16[64,2048]{1,0:T(8,128)(2,1)}, bf16[64,2048]{1,0:T(8,128)(2,1)S(1)}, u32[]{:S(2)}, u32[]{:S(2)}) %collective-permute-start.10) | collective-permute-done | bytes 262176 | tf_op jit(solution)/shard_map/ppermute | solution.py:33
  14.4 7.3 %collective-permute-done.8.refs_1_ = bf16[64,2048]{1,0:T(8,128)(2,1)S(1)} collective-permute-done((bf16[64,2048]{1,0:T(8,128)(2,1)}, bf16[64,2048]{1,0:T(8,128)(2,1)S(1)}, u32[]{:S(2)}, u32[]{:S(2)}) %collective-permute-start.8) | collective-permute-done | bytes 262176 | tf_op jit(solution)/shard_map/ppermute | solution.py:33
  27.2 2.6 %collective-permute-start.14 = (bf16[512,128]{1,0:T(8,128)(2,1)S(1)}, bf16[512,128]{1,0:T(8,128)(2,1)S(1)}, u32[]{:S(2)}, u32[]{:S(2)}) collective-permute-start(bf16[512,128]{1,0:T(8,128)(2,1)S(1)} %constant_dynamic-update-slice_fusion), channel_id=1, source_target_pairs={{0,4},{1,17},{2,6},{3,19},{4,0},{5,21},{6,2},{7,23},{8,12},{9,25},... | collective-permute-start | bytes 393224 | tf_op jit(solution)/shard_map/ppermute | solution.py:352
  31.3 2.3 %collective-permute-done.14 = bf16[512,128]{1,0:T(8,128)(2,1)S(1)} collective-permute-done((bf16[512,128]{1,0:T(8,128)(2,1)S(1)}, bf16[512,128]{1,0:T(8,128)(2,1)S(1)}, u32[]{:S(2)}, u32[]{:S(2)}) %collective-permute-start.14) | collective-permute-done | bytes 131104 | tf_op jit(solution)/shard_map/ppermute | solution.py:352
  39.2 12.6 %collective-permute-done.1.refs_2_ = bf16[16,2048]{1,0:T(8,128)(2,1)S(1)} collective-permute-done((bf16[16,2048]{1,0:T(8,128)(2,1)S(1)}, bf16[16,2048]{1,0:T(8,128)(2,1)S(1)}, u32[]{:S(2)}, u32[]{:S(2)}) %collective-permute-start.1) | collective-permute-done | bytes 65568 | tf_op jit(solution)/shard_map/ppermute | solution.py:33
  61.9 2.8 %shard_map.92.refs_0_ = bf16[128,512]{1,0:T(8,128)(2,1)} custom-call(bf16[16,2048]{1,0:T(8,128)(2,1)} %get-tuple-element.24.refs_0_, bf16[16,2048]{1,0:T(8,128)(2,1)} %copy-done.9, bf16[16,2048]{1,0:T(8,128)(2,1)} %copy-done.6, bf16[16,2048]{1,0:T(8,128)(2,1)} %copy-done.10, bf16[16,2048]{1,0:T(8,128)(2,1)} %copy-done.7, bf16[16,2048]{1,0:T(8,128)(2,1)} %copy-done.11, ...), custom_call_target="tpu_custom_call" | custom-call | flops 268435456 | bytes 3145728 | tf_op jit(solution)/shard_map/pallas_call | solution.py:125
  64.7 7.0 %collective-permute-start.7 = (bf16[128,512]{1,0:T(8,128)(2,1)}, bf16[128,512]{1,0:T(8,128)(2,1)S(1)}, u32[]{:S(2)}, u32[]{:S(2)}) collective-permute-start(bf16[128,512]{1,0:T(8,128)(2,1)} %shard_map.92.refs_0_), channel_id=1, source_target_pairs={{0,128},{32,160},{64,192},{96,224},{128,0},{160,32},{192,64},{224,... | collective-permute-start | bytes 393224 | tf_op jit(solution)/shard_map/ppermute | solution.py:33
  71.7 3.7 %collective-permute-done.7.query = bf16[128,512]{1,0:T(8,128)(2,1)S(1)} collective-permute-done((bf16[128,512]{1,0:T(8,128)(2,1)}, bf16[128,512]{1,0:T(8,128)(2,1)S(1)}, u32[]{:S(2)}, u32[]{:S(2)}) %collective-permute-start.7) | collective-permute-done | bytes 131104 | tf_op jit(solution)/shard_map/ppermute | solution.py:33
  75.4 4.8 %collective-permute-start.27 = (bf16[128,512]{1,0:T(8,128)(2,1)}, bf16[128,512]{1,0:T(8,128)(2,1)S(1)}, u32[]{:S(2)}, u32[]{:S(2)}) collective-permute-start(bf16[128,512]{1,0:T(8,128)(2,1)} %shard_map.92.refs_0_), channel_id=1, source_target_pairs={{0,160},{32,192},{64,224},{96,0},{128,32},{160,64},{192,96},{224,1... | collective-permute-start | bytes 393224 | tf_op jit(solution)/shard_map/ppermute | solution.py:33
  80.2 3.8 %shard_map.94 = (bf16[528,128]{1,0:T(8,128)(2,1)S(1)}, bf16[4,4,512,128]{3,2,1,0:T(8,128)(2,1)S(1)}, bf16[4,4,512,128]{3,2,1,0:T(8,128)(2,1)S(1)}) custom-call(bf16[128,512]{1,0:T(8,128)(2,1)S(1)} %collective-permute-done.7.query, bf16[4,512,128]{2,1,0:T(8,128)(2,1)S(1)} %pad_maximum_fusion.1.refs_0_, ...), custom_call_target="tpu_custom_call" | custom-call | flops 536870912 | bytes 4194304 | tf_op jit(solution)/shard_map/pallas_call | solution.py:249
  84.0 3.4 %collective-permute-start.29 = (bf16[528,128]{1,0:T(8,128)(2,1)S(1)}, bf16[528,128]{1,0:T(8,128)(2,1)S(1)}, u32[]{:S(2)}, u32[]{:S(2)}) collective-permute-start(bf16[528,128]{1,0:T(8,128)(2,1)S(1)} %get-tuple-element.33), channel_id=1, source_target_pairs={{0,32},{32,64},{64,96},{96,128},{128,160},{160,192},{192,224},{224... | collective-permute-start | bytes 405512 | tf_op jit(solution)/shard_map/ppermute | solution.py:33
  87.4 3.4 %collective-permute-start.25 = (bf16[128,512]{1,0:T(8,128)(2,1)S(1)}, bf16[128,512]{1,0:T(8,128)(2,1)S(1)}, u32[]{:S(2)}, u32[]{:S(2)}) collective-permute-start(bf16[128,512]{1,0:T(8,128)(2,1)S(1)} %copy-done.1), channel_id=1, source_target_pairs={{0,192},{32,224},{64,0},{96,32},{128,64},{160,96},{192,128},{224,1... | collective-permute-start | bytes 393224 | tf_op jit(solution)/shard_map/ppermute | solution.py:33
  90.8 2.8 %shard_map.98 = (bf16[528,128]{1,0:T(8,128)(2,1)S(1)}, bf16[528,128]{1,0:T(8,128)(2,1)S(1)}) custom-call(bf16[128,512]{1,0:T(8,128)(2,1)S(1)} %collective-permute-done.27.refs_0_, bf16[128,512]{1,0:T(8,128)(2,1)S(1)} %collective-permute-done.28.refs_1_, bf16[4,4,512,128]{3,2,1,0:T(8,128)(2,1)S(1)} %get-tuple-element.28.refs_1_.refs_2_, ...), custom_call_target="tpu_custom_call" | custom-call | flops 1073741824 | bytes 4194304 | tf_op jit(solution)/shard_map/pallas_call | solution.py:269
  93.7 3.2 %collective-permute-start.33 = (bf16[528,128]{1,0:T(8,128)(2,1)S(1)}, bf16[528,128]{1,0:T(8,128)(2,1)S(1)}, u32[]{:S(2)}, u32[]{:S(2)}) collective-permute-start(bf16[528,128]{1,0:T(8,128)(2,1)S(1)} %get-tuple-element.36), channel_id=1, source_target_pairs={{0,224},{32,0},{64,32},{96,64},{128,96},{160,128},{192,160},{224,1... | collective-permute-start | bytes 405512 | tf_op jit(solution)/shard_map/ppermute | solution.py:33
  96.9 3.3 %collective-permute-done.29.refs_1_ = bf16[528,128]{1,0:T(8,128)(2,1)S(1)} collective-permute-done((bf16[528,128]{1,0:T(8,128)(2,1)S(1)}, bf16[528,128]{1,0:T(8,128)(2,1)S(1)}, u32[]{:S(2)}, u32[]{:S(2)}) %collective-permute-start.29) | collective-permute-done | bytes 135200 | tf_op jit(solution)/shard_map/ppermute | solution.py:33
  100.4 2.7 %collective-permute-start.23 = (bf16[128,512]{1,0:T(8,128)(2,1)S(1)}, bf16[128,512]{1,0:T(8,128)(2,1)S(1)}, u32[]{:S(2)}, u32[]{:S(2)}) collective-permute-start(bf16[128,512]{1,0:T(8,128)(2,1)S(1)} %copy-done.1), channel_id=1, source_target_pairs={{0,224},{32,0},{64,32},{96,64},{128,96},{160,128},{192,160},{224,1... | collective-permute-start | bytes 393224 | tf_op jit(solution)/shard_map/ppermute | solution.py:33
  103.1 2.9 %shard_map.97 = (bf16[528,128]{1,0:T(8,128)(2,1)S(1)}, bf16[528,128]{1,0:T(8,128)(2,1)S(1)}) custom-call(bf16[128,512]{1,0:T(8,128)(2,1)S(1)} %collective-permute-done.25.refs_0_, bf16[128,512]{1,0:T(8,128)(2,1)S(1)} %collective-permute-done.26.refs_1_, bf16[4,4,512,128]{3,2,1,0:T(8,128)(2,1)S(1)} %get-tuple-element.28.refs_1_.refs_2_, ...), custom_call_target="tpu_custom_call" | custom-call | flops 1073741824 | bytes 4194304 | tf_op jit(solution)/shard_map/pallas_call | solution.py:269
  106.0 2.7 %collective-permute-start.34 = (bf16[528,128]{1,0:T(8,128)(2,1)S(1)}, bf16[528,128]{1,0:T(8,128)(2,1)S(1)}, u32[]{:S(2)}, u32[]{:S(2)}) collective-permute-start(bf16[528,128]{1,0:T(8,128)(2,1)S(1)} %shard_map.102), channel_id=1, source_target_pairs={{0,224},{32,0},{64,32},{96,64},{128,96},{160,128},{192,160},{224,1... | collective-permute-start | bytes 405512 | tf_op jit(solution)/shard_map/ppermute | solution.py:33
  108.9 2.8 %shard_map.96 = (bf16[528,128]{1,0:T(8,128)(2,1)S(1)}, bf16[528,128]{1,0:T(8,128)(2,1)S(1)}) custom-call(bf16[128,512]{1,0:T(8,128)(2,1)S(1)} %collective-permute-done.23.refs_0_, bf16[128,512]{1,0:T(8,128)(2,1)S(1)} %collective-permute-done.24.refs_1_, bf16[4,4,512,128]{3,2,1,0:T(8,128)(2,1)S(1)} %get-tuple-element.28.refs_1_.refs_2_, ...), custom_call_target="tpu_custom_call" | custom-call | flops 1073741824 | bytes 4194304 | tf_op jit(solution)/shard_map/pallas_call | solution.py:269
  111.9 2.7 %collective-permute-start.35 = (bf16[528,128]{1,0:T(8,128)(2,1)S(1)}, bf16[528,128]{1,0:T(8,128)(2,1)S(1)}, u32[]{:S(2)}, u32[]{:S(2)}) collective-permute-start(bf16[528,128]{1,0:T(8,128)(2,1)S(1)} %shard_map.103), channel_id=1, source_target_pairs={{0,224},{32,0},{64,32},{96,64},{128,96},{160,128},{192,160},{224,1... | collective-permute-start | bytes 405512 | tf_op jit(solution)/shard_map/ppermute | solution.py:33
  114.8 2.5 %shard_map.95.refs_0_ = bf16[528,128]{1,0:T(8,128)(2,1)S(1)} custom-call(bf16[128,512]{1,0:T(8,128)(2,1)S(1)} %copy-done.1, bf16[4,4,512,128]{3,2,1,0:T(8,128)(2,1)S(1)} %get-tuple-element.28.refs_1_.refs_2_, bf16[4,4,512,128]{3,2,1,0:T(8,128)(2,1)S(1)} %get-tuple-element.29.refs_2_.refs_3_), custom_call_target="tpu_custom_call" | custom-call | flops 536870912 | bytes 4194304 | tf_op jit(solution)/shard_map/pallas_call | solution.py:269
  117.3 2.5 %collective-permute-done.32.refs_1_ = bf16[528,128]{1,0:T(8,128)(2,1)S(1)} collective-permute-done((bf16[528,128]{1,0:T(8,128)(2,1)S(1)}, bf16[528,128]{1,0:T(8,128)(2,1)S(1)}, u32[]{:S(2)}, u32[]{:S(2)}) %collective-permute-start.32) | collective-permute-done | bytes 135200 | tf_op jit(solution)/shard_map/ppermute | solution.py:33
  120.4 3.7 %collective-permute-start.36 = (bf16[64,2048]{1,0:T(8,128)(2,1)S(1)}, bf16[64,2048]{1,0:T(8,128)(2,1)S(1)}, u32[]{:S(2)}, u32[]{:S(2)}) collective-permute-start(bf16[64,2048]{1,0:T(8,128)(2,1)S(1)} %get-tuple-element.38), channel_id=1, source_target_pairs={{0,1},{1,0},{2,3},{3,2},{4,5},{5,4},{6,7},{7,6},{8,9},{9,8},{10,11... | collective-permute-start | bytes 786440 | tf_op jit(solution)/shard_map/ppermute | solution.py:33
  (102 shorter events, 38.3 us)
Async XLA Ops:
  1.1 20.7 %collective-permute-start.11 = (bf16[128,2048]{1,0:T(8,128)(2,1)S(1)}, bf16[128,2048]{1,0:T(8,128)(2,1)S(1)}, u32[]{:S(2)}, u32[]{:S(2)}) collective-permute-start(bf16[128,2048]{1,0:T(8,128)(2,1)S(1)} %pad_maximum_fusion.refs_4_), channel_id=1, source_target_pairs={{0,1},{1,0},{2,3},{3,2},{4,5},{5,4},{6,7},{7,6},{8,9},{9,8},{10,11... | collective-permute-start | bytes 1572872 | tf_op jit(solution)/shard_map/ppermute | solution.py:33
  6.3 8.1 %collective-permute-start.10 = (bf16[64,2048]{1,0:T(8,128)(2,1)}, bf16[64,2048]{1,0:T(8,128)(2,1)S(1)}, u32[]{:S(2)}, u32[]{:S(2)}) collective-permute-start(bf16[64,2048]{1,0:T(8,128)(2,1)} %get-tuple-element.25.refs_0_), channel_id=1, source_target_pairs={{0,6},{2,0},{4,2},{6,4},{1,7},{3,1},{5,3},{7,5},{8,14},{10,8},{12,... | collective-permute-start | bytes 786440 | tf_op jit(solution)/shard_map/ppermute | solution.py:33
  7.1 14.6 %collective-permute-start.8 = (bf16[64,2048]{1,0:T(8,128)(2,1)}, bf16[64,2048]{1,0:T(8,128)(2,1)S(1)}, u32[]{:S(2)}, u32[]{:S(2)}) collective-permute-start(bf16[64,2048]{1,0:T(8,128)(2,1)} %get-tuple-element.25.refs_0_), channel_id=1, source_target_pairs={{0,2},{2,4},{4,6},{6,0},{1,3},{3,5},{5,7},{7,1},{8,10},{10,12},{12... | collective-permute-start | bytes 786440 | tf_op jit(solution)/shard_map/ppermute | solution.py:33
  7.8 13.9 %collective-permute-start.9 = (bf16[64,2048]{1,0:T(8,128)(2,1)}, bf16[64,2048]{1,0:T(8,128)(2,1)S(1)}, u32[]{:S(2)}, u32[]{:S(2)}) collective-permute-start(bf16[64,2048]{1,0:T(8,128)(2,1)} %get-tuple-element.25.refs_0_), channel_id=1, source_target_pairs={{0,4},{2,6},{4,0},{6,2},{1,5},{3,7},{5,1},{7,3},{8,12},{10,14},{12... | collective-permute-start | bytes 786440 | tf_op jit(solution)/shard_map/ppermute | solution.py:33
  27.2 6.4 %collective-permute-start.14 = (bf16[512,128]{1,0:T(8,128)(2,1)S(1)}, bf16[512,128]{1,0:T(8,128)(2,1)S(1)}, u32[]{:S(2)}, u32[]{:S(2)}) collective-permute-start(bf16[512,128]{1,0:T(8,128)(2,1)S(1)} %constant_dynamic-update-slice_fusion), channel_id=1, source_target_pairs={{0,4},{1,17},{2,6},{3,19},{4,0},{5,21},{6,2},{7,23},{8,12},{9,25},... | collective-permute-start | bytes 393224 | tf_op jit(solution)/shard_map/ppermute | solution.py:352
  34.0 19.7 %collective-permute-start.16 = (bf16[4,512,128]{2,1,0:T(8,128)(2,1)S(1)}, bf16[4,512,128]{2,1,0:T(8,128)(2,1)S(1)}, u32[]{:S(2)}, u32[]{:S(2)}) collective-permute-start(bf16[4,512,128]{2,1,0:T(8,128)(2,1)S(1)} %pad_maximum_fusion.1.refs_0_), channel_id=1, source_target_pairs={{0,8},{1,3},{2,10},{3,5},{4,12},{5,7},{6,14},{7,1},{8,16},{9,11},{... | collective-permute-start | bytes 1572872 | tf_op jit(solution)/shard_map/ppermute | solution.py:352
  34.1 19.6 %collective-permute-start.17 = (bf16[4,512,128]{2,1,0:T(8,128)(2,1)S(1)}, bf16[4,512,128]{2,1,0:T(8,128)(2,1)S(1)}, u32[]{:S(2)}, u32[]{:S(2)}) collective-permute-start(bf16[4,512,128]{2,1,0:T(8,128)(2,1)S(1)} %pad_maximum_fusion.1.refs_0_), channel_id=1, source_target_pairs={{0,16},{1,5},{2,18},{3,7},{4,20},{5,1},{6,22},{7,3},{8,24},{9,13},... | collective-permute-start | bytes 1572872 | tf_op jit(solution)/shard_map/ppermute | solution.py:352
  35.3 18.9 %collective-permute-start.18 = (bf16[4,512,128]{2,1,0:T(8,128)(2,1)S(1)}, bf16[4,512,128]{2,1,0:T(8,128)(2,1)S(1)}, u32[]{:S(2)}, u32[]{:S(2)}) collective-permute-start(bf16[4,512,128]{2,1,0:T(8,128)(2,1)S(1)} %pad_maximum_fusion.1.refs_0_), channel_id=1, source_target_pairs={{0,24},{1,7},{2,26},{3,1},{4,28},{5,3},{6,30},{7,5},{8,0},{9,15},{... | collective-permute-start | bytes 1572872 | tf_op jit(solution)/shard_map/ppermute | solution.py:352
  36.8 15.0 %collective-permute-start.1 = (bf16[16,2048]{1,0:T(8,128)(2,1)S(1)}, bf16[16,2048]{1,0:T(8,128)(2,1)S(1)}, u32[]{:S(2)}, u32[]{:S(2)}) collective-permute-start(bf16[16,2048]{1,0:T(8,128)(2,1)S(1)} %copy-done.5), channel_id=1, source_target_pairs={{0,2},{2,4},{4,6},{6,0},{1,3},{3,5},{5,7},{7,1},{8,10},{10,12},{12... | collective-permute-start | bytes 196616 | tf_op jit(solution)/shard_map/ppermute | solution.py:33
  37.4 14.4 %collective-permute-start.3 = (bf16[16,2048]{1,0:T(8,128)(2,1)S(1)}, bf16[16,2048]{1,0:T(8,128)(2,1)S(1)}, u32[]{:S(2)}, u32[]{:S(2)}) collective-permute-start(bf16[16,2048]{1,0:T(8,128)(2,1)S(1)} %copy-done.5), channel_id=1, source_target_pairs={{0,4},{2,6},{4,0},{6,2},{1,5},{3,7},{5,1},{7,3},{8,12},{10,14},{12... | collective-permute-start | bytes 196616 | tf_op jit(solution)/shard_map/ppermute | solution.py:33
  51.8 28.4 %collective-permute-start.19 = (bf16[4,512,128]{2,1,0:T(8,128)(2,1)S(1)}, bf16[4,512,128]{2,1,0:T(8,128)(2,1)S(1)}, u32[]{:S(2)}, u32[]{:S(2)}) collective-permute-start(bf16[4,512,128]{2,1,0:T(8,128)(2,1)S(1)} %pad_maximum_fusion.1.refs_0_), channel_id=1, source_target_pairs={{0,1},{1,0},{2,3},{3,2},{4,5},{5,4},{6,7},{7,6},{8,9},{9,8},{10,11... | collective-permute-start | bytes 1572872 | tf_op jit(solution)/shard_map/ppermute | solution.py:33
  53.7 26.5 %collective-permute-start.20 = (bf16[4,512,128]{2,1,0:T(8,128)(2,1)S(1)}, bf16[4,512,128]{2,1,0:T(8,128)(2,1)S(1)}, u32[]{:S(2)}, u32[]{:S(2)}) collective-permute-start(bf16[4,512,128]{2,1,0:T(8,128)(2,1)S(1)} %collective-permute-done.16.refs_1_), channel_id=1, source_target_pairs={{0,1},{1,0},{2,3},{3,2},{4,5},{5,4},{6,7},{7,6},{8,9},{9,8},{10,11... | collective-permute-start | bytes 1572872 | tf_op jit(solution)/shard_map/ppermute | solution.py:33
  53.7 26.5 %collective-permute-start.21 = (bf16[4,512,128]{2,1,0:T(8,128)(2,1)S(1)}, bf16[4,512,128]{2,1,0:T(8,128)(2,1)S(1)}, u32[]{:S(2)}, u32[]{:S(2)}) collective-permute-start(bf16[4,512,128]{2,1,0:T(8,128)(2,1)S(1)} %collective-permute-done.17.refs_2_), channel_id=1, source_target_pairs={{0,1},{1,0},{2,3},{3,2},{4,5},{5,4},{6,7},{7,6},{8,9},{9,8},{10,11... | collective-permute-start | bytes 1572872 | tf_op jit(solution)/shard_map/ppermute | solution.py:33
  54.2 26.0 %collective-permute-start.22 = (bf16[4,512,128]{2,1,0:T(8,128)(2,1)S(1)}, bf16[4,512,128]{2,1,0:T(8,128)(2,1)}, u32[]{:S(2)}, u32[]{:S(2)}) collective-permute-start(bf16[4,512,128]{2,1,0:T(8,128)(2,1)S(1)} %collective-permute-done.18.refs_3_), channel_id=1, source_target_pairs={{0,1},{1,0},{2,3},{3,2},{4,5},{5,4},{6,7},{7,6},{8,9},{9,8},{10,11... | collective-permute-start | bytes 1572872 | tf_op jit(solution)/shard_map/ppermute | solution.py:33
  64.7 10.7 %collective-permute-start.7 = (bf16[128,512]{1,0:T(8,128)(2,1)}, bf16[128,512]{1,0:T(8,128)(2,1)S(1)}, u32[]{:S(2)}, u32[]{:S(2)}) collective-permute-start(bf16[128,512]{1,0:T(8,128)(2,1)} %shard_map.92.refs_0_), channel_id=1, source_target_pairs={{0,128},{32,160},{64,192},{96,224},{128,0},{160,32},{192,64},{224,... | collective-permute-start | bytes 393224 | tf_op jit(solution)/shard_map/ppermute | solution.py:33
  75.4 15.4 %collective-permute-start.27 = (bf16[128,512]{1,0:T(8,128)(2,1)}, bf16[128,512]{1,0:T(8,128)(2,1)S(1)}, u32[]{:S(2)}, u32[]{:S(2)}) collective-permute-start(bf16[128,512]{1,0:T(8,128)(2,1)} %shard_map.92.refs_0_), channel_id=1, source_target_pairs={{0,160},{32,192},{64,224},{96,0},{128,32},{160,64},{192,96},{224,1... | collective-permute-start | bytes 393224 | tf_op jit(solution)/shard_map/ppermute | solution.py:33
  80.2 10.6 %collective-permute-start.28 = (bf16[128,512]{1,0:T(8,128)(2,1)}, bf16[128,512]{1,0:T(8,128)(2,1)S(1)}, u32[]{:S(2)}, u32[]{:S(2)}) collective-permute-start(bf16[128,512]{1,0:T(8,128)(2,1)} %shard_map.92.refs_0_), channel_id=1, source_target_pairs={{0,96},{32,128},{64,160},{96,192},{128,224},{160,0},{192,32},{224,... | collective-permute-start | bytes 393224 | tf_op jit(solution)/shard_map/ppermute | solution.py:33
  84.0 16.2 %collective-permute-start.29 = (bf16[528,128]{1,0:T(8,128)(2,1)S(1)}, bf16[528,128]{1,0:T(8,128)(2,1)S(1)}, u32[]{:S(2)}, u32[]{:S(2)}) collective-permute-start(bf16[528,128]{1,0:T(8,128)(2,1)S(1)} %get-tuple-element.33), channel_id=1, source_target_pairs={{0,32},{32,64},{64,96},{96,128},{128,160},{160,192},{192,224},{224... | collective-permute-start | bytes 405512 | tf_op jit(solution)/shard_map/ppermute | solution.py:33
  87.4 15.6 %collective-permute-start.25 = (bf16[128,512]{1,0:T(8,128)(2,1)S(1)}, bf16[128,512]{1,0:T(8,128)(2,1)S(1)}, u32[]{:S(2)}, u32[]{:S(2)}) collective-permute-start(bf16[128,512]{1,0:T(8,128)(2,1)S(1)} %copy-done.1), channel_id=1, source_target_pairs={{0,192},{32,224},{64,0},{96,32},{128,64},{160,96},{192,128},{224,1... | collective-permute-start | bytes 393224 | tf_op jit(solution)/shard_map/ppermute | solution.py:33
  90.8 12.2 %collective-permute-start.26 = (bf16[128,512]{1,0:T(8,128)(2,1)S(1)}, bf16[128,512]{1,0:T(8,128)(2,1)S(1)}, u32[]{:S(2)}, u32[]{:S(2)}) collective-permute-start(bf16[128,512]{1,0:T(8,128)(2,1)S(1)} %copy-done.1), channel_id=1, source_target_pairs={{0,64},{32,96},{64,128},{96,160},{128,192},{160,224},{192,0},{224,... | collective-permute-start | bytes 393224 | tf_op jit(solution)/shard_map/ppermute | solution.py:33
  93.7 12.2 %collective-permute-start.33 = (bf16[528,128]{1,0:T(8,128)(2,1)S(1)}, bf16[528,128]{1,0:T(8,128)(2,1)S(1)}, u32[]{:S(2)}, u32[]{:S(2)}) collective-permute-start(bf16[528,128]{1,0:T(8,128)(2,1)S(1)} %get-tuple-element.36), channel_id=1, source_target_pairs={{0,224},{32,0},{64,32},{96,64},{128,96},{160,128},{192,160},{224,1... | collective-permute-start | bytes 405512 | tf_op jit(solution)/shard_map/ppermute | solution.py:33
  100.3 8.4 %collective-permute-start.30 = (bf16[528,128]{1,0:T(8,128)(2,1)S(1)}, bf16[528,128]{1,0:T(8,128)(2,1)S(1)}, u32[]{:S(2)}, u32[]{:S(2)}) collective-permute-start(bf16[528,128]{1,0:T(8,128)(2,1)S(1)} %shard_map.99), channel_id=1, source_target_pairs={{0,32},{32,64},{64,96},{96,128},{128,160},{160,192},{192,224},{224... | collective-permute-start | bytes 405512 | tf_op jit(solution)/shard_map/ppermute | solution.py:33
  100.4 8.5 %collective-permute-start.23 = (bf16[128,512]{1,0:T(8,128)(2,1)S(1)}, bf16[128,512]{1,0:T(8,128)(2,1)S(1)}, u32[]{:S(2)}, u32[]{:S(2)}) collective-permute-start(bf16[128,512]{1,0:T(8,128)(2,1)S(1)} %copy-done.1), channel_id=1, source_target_pairs={{0,224},{32,0},{64,32},{96,64},{128,96},{160,128},{192,160},{224,1... | collective-permute-start | bytes 393224 | tf_op jit(solution)/shard_map/ppermute | solution.py:33
  103.1 5.9 %collective-permute-start.24 = (bf16[128,512]{1,0:T(8,128)(2,1)S(1)}, bf16[128,512]{1,0:T(8,128)(2,1)S(1)}, u32[]{:S(2)}, u32[]{:S(2)}) collective-permute-start(bf16[128,512]{1,0:T(8,128)(2,1)S(1)} %copy-done.1), channel_id=1, source_target_pairs={{0,32},{32,64},{64,96},{96,128},{128,160},{160,192},{192,224},{224... | collective-permute-start | bytes 393224 | tf_op jit(solution)/shard_map/ppermute | solution.py:33
  (29 other events, 167.7 us)

commit v4 on v3

--- a/solution.py
+++ b/solution.py
@@ -180,7 +180,7 @@
     )(*own, *met)
 
 
-def soft_part(q, keys, values, outs, arrivals, scores, numerator):
+def soft_part(q, keys, values, outs, arrivals, scores, numerator, rounded):
     width = q.shape[0]
     for arrival in arrivals[:NY]:
         arrival.wait()
@@ -194,18 +194,25 @@
     top = lax.fori_loop(0, NY, score_step, jnp.full((1, width), -jnp.inf, F32))
     for arrival in arrivals[NY:]:
         arrival.wait()
-    numerator[...] = jnp.zeros_like(numerator)
 
     def weight_step(m, total):
         weights = jnp.exp(scores[m] - top)
+        rounded[m] = weights.astype(BF)
+        return total + jnp.sum(weights, axis=0, keepdims=True)
+
+    total = lax.fori_loop(0, NY, weight_step, jnp.zeros((1, width), F32))
+
+    def value_step(pair, carry):
         block = jnp.concatenate([
-            jnp.concatenate(
-                [values[k, m, pl.ds(row, 128), :] for row in (256, 384, 0, 128)], axis=1)
-            for k in range(NX)], axis=0)
-        numerator[...] += jnp.dot(block, weights.astype(BF), preferred_element_type=F32)
-        return total + jnp.sum(weights, axis=0, keepdims=True)
-
-    total = lax.fori_loop(0, NY, weight_step, jnp.zeros((1, width), F32))
+            jnp.concatenate([
+                values[2 * pair + k, m, pl.ds(row, 128), :]
+                for m in range(NY) for row in (256, 384, 0, 128)], axis=1)
+            for k in range(2)], axis=0)
+        numerator[pl.ds(pl.multiple_of(pair * 256, 256), 256), :] = jnp.dot(
+            block, rounded[...].reshape(2048, width), preferred_element_type=F32)
+        return carry
+
+    lax.fori_loop(0, 2, value_step, 0)
     for side, out in enumerate(outs):
         cols = slice(side * 128, side * 128 + 128)
         write_part(out, numerator[:, cols] / total[:, cols], top[:, cols], total[:, cols])
@@ -213,7 +220,7 @@
 
 def first_kernel(query, *refs):
     near, other = refs[:NX], refs[NX : 2 * NX]
-    out, keys, values, sems, scores, numerator = refs[2 * NX :]
+    out, keys, values, sems, *work = refs[2 * NX :]
     core = lax.axis_index("c")
 
     def copies(key_blocks, value_blocks):
@@ -232,11 +239,13 @@
         for copy in copies(other, near):
             copy.start()
 
-    soft_part(query[...], keys, values, [out], copies(near, other), scores, numerator)
+    soft_part(query[...], keys, values, [out], copies(near, other), *work)
 
 
 def work_for(n):
-    return [pltpu.VMEM((4, 512, 128 * n), F32), pltpu.VMEM((HD, 128 * n), F32)]
+    return [
+        pltpu.VMEM((4, 512, 128 * n), F32), pltpu.VMEM((HD, 128 * n), F32),
+        pltpu.VMEM((4, 512, 128 * n), BF)]
 
 
 def cost_of(n):

time: 133 us -> 133 us (level)
  transfers between devices with their start and end apart: 40 -> 40, of which waited for: 19 -> 19; matrix products, arithmetic and copies ran while one was open for 0% -> 0% of each run, Pallas kernels for 15% -> 14%
where the time goes in v4:
time: 133 us
  starting transfers between devices  58.4 us (44%)
  waiting for transfers between devices  50 us (38%)
  Pallas kernels  21.6 us (16%)
  local copies, waits for them, and re-layouts  1.59 us (1%)
    ppermute x34, starting transfers between devices, moved(): return lax.ppermute(array, axis, [(i, (i + shift) % n) for i in range(n)])  50.6 us
    ppermute x34, waiting for transfers between devices, moved(): return lax.ppermute(array, axis, [(i, (i + shift) % n) for i in range(n)])  47 us
    pallas_call x4, Pallas kernels, attend(): pl.pallas_call(functools.partial(attend_kernel, n), out_shape=[jax.ShapeD...  10.4 us
    ppermute x6, starting transfers between devices, by_role(): return lax.ppermute(array, ('y', 'x', 'c'), pairs)  7.81 us
    pallas_call x1, Pallas kernels, attend_first(): pl.pallas_call(first_kernel, out_shape=[jax.ShapeDtypeStruct((HD + EXTRA,...  3.69 us
    ppermute x6, waiting for transfers between devices, by_role(): return lax.ppermute(array, ('y', 'x', 'c'), pairs)  3.05 us
    pallas_call x1, Pallas kernels, query_rows(): pl.pallas_call(query_kernel, out_shape=jax.ShapeDtypeStruct((128, HD), BF...  2.83 us
  transfers between devices with their start and end apart: 40, of which 19 were waited for; matrix products, arithmetic and copies ran while one was open for 0% of the time, Pallas kernels for 14%

profile of v4, /device:TPU:1, one launch (start us, length us, event | category | flops | bytes accessed | tf_op | source)
XLA Modules:
  0.0 133.1 jit_solution(11834890780982065458)
XLA Ops:
  1.1 3.3 %collective-permute-start.11 = (bf16[128,2048]{1,0:T(8,128)(2,1)S(1)}, bf16[128,2048]{1,0:T(8,128)(2,1)S(1)}, u32[]{:S(2)}, u32[]{:S(2)}) collective-permute-start(bf16[128,2048]{1,0:T(8,128)(2,1)S(1)} %pad_maximum_fusion.refs_4_), channel_id=1, source_target_pairs={{0,1},{1,0},{2,3},{3,2},{4,5},{5,4},{6,7},{7,6},{8,9},{9,8},{10,11... | collective-permute-start | bytes 1572872 | tf_op jit(solution)/shard_map/ppermute | solution.py:33
  8.9 5.6 %collective-permute-done.10.refs_3_ = bf16[64,2048]{1,0:T(8,128)(2,1)S(1)} collective-permute-done((bf16[64,2048]{1,0:T(8,128)(2,1)}, bf16[64,2048]{1,0:T(8,128)(2,1)S(1)}, u32[]{:S(2)}, u32[]{:S(2)}) %collective-permute-start.10) | collective-permute-done | bytes 262176 | tf_op jit(solution)/shard_map/ppermute | solution.py:33
  14.4 7.3 %collective-permute-done.8.refs_1_ = bf16[64,2048]{1,0:T(8,128)(2,1)S(1)} collective-permute-done((bf16[64,2048]{1,0:T(8,128)(2,1)}, bf16[64,2048]{1,0:T(8,128)(2,1)S(1)}, u32[]{:S(2)}, u32[]{:S(2)}) %collective-permute-start.8) | collective-permute-done | bytes 262176 | tf_op jit(solution)/shard_map/ppermute | solution.py:33
  27.2 2.6 %collective-permute-start.14 = (bf16[512,128]{1,0:T(8,128)(2,1)S(1)}, bf16[512,128]{1,0:T(8,128)(2,1)S(1)}, u32[]{:S(2)}, u32[]{:S(2)}) collective-permute-start(bf16[512,128]{1,0:T(8,128)(2,1)S(1)} %constant_dynamic-update-slice_fusion), channel_id=1, source_target_pairs={{0,4},{1,17},{2,6},{3,19},{4,0},{5,21},{6,2},{7,23},{8,12},{9,25},... | collective-permute-start | bytes 393224 | tf_op jit(solution)/shard_map/ppermute | solution.py:361
  31.3 2.3 %collective-permute-done.14 = bf16[512,128]{1,0:T(8,128)(2,1)S(1)} collective-permute-done((bf16[512,128]{1,0:T(8,128)(2,1)S(1)}, bf16[512,128]{1,0:T(8,128)(2,1)S(1)}, u32[]{:S(2)}, u32[]{:S(2)}) %collective-permute-start.14) | collective-permute-done | bytes 131104 | tf_op jit(solution)/shard_map/ppermute | solution.py:361
  39.2 12.6 %collective-permute-done.1.refs_2_ = bf16[16,2048]{1,0:T(8,128)(2,1)S(1)} collective-permute-done((bf16[16,2048]{1,0:T(8,128)(2,1)S(1)}, bf16[16,2048]{1,0:T(8,128)(2,1)S(1)}, u32[]{:S(2)}, u32[]{:S(2)}) %collective-permute-start.1) | collective-permute-done | bytes 65568 | tf_op jit(solution)/shard_map/ppermute | solution.py:33
  61.9 2.8 %shard_map.92.refs_0_ = bf16[128,512]{1,0:T(8,128)(2,1)} custom-call(bf16[16,2048]{1,0:T(8,128)(2,1)} %get-tuple-element.24.refs_0_, bf16[16,2048]{1,0:T(8,128)(2,1)} %copy-done.9, bf16[16,2048]{1,0:T(8,128)(2,1)} %copy-done.6, bf16[16,2048]{1,0:T(8,128)(2,1)} %copy-done.10, bf16[16,2048]{1,0:T(8,128)(2,1)} %copy-done.7, bf16[16,2048]{1,0:T(8,128)(2,1)} %copy-done.11, ...), custom_call_target="tpu_custom_call" | custom-call | flops 268435456 | bytes 3145728 | tf_op jit(solution)/shard_map/pallas_call | solution.py:125
  64.7 7.0 %collective-permute-start.7 = (bf16[128,512]{1,0:T(8,128)(2,1)}, bf16[128,512]{1,0:T(8,128)(2,1)S(1)}, u32[]{:S(2)}, u32[]{:S(2)}) collective-permute-start(bf16[128,512]{1,0:T(8,128)(2,1)} %shard_map.92.refs_0_), channel_id=1, source_target_pairs={{0,128},{32,160},{64,192},{96,224},{128,0},{160,32},{192,64},{224,... | collective-permute-start | bytes 393224 | tf_op jit(solution)/shard_map/ppermute | solution.py:33
  71.7 3.7 %collective-permute-done.7.query = bf16[128,512]{1,0:T(8,128)(2,1)S(1)} collective-permute-done((bf16[128,512]{1,0:T(8,128)(2,1)}, bf16[128,512]{1,0:T(8,128)(2,1)S(1)}, u32[]{:S(2)}, u32[]{:S(2)}) %collective-permute-start.7) | collective-permute-done | bytes 131104 | tf_op jit(solution)/shard_map/ppermute | solution.py:33
  75.4 4.8 %collective-permute-start.27 = (bf16[128,512]{1,0:T(8,128)(2,1)}, bf16[128,512]{1,0:T(8,128)(2,1)S(1)}, u32[]{:S(2)}, u32[]{:S(2)}) collective-permute-start(bf16[128,512]{1,0:T(8,128)(2,1)} %shard_map.92.refs_0_), channel_id=1, source_target_pairs={{0,160},{32,192},{64,224},{96,0},{128,32},{160,64},{192,96},{224,1... | collective-permute-start | bytes 393224 | tf_op jit(solution)/shard_map/ppermute | solution.py:33
  80.2 3.7 %shard_map.94 = (bf16[528,128]{1,0:T(8,128)(2,1)S(1)}, bf16[4,4,512,128]{3,2,1,0:T(8,128)(2,1)S(1)}, bf16[4,4,512,128]{3,2,1,0:T(8,128)(2,1)S(1)}) custom-call(bf16[128,512]{1,0:T(8,128)(2,1)S(1)} %collective-permute-done.7.query, bf16[4,512,128]{2,1,0:T(8,128)(2,1)S(1)} %pad_maximum_fusion.1.refs_0_, ...), custom_call_target="tpu_custom_call" | custom-call | flops 536870912 | bytes 4194304 | tf_op jit(solution)/shard_map/pallas_call | solution.py:258
  83.9 3.4 %collective-permute-start.29 = (bf16[528,128]{1,0:T(8,128)(2,1)S(1)}, bf16[528,128]{1,0:T(8,128)(2,1)S(1)}, u32[]{:S(2)}, u32[]{:S(2)}) collective-permute-start(bf16[528,128]{1,0:T(8,128)(2,1)S(1)} %get-tuple-element.33), channel_id=1, source_target_pairs={{0,32},{32,64},{64,96},{96,128},{128,160},{160,192},{192,224},{224... | collective-permute-start | bytes 405512 | tf_op jit(solution)/shard_map/ppermute | solution.py:33
  87.4 3.4 %collective-permute-start.25 = (bf16[128,512]{1,0:T(8,128)(2,1)S(1)}, bf16[128,512]{1,0:T(8,128)(2,1)S(1)}, u32[]{:S(2)}, u32[]{:S(2)}) collective-permute-start(bf16[128,512]{1,0:T(8,128)(2,1)S(1)} %copy-done.1), channel_id=1, source_target_pairs={{0,192},{32,224},{64,0},{96,32},{128,64},{160,96},{192,128},{224,1... | collective-permute-start | bytes 393224 | tf_op jit(solution)/shard_map/ppermute | solution.py:33
  90.8 2.6 %shard_map.98 = (bf16[528,128]{1,0:T(8,128)(2,1)S(1)}, bf16[528,128]{1,0:T(8,128)(2,1)S(1)}) custom-call(bf16[128,512]{1,0:T(8,128)(2,1)S(1)} %collective-permute-done.27.refs_0_, bf16[128,512]{1,0:T(8,128)(2,1)S(1)} %collective-permute-done.28.refs_1_, bf16[4,4,512,128]{3,2,1,0:T(8,128)(2,1)S(1)} %get-tuple-element.28.refs_1_.refs_2_, ...), custom_call_target="tpu_custom_call" | custom-call | flops 1073741824 | bytes 4194304 | tf_op jit(solution)/shard_map/pallas_call | solution.py:278
  93.4 3.4 %collective-permute-start.33 = (bf16[528,128]{1,0:T(8,128)(2,1)S(1)}, bf16[528,128]{1,0:T(8,128)(2,1)S(1)}, u32[]{:S(2)}, u32[]{:S(2)}) collective-permute-start(bf16[528,128]{1,0:T(8,128)(2,1)S(1)} %get-tuple-element.36), channel_id=1, source_target_pairs={{0,224},{32,0},{64,32},{96,64},{128,96},{160,128},{192,160},{224,1... | collective-permute-start | bytes 405512 | tf_op jit(solution)/shard_map/ppermute | solution.py:33
  96.8 3.6 %collective-permute-done.29.refs_1_ = bf16[528,128]{1,0:T(8,128)(2,1)S(1)} collective-permute-done((bf16[528,128]{1,0:T(8,128)(2,1)S(1)}, bf16[528,128]{1,0:T(8,128)(2,1)S(1)}, u32[]{:S(2)}, u32[]{:S(2)}) %collective-permute-start.29) | collective-permute-done | bytes 135200 | tf_op jit(solution)/shard_map/ppermute | solution.py:33
  100.6 2.7 %collective-permute-start.23 = (bf16[128,512]{1,0:T(8,128)(2,1)S(1)}, bf16[128,512]{1,0:T(8,128)(2,1)S(1)}, u32[]{:S(2)}, u32[]{:S(2)}) collective-permute-start(bf16[128,512]{1,0:T(8,128)(2,1)S(1)} %copy-done.1), channel_id=1, source_target_pairs={{0,224},{32,0},{64,32},{96,64},{128,96},{160,128},{192,160},{224,1... | collective-permute-start | bytes 393224 | tf_op jit(solution)/shard_map/ppermute | solution.py:33
  103.2 2.7 %shard_map.97 = (bf16[528,128]{1,0:T(8,128)(2,1)S(1)}, bf16[528,128]{1,0:T(8,128)(2,1)S(1)}) custom-call(bf16[128,512]{1,0:T(8,128)(2,1)S(1)} %collective-permute-done.25.refs_0_, bf16[128,512]{1,0:T(8,128)(2,1)S(1)} %collective-permute-done.26.refs_1_, bf16[4,4,512,128]{3,2,1,0:T(8,128)(2,1)S(1)} %get-tuple-element.28.refs_1_.refs_2_, ...), custom_call_target="tpu_custom_call" | custom-call | flops 1073741824 | bytes 4194304 | tf_op jit(solution)/shard_map/pallas_call | solution.py:278
  106.0 2.7 %collective-permute-start.34 = (bf16[528,128]{1,0:T(8,128)(2,1)S(1)}, bf16[528,128]{1,0:T(8,128)(2,1)S(1)}, u32[]{:S(2)}, u32[]{:S(2)}) collective-permute-start(bf16[528,128]{1,0:T(8,128)(2,1)S(1)} %shard_map.102), channel_id=1, source_target_pairs={{0,224},{32,0},{64,32},{96,64},{128,96},{160,128},{192,160},{224,1... | collective-permute-start | bytes 405512 | tf_op jit(solution)/shard_map/ppermute | solution.py:33
  109.0 2.6 %shard_map.96 = (bf16[528,128]{1,0:T(8,128)(2,1)S(1)}, bf16[528,128]{1,0:T(8,128)(2,1)S(1)}) custom-call(bf16[128,512]{1,0:T(8,128)(2,1)S(1)} %collective-permute-done.23.refs_0_, bf16[128,512]{1,0:T(8,128)(2,1)S(1)} %collective-permute-done.24.refs_1_, bf16[4,4,512,128]{3,2,1,0:T(8,128)(2,1)S(1)} %get-tuple-element.28.refs_1_.refs_2_, ...), custom_call_target="tpu_custom_call" | custom-call | flops 1073741824 | bytes 4194304 | tf_op jit(solution)/shard_map/pallas_call | solution.py:278
  111.7 2.8 %collective-permute-start.35 = (bf16[528,128]{1,0:T(8,128)(2,1)S(1)}, bf16[528,128]{1,0:T(8,128)(2,1)S(1)}, u32[]{:S(2)}, u32[]{:S(2)}) collective-permute-start(bf16[528,128]{1,0:T(8,128)(2,1)S(1)} %shard_map.103), channel_id=1, source_target_pairs={{0,224},{32,0},{64,32},{96,64},{128,96},{160,128},{192,160},{224,1... | collective-permute-start | bytes 405512 | tf_op jit(solution)/shard_map/ppermute | solution.py:33
  114.7 2.4 %shard_map.95.refs_0_ = bf16[528,128]{1,0:T(8,128)(2,1)S(1)} custom-call(bf16[128,512]{1,0:T(8,128)(2,1)S(1)} %copy-done.1, bf16[4,4,512,128]{3,2,1,0:T(8,128)(2,1)S(1)} %get-tuple-element.28.refs_1_.refs_2_, bf16[4,4,512,128]{3,2,1,0:T(8,128)(2,1)S(1)} %get-tuple-element.29.refs_2_.refs_3_), custom_call_target="tpu_custom_call" | custom-call | flops 536870912 | bytes 4194304 | tf_op jit(solution)/shard_map/pallas_call | solution.py:278
  117.2 2.6 %collective-permute-done.32.refs_1_ = bf16[528,128]{1,0:T(8,128)(2,1)S(1)} collective-permute-done((bf16[528,128]{1,0:T(8,128)(2,1)S(1)}, bf16[528,128]{1,0:T(8,128)(2,1)S(1)}, u32[]{:S(2)}, u32[]{:S(2)}) %collective-permute-start.32) | collective-permute-done | bytes 135200 | tf_op jit(solution)/shard_map/ppermute | solution.py:33
  120.3 3.8 %collective-permute-start.36 = (bf16[64,2048]{1,0:T(8,128)(2,1)S(1)}, bf16[64,2048]{1,0:T(8,128)(2,1)S(1)}, u32[]{:S(2)}, u32[]{:S(2)}) collective-permute-start(bf16[64,2048]{1,0:T(8,128)(2,1)S(1)} %get-tuple-element.38), channel_id=1, source_target_pairs={{0,1},{1,0},{2,3},{3,2},{4,5},{5,4},{6,7},{7,6},{8,9},{9,8},{10,11... | collective-permute-start | bytes 786440 | tf_op jit(solution)/shard_map/ppermute | solution.py:33
  (102 shorter events, 38.3 us)
Async XLA Ops:
  1.1 20.7 %collective-permute-start.11 = (bf16[128,2048]{1,0:T(8,128)(2,1)S(1)}, bf16[128,2048]{1,0:T(8,128)(2,1)S(1)}, u32[]{:S(2)}, u32[]{:S(2)}) collective-permute-start(bf16[128,2048]{1,0:T(8,128)(2,1)S(1)} %pad_maximum_fusion.refs_4_), channel_id=1, source_target_pairs={{0,1},{1,0},{2,3},{3,2},{4,5},{5,4},{6,7},{7,6},{8,9},{9,8},{10,11... | collective-permute-start | bytes 1572872 | tf_op jit(solution)/shard_map/ppermute | solution.py:33
  6.3 8.1 %collective-permute-start.10 = (bf16[64,2048]{1,0:T(8,128)(2,1)}, bf16[64,2048]{1,0:T(8,128)(2,1)S(1)}, u32[]{:S(2)}, u32[]{:S(2)}) collective-permute-start(bf16[64,2048]{1,0:T(8,128)(2,1)} %get-tuple-element.25.refs_0_), channel_id=1, source_target_pairs={{0,6},{2,0},{4,2},{6,4},{1,7},{3,1},{5,3},{7,5},{8,14},{10,8},{12,... | collective-permute-start | bytes 786440 | tf_op jit(solution)/shard_map/ppermute | solution.py:33
  7.1 14.6 %collective-permute-start.8 = (bf16[64,2048]{1,0:T(8,128)(2,1)}, bf16[64,2048]{1,0:T(8,128)(2,1)S(1)}, u32[]{:S(2)}, u32[]{:S(2)}) collective-permute-start(bf16[64,2048]{1,0:T(8,128)(2,1)} %get-tuple-element.25.refs_0_), channel_id=1, source_target_pairs={{0,2},{2,4},{4,6},{6,0},{1,3},{3,5},{5,7},{7,1},{8,10},{10,12},{12... | collective-permute-start | bytes 786440 | tf_op jit(solution)/shard_map/ppermute | solution.py:33
  7.8 13.9 %collective-permute-start.9 = (bf16[64,2048]{1,0:T(8,128)(2,1)}, bf16[64,2048]{1,0:T(8,128)(2,1)S(1)}, u32[]{:S(2)}, u32[]{:S(2)}) collective-permute-start(bf16[64,2048]{1,0:T(8,128)(2,1)} %get-tuple-element.25.refs_0_), channel_id=1, source_target_pairs={{0,4},{2,6},{4,0},{6,2},{1,5},{3,7},{5,1},{7,3},{8,12},{10,14},{12... | collective-permute-start | bytes 786440 | tf_op jit(solution)/shard_map/ppermute | solution.py:33
  27.2 6.4 %collective-permute-start.14 = (bf16[512,128]{1,0:T(8,128)(2,1)S(1)}, bf16[512,128]{1,0:T(8,128)(2,1)S(1)}, u32[]{:S(2)}, u32[]{:S(2)}) collective-permute-start(bf16[512,128]{1,0:T(8,128)(2,1)S(1)} %constant_dynamic-update-slice_fusion), channel_id=1, source_target_pairs={{0,4},{1,17},{2,6},{3,19},{4,0},{5,21},{6,2},{7,23},{8,12},{9,25},... | collective-permute-start | bytes 393224 | tf_op jit(solution)/shard_map/ppermute | solution.py:361
  34.0 19.7 %collective-permute-start.16 = (bf16[4,512,128]{2,1,0:T(8,128)(2,1)S(1)}, bf16[4,512,128]{2,1,0:T(8,128)(2,1)S(1)}, u32[]{:S(2)}, u32[]{:S(2)}) collective-permute-start(bf16[4,512,128]{2,1,0:T(8,128)(2,1)S(1)} %pad_maximum_fusion.1.refs_0_), channel_id=1, source_target_pairs={{0,8},{1,3},{2,10},{3,5},{4,12},{5,7},{6,14},{7,1},{8,16},{9,11},{... | collective-permute-start | bytes 1572872 | tf_op jit(solution)/shard_map/ppermute | solution.py:361
  34.1 19.6 %collective-permute-start.17 = (bf16[4,512,128]{2,1,0:T(8,128)(2,1)S(1)}, bf16[4,512,128]{2,1,0:T(8,128)(2,1)S(1)}, u32[]{:S(2)}, u32[]{:S(2)}) collective-permute-start(bf16[4,512,128]{2,1,0:T(8,128)(2,1)S(1)} %pad_maximum_fusion.1.refs_0_), channel_id=1, source_target_pairs={{0,16},{1,5},{2,18},{3,7},{4,20},{5,1},{6,22},{7,3},{8,24},{9,13},... | collective-permute-start | bytes 1572872 | tf_op jit(solution)/shard_map/ppermute | solution.py:361
  35.3 18.9 %collective-permute-start.18 = (bf16[4,512,128]{2,1,0:T(8,128)(2,1)S(1)}, bf16[4,512,128]{2,1,0:T(8,128)(2,1)S(1)}, u32[]{:S(2)}, u32[]{:S(2)}) collective-permute-start(bf16[4,512,128]{2,1,0:T(8,128)(2,1)S(1)} %pad_maximum_fusion.1.refs_0_), channel_id=1, source_target_pairs={{0,24},{1,7},{2,26},{3,1},{4,28},{5,3},{6,30},{7,5},{8,0},{9,15},{... | collective-permute-start | bytes 1572872 | tf_op jit(solution)/shard_map/ppermute | solution.py:361
  36.8 15.0 %collective-permute-start.1 = (bf16[16,2048]{1,0:T(8,128)(2,1)S(1)}, bf16[16,2048]{1,0:T(8,128)(2,1)S(1)}, u32[]{:S(2)}, u32[]{:S(2)}) collective-permute-start(bf16[16,2048]{1,0:T(8,128)(2,1)S(1)} %copy-done.5), channel_id=1, source_target_pairs={{0,2},{2,4},{4,6},{6,0},{1,3},{3,5},{5,7},{7,1},{8,10},{10,12},{12... | collective-permute-start | bytes 196616 | tf_op jit(solution)/shard_map/ppermute | solution.py:33
  37.4 14.4 %collective-permute-start.3 = (bf16[16,2048]{1,0:T(8,128)(2,1)S(1)}, bf16[16,2048]{1,0:T(8,128)(2,1)S(1)}, u32[]{:S(2)}, u32[]{:S(2)}) collective-permute-start(bf16[16,2048]{1,0:T(8,128)(2,1)S(1)} %copy-done.5), channel_id=1, source_target_pairs={{0,4},{2,6},{4,0},{6,2},{1,5},{3,7},{5,1},{7,3},{8,12},{10,14},{12... | collective-permute-start | bytes 196616 | tf_op jit(solution)/shard_map/ppermute | solution.py:33
  51.8 28.4 %collective-permute-start.19 = (bf16[4,512,128]{2,1,0:T(8,128)(2,1)S(1)}, bf16[4,512,128]{2,1,0:T(8,128)(2,1)S(1)}, u32[]{:S(2)}, u32[]{:S(2)}) collective-permute-start(bf16[4,512,128]{2,1,0:T(8,128)(2,1)S(1)} %pad_maximum_fusion.1.refs_0_), channel_id=1, source_target_pairs={{0,1},{1,0},{2,3},{3,2},{4,5},{5,4},{6,7},{7,6},{8,9},{9,8},{10,11... | collective-permute-start | bytes 1572872 | tf_op jit(solution)/shard_map/ppermute | solution.py:33
  53.7 26.5 %collective-permute-start.20 = (bf16[4,512,128]{2,1,0:T(8,128)(2,1)S(1)}, bf16[4,512,128]{2,1,0:T(8,128)(2,1)S(1)}, u32[]{:S(2)}, u32[]{:S(2)}) collective-permute-start(bf16[4,512,128]{2,1,0:T(8,128)(2,1)S(1)} %collective-permute-done.16.refs_1_), channel_id=1, source_target_pairs={{0,1},{1,0},{2,3},{3,2},{4,5},{5,4},{6,7},{7,6},{8,9},{9,8},{10,11... | collective-permute-start | bytes 1572872 | tf_op jit(solution)/shard_map/ppermute | solution.py:33
  53.7 26.5 %collective-permute-start.21 = (bf16[4,512,128]{2,1,0:T(8,128)(2,1)S(1)}, bf16[4,512,128]{2,1,0:T(8,128)(2,1)S(1)}, u32[]{:S(2)}, u32[]{:S(2)}) collective-permute-start(bf16[4,512,128]{2,1,0:T(8,128)(2,1)S(1)} %collective-permute-done.17.refs_2_), channel_id=1, source_target_pairs={{0,1},{1,0},{2,3},{3,2},{4,5},{5,4},{6,7},{7,6},{8,9},{9,8},{10,11... | collective-permute-start | bytes 1572872 | tf_op jit(solution)/shard_map/ppermute | solution.py:33
  54.2 26.0 %collective-permute-start.22 = (bf16[4,512,128]{2,1,0:T(8,128)(2,1)S(1)}, bf16[4,512,128]{2,1,0:T(8,128)(2,1)}, u32[]{:S(2)}, u32[]{:S(2)}) collective-permute-start(bf16[4,512,128]{2,1,0:T(8,128)(2,1)S(1)} %collective-permute-done.18.refs_3_), channel_id=1, source_target_pairs={{0,1},{1,0},{2,3},{3,2},{4,5},{5,4},{6,7},{7,6},{8,9},{9,8},{10,11... | collective-permute-start | bytes 1572872 | tf_op jit(solution)/shard_map/ppermute | solution.py:33
  64.7 10.7 %collective-permute-start.7 = (bf16[128,512]{1,0:T(8,128)(2,1)}, bf16[128,512]{1,0:T(8,128)(2,1)S(1)}, u32[]{:S(2)}, u32[]{:S(2)}) collective-permute-start(bf16[128,512]{1,0:T(8,128)(2,1)} %shard_map.92.refs_0_), channel_id=1, source_target_pairs={{0,128},{32,160},{64,192},{96,224},{128,0},{160,32},{192,64},{224,... | collective-permute-start | bytes 393224 | tf_op jit(solution)/shard_map/ppermute | solution.py:33
  75.4 15.3 %collective-permute-start.27 = (bf16[128,512]{1,0:T(8,128)(2,1)}, bf16[128,512]{1,0:T(8,128)(2,1)S(1)}, u32[]{:S(2)}, u32[]{:S(2)}) collective-permute-start(bf16[128,512]{1,0:T(8,128)(2,1)} %shard_map.92.refs_0_), channel_id=1, source_target_pairs={{0,160},{32,192},{64,224},{96,0},{128,32},{160,64},{192,96},{224,1... | collective-permute-start | bytes 393224 | tf_op jit(solution)/shard_map/ppermute | solution.py:33
  80.2 10.6 %collective-permute-start.28 = (bf16[128,512]{1,0:T(8,128)(2,1)}, bf16[128,512]{1,0:T(8,128)(2,1)S(1)}, u32[]{:S(2)}, u32[]{:S(2)}) collective-permute-start(bf16[128,512]{1,0:T(8,128)(2,1)} %shard_map.92.refs_0_), channel_id=1, source_target_pairs={{0,96},{32,128},{64,160},{96,192},{128,224},{160,0},{192,32},{224,... | collective-permute-start | bytes 393224 | tf_op jit(solution)/shard_map/ppermute | solution.py:33
  83.9 16.5 %collective-permute-start.29 = (bf16[528,128]{1,0:T(8,128)(2,1)S(1)}, bf16[528,128]{1,0:T(8,128)(2,1)S(1)}, u32[]{:S(2)}, u32[]{:S(2)}) collective-permute-start(bf16[528,128]{1,0:T(8,128)(2,1)S(1)} %get-tuple-element.33), channel_id=1, source_target_pairs={{0,32},{32,64},{64,96},{96,128},{128,160},{160,192},{192,224},{224... | collective-permute-start | bytes 405512 | tf_op jit(solution)/shard_map/ppermute | solution.py:33
  87.4 15.9 %collective-permute-start.25 = (bf16[128,512]{1,0:T(8,128)(2,1)S(1)}, bf16[128,512]{1,0:T(8,128)(2,1)S(1)}, u32[]{:S(2)}, u32[]{:S(2)}) collective-permute-start(bf16[128,512]{1,0:T(8,128)(2,1)S(1)} %copy-done.1), channel_id=1, source_target_pairs={{0,192},{32,224},{64,0},{96,32},{128,64},{160,96},{192,128},{224,1... | collective-permute-start | bytes 393224 | tf_op jit(solution)/shard_map/ppermute | solution.py:33
  90.8 12.5 %collective-permute-start.26 = (bf16[128,512]{1,0:T(8,128)(2,1)S(1)}, bf16[128,512]{1,0:T(8,128)(2,1)S(1)}, u32[]{:S(2)}, u32[]{:S(2)}) collective-permute-start(bf16[128,512]{1,0:T(8,128)(2,1)S(1)} %copy-done.1), channel_id=1, source_target_pairs={{0,64},{32,96},{64,128},{96,160},{128,192},{160,224},{192,0},{224,... | collective-permute-start | bytes 393224 | tf_op jit(solution)/shard_map/ppermute | solution.py:33
  93.4 12.5 %collective-permute-start.33 = (bf16[528,128]{1,0:T(8,128)(2,1)S(1)}, bf16[528,128]{1,0:T(8,128)(2,1)S(1)}, u32[]{:S(2)}, u32[]{:S(2)}) collective-permute-start(bf16[528,128]{1,0:T(8,128)(2,1)S(1)} %get-tuple-element.36), channel_id=1, source_target_pairs={{0,224},{32,0},{64,32},{96,64},{128,96},{160,128},{192,160},{224,1... | collective-permute-start | bytes 405512 | tf_op jit(solution)/shard_map/ppermute | solution.py:33
  100.5 8.3 %collective-permute-start.30 = (bf16[528,128]{1,0:T(8,128)(2,1)S(1)}, bf16[528,128]{1,0:T(8,128)(2,1)S(1)}, u32[]{:S(2)}, u32[]{:S(2)}) collective-permute-start(bf16[528,128]{1,0:T(8,128)(2,1)S(1)} %shard_map.99), channel_id=1, source_target_pairs={{0,32},{32,64},{64,96},{96,128},{128,160},{160,192},{192,224},{224... | collective-permute-start | bytes 405512 | tf_op jit(solution)/shard_map/ppermute | solution.py:33
  100.6 8.4 %collective-permute-start.23 = (bf16[128,512]{1,0:T(8,128)(2,1)S(1)}, bf16[128,512]{1,0:T(8,128)(2,1)S(1)}, u32[]{:S(2)}, u32[]{:S(2)}) collective-permute-start(bf16[128,512]{1,0:T(8,128)(2,1)S(1)} %copy-done.1), channel_id=1, source_target_pairs={{0,224},{32,0},{64,32},{96,64},{128,96},{160,128},{192,160},{224,1... | collective-permute-start | bytes 393224 | tf_op jit(solution)/shard_map/ppermute | solution.py:33
  103.2 5.7 %collective-permute-start.24 = (bf16[128,512]{1,0:T(8,128)(2,1)S(1)}, bf16[128,512]{1,0:T(8,128)(2,1)S(1)}, u32[]{:S(2)}, u32[]{:S(2)}) collective-permute-start(bf16[128,512]{1,0:T(8,128)(2,1)S(1)} %copy-done.1), channel_id=1, source_target_pairs={{0,32},{32,64},{64,96},{96,128},{128,160},{160,192},{192,224},{224... | collective-permute-start | bytes 393224 | tf_op jit(solution)/shard_map/ppermute | solution.py:33
  (29 other events, 167.8 us)
